TPU v7x, 512 devices: a 8x2x16 block of a 8x8x16 slice. The times are simulated.
512 devices in a mesh: grp: 2 (over y), sp: 16 (over z), tp: 16 (over x, core).
Axes of the slice: x: 8, y: 2, z: 16, core: 2. Of those that a mesh axis runs over, the one named last changes fastest.
The devices are a block of a 8x8x16 slice.
Arguments:
- hidden_items: bfloat16 [4096, 4096], P(('grp', 'sp', 'tp')), parts along dimension 0, may hold values from -6 to 6
- sample_cond: bfloat16 [8192], P('grp'), parts along dimension 0, may hold values from -6 to 6
- prompt_items: bfloat16 [256, 4096], P(('grp', 'sp')), parts along dimension 0, may hold values from -6 to 6
- prompt_cond: bfloat16 [4096], replicated, may hold values from -6 to 6
- adjust_shifting: bfloat16 [4096, 4096], P('sp', 'tp'), may hold values from -0.125 to 0.125
- adjust_stretch: bfloat16 [4096, 4096], P('sp', 'tp'), may hold values from -0.125 to 0.125
- skip_valve: bfloat16 [4096, 4096], P('sp', 'tp'), may hold values from -0.125 to 0.125
- receiver_matrix: bfloat16 [4096, 2048], P(None, 'tp'), may hold values from -0.09375 to 0.09375
- address_matrix: bfloat16 [4096, 2048], P(None, 'tp'), may hold values from -0.09375 to 0.09375
- payload_matrix: bfloat16 [4096, 2048], P(None, 'tp'), may hold values from -0.09375 to 0.09375
- joint_lower_projector: bfloat16 [4096, 64], P('sp'), may hold values from -0.09375 to 0.09375
- fading_raise_matrix: bfloat16 [64, 2048], P(None, 'tp'), may hold values from -1.5 to 1.5
- step_raise_matrix: bfloat16 [64, 2048], P(None, 'tp'), may hold values from -1.5 to 1.5
- feature_fading: float32 [2048], P('tp'), may hold values from 0 to 0.1, as said below
- spike_logfade: float32 [4096, 32], P(('grp', 'sp'), 'tp'), parts along dimension 0, may hold values from 0 to 2
- group_standard_factor: float32 [2048], P('tp'), may hold values from 0.1 to 1.9
- emit_matrix: bfloat16 [2048, 4096], P('tp', 'sp'), may hold values from -0.125 to 0.125
Outputs:
- latent_out: bfloat16 [4096, 4096], P(('grp', 'sp', 'tp')), parts along dimension 0
There are 2 independent parts, one for each index of `grp`. A program takes and returns all parts, laid end to end along the dimension named above; an argument that names none is the same for every part. Nothing has to cross between parts.
Inputs may be any that keep to these rules, and one draw needn't show every extreme that they name: `feature_fading`: per-token decay rate of each channel.
All inputs are finite; a program needn't handle non-finite values.
Results may differ from a plain program's by a relative error of at most 0.015.
Values may be sent and summed in bfloat16 or wider, within the bound.
No kernel may reach another device: no remote copies, remote signals or barrier semaphores. Data moves between devices by JAX's collectives and lax.ppermute only.
A program may use at most 64 MiB of HBM per device.

v0:
```python
import math

import jax
import jax.numpy as jnp
from jax import lax
from jax.sharding import PartitionSpec as P

ATTEND_WIDTH = 64


EPS_ROW = 1e-05
EPS_HEAD = 0.00064
EPS_KEY = 1e-06
rate_shift = 5.0


def copy_for_each(shard, axis):
    peers = lax.axis_size(axis)
    return lax.all_to_all(
        jnp.broadcast_to(shard[None], (peers, *shard.shape)), axis, 0, 0, tiled=True
    )


def of_everyone(shard, axis):
    return copy_for_each(shard, axis).sum(axis=0)


def packed_total(arrays, axis):
    vector, at, gathered = (jnp.concatenate([a.reshape(-1) for a in arrays]), 0, [])
    subtotal = of_everyone(vector, axis)
    for a in arrays:
        gathered.append(subtotal[at : at + a.size].reshape(a.shape))
        at += a.size
    return tuple(gathered)


def in_one_piece(arrays, axis, dim, along):
    ends, at = ([], 0)
    for a in arrays[:-1]:
        at += a.shape[along]
        ends.append(at)
    both = jnp.concatenate(arrays, axis=along)
    return tuple(jnp.split(lax.all_gather(both, axis, axis=dim, tiled=True), ends, axis=along))


def rows_first(arrays, axis, dims):
    turned = [jnp.moveaxis(a, dim, 0) for a, dim in zip(arrays, dims)]
    both = jnp.concatenate([t.reshape(len(t), -1) for t in turned], axis=1)
    result, at, gathered = (lax.all_gather(both, axis, axis=0, tiled=True), 0, [])
    for t, dim in zip(turned, dims):
        slab = result[:, at : at + t[0].size].reshape(-1, *t.shape[1:])
        gathered.append(jnp.moveaxis(slab, 0, dim))
        at += t[0].size
    return tuple(gathered)


def collected_together(shard, axis):
    leaves = jax.tree.leaves(shard)
    order = sorted(range(len(leaves)), key=lambda k: -leaves[k].size)
    width = (1, *leaves[order[0]].shape)[-1]
    lines = [
        jnp.pad(leaves[k].reshape(-1), (0, -leaves[k].size % width)).reshape(-1, width)
        for k in order
    ]
    both, at, found = (lax.all_gather(jnp.concatenate(lines), axis), 0, {})
    for k, line in zip(order, lines):
        slab = both[:, at : at + len(line)].reshape(len(both), -1)
        found[k] = slab[:, : leaves[k].size].reshape(-1, *leaves[k].shape)
        at += len(line)
    numbers = iter(range(len(leaves)))
    return jax.tree.map(lambda _: found[next(numbers)], shard)


def entering(shard, axis, combine, identity):
    peers, mine = (lax.axis_size(axis), lax.axis_index(axis))
    everything = collected_together(
        jax.tree.map(lambda part, kind: part.astype(kind), shard, (jnp.bfloat16, jnp.bfloat16)),
        axis,
    )
    start = jax.tree.map(
        lambda part, zero: jnp.broadcast_to(jnp.asarray(zero, part.dtype), part.shape),
        shard,
        identity,
    )

    def step(k, before):
        reached = k < mine
        new = combine(
            before, jax.tree.map(lambda part, own: part[k].astype(own.dtype), everything, shard)
        )
        return jax.tree.map(lambda a, b: jnp.where(reached, a, b), new, before)

    return lax.fori_loop(0, peers, step, start)


def gathered_once(shard, axis):
    leaves = jax.tree.leaves(shard)
    order = sorted(range(len(leaves)), key=lambda k: -leaves[k].size)
    width = (1, *leaves[order[0]].shape)[-1]
    lines = [
        jnp.pad(leaves[k].reshape(-1), (0, -leaves[k].size % width)).reshape(-1, width)
        for k in order
    ]
    both, at, found = (copy_for_each(jnp.concatenate(lines), axis), 0, {})
    for k, line in zip(order, lines):
        slab = both[:, at : at + len(line)].reshape(len(both), -1)
        found[k] = slab[:, : leaves[k].size].reshape(-1, *leaves[k].shape)
        at += len(line)
    numbers = iter(range(len(leaves)))
    return jax.tree.map(lambda _: found[next(numbers)], shard)


def folded_in_pairs(pieces, combine):
    while len(jax.tree.leaves(pieces)[0]) > 1:
        pieces = jax.vmap(combine)(
            *(jax.tree.map(lambda part: part[side::2], pieces) for side in (0, 1))
        )
    return jax.tree.map(lambda part: part[0], pieces)


def entering_2(shard, axis, combine, identity):
    peers, mine = (lax.axis_size(axis), lax.axis_index(axis))
    passed = jnp.arange(peers) > mine

    def kept(part, zero, own):
        part = jnp.where(
            passed.reshape(-1, *(1 for _ in own.shape)),
            part.astype(own.dtype),
            jnp.asarray(zero, own.dtype),
        )
        return part[::-1]

    pieces = gathered_once(
        jax.tree.map(lambda part, kind: part.astype(kind), shard, (jnp.bfloat16, jnp.bfloat16)),
        axis,
    )
    return folded_in_pairs(jax.tree.map(kept, pieces, identity, shard), combine)


def cut_along(shard, dim, peers):
    dims = shard.shape
    tiles = shard.reshape(*dims[:dim], peers, dims[dim] // peers, *dims[dim + 1 :])
    return jnp.moveaxis(tiles, dim, 0)


def sent_and_summed(shard, axis, dim):
    peers = lax.axis_size(axis)
    tiles = lax.all_to_all(cut_along(shard, dim, peers), axis, 0, 0, tiled=True)
    return jnp.sum(tiles.astype(jnp.float32), axis=0)


def stored(value):
    return lax.optimization_barrier(value.astype(jnp.bfloat16))


def product(left, right):
    return jnp.dot(left, right, preferred_element_type=jnp.float32)


def batch_dot(left, right):
    return jnp.matmul(left, right)


def flipped(tensor):
    return jnp.swapaxes(tensor, -1, -2)


def modulate(rows, shifts, scales):
    values = rows.astype(jnp.float32)
    centre = jnp.mean(values, -1, keepdims=True)
    spread = jnp.mean(jnp.square(values - centre), -1, keepdims=True)
    normed = (values - centre) * lax.rsqrt(spread + EPS_ROW)
    return (normed * (1.0 + scales) + shifts).astype(jnp.bfloat16)


def both_ways(tensor):
    return jnp.stack([tensor, jnp.flip(tensor, axis=1)])


def chain_inputs(
    key_rows,
    value_rows,
    low_rows,
    query_rows,
    fading_raise_matrix,
    step_raise_matrix,
    feature_fading,
    surplus_entries,
):
    row_count = key_rows.shape[0]
    head_count = key_rows.shape[1] // ATTEND_WIDTH
    squashed = jnp.tanh(low_rows.astype(jnp.float32)).astype(jnp.bfloat16)
    logdecay = (
        -feature_fading * jax.nn.sigmoid(product(squashed, fading_raise_matrix)) - surplus_entries
    )
    learned = jax.nn.sigmoid(product(squashed, step_raise_matrix) - rate_shift)

    def by_head(tensor):
        return jnp.transpose(
            tensor.astype(jnp.float32).reshape(row_count, head_count, ATTEND_WIDTH), (1, 0, 2)
        )

    key_heads = by_head(key_rows)
    unit_keys = key_heads * lax.rsqrt(jnp.sum(key_heads * key_heads, -1, keepdims=True) + EPS_KEY)
    removal = unit_keys * by_head(learned)
    return tuple(
        (
            both_ways(tensor)
            for tensor in (
                by_head(logdecay),
                key_heads,
                by_head(value_rows),
                unit_keys,
                removal,
                by_head(query_rows),
            )
        )
    )


def sub_block(carried, inputs, reading):
    logdecay, key_heads, value_heads, unit_keys, removal, query_heads = inputs
    sub_len = logdecay.shape[-2]
    totals = jnp.cumsum(logdecay, axis=-2)
    inclusive = jnp.exp(totals)
    exclusive = jnp.exp(totals - logdecay)
    inverse = jnp.exp(-totals)
    probed = exclusive * unit_keys
    key_in = key_heads * inverse
    removal_in = removal * inverse
    places = lax.iota(jnp.int32, sub_len)
    strict = (places[:, None] > places[None, :]).astype(jnp.float32)
    system = batch_dot(probed, flipped(removal_in)) * strict + jnp.eye(sub_len, dtype=jnp.float32)
    right_side = batch_dot(probed, flipped(carried)) + batch_dot(
        batch_dot(probed, flipped(key_in)) * strict, value_heads
    )
    solved = jax.scipy.linalg.solve_triangular(system, right_side, lower=True, unit_diagonal=True)
    final_row = inclusive[..., -1:, :]
    ending = (
        carried * final_row
        + batch_dot(flipped(value_heads), key_in * final_row)
        - batch_dot(flipped(solved), removal_in * final_row)
    )
    if not reading:
        return (ending, jnp.zeros((), jnp.float32))
    weighted = inclusive * query_heads
    upto_mask = (places[:, None] >= places[None, :]).astype(jnp.float32)
    outputs = (
        batch_dot(weighted, flipped(carried))
        + batch_dot(batch_dot(weighted, flipped(key_in)) * upto_mask, value_heads)
        - batch_dot(batch_dot(weighted, flipped(removal_in)) * upto_mask, solved)
    )
    return (ending, outputs)


def run_chain(carried, inputs, reading):
    length = inputs[0].shape[-2]
    sub_len = math.gcd(64, length)

    def to_blocks(tensor):
        leading = tensor.shape[:-2]
        shaped = tensor.reshape(leading + (length // sub_len, sub_len, tensor.shape[-1]))
        return jnp.moveaxis(shaped, -3, 0)

    def advance(state_now, pieces):
        return sub_block(state_now, pieces, reading)

    ending, outputs = lax.scan(advance, carried, tuple((to_blocks(tensor) for tensor in inputs)))
    if reading:
        outputs = jnp.moveaxis(outputs, 0, -3)
        outputs = outputs.reshape(outputs.shape[:-3] + (length, outputs.shape[-1]))
    return (ending, outputs)


def shards(
    hidden_items,
    sample_cond,
    prompt_items,
    prompt_cond,
    adjust_shifting,
    adjust_stretch,
    skip_valve,
    receiver_matrix,
    address_matrix,
    payload_matrix,
    joint_lower_projector,
    fading_raise_matrix,
    step_raise_matrix,
    feature_fading,
    spike_logfade,
    group_standard_factor,
    emit_matrix,
):
    width = hidden_items.shape[1]
    span_rows = adjust_shifting.shape[0]
    conditions = jnp.stack([sample_cond, prompt_cond])
    activated = jax.nn.silu(conditions.astype(jnp.float32)).astype(jnp.bfloat16)
    own_cols = lax.dynamic_slice_in_dim(activated, lax.axis_index("sp") * span_rows, span_rows, 1)
    part_shift = product(own_cols, adjust_shifting)
    part_scale = product(own_cols, adjust_stretch)
    part_gate = product(own_cols[:1], skip_valve)
    summed = packed_total((part_shift, part_scale, part_gate), "sp")
    shifts, scales, gates = in_one_piece((summed[0], summed[1], summed[2]), "tp", 1, 0)
    out_weight, down_weight = rows_first((emit_matrix, joint_lower_projector), "sp", (1, 0))
    u_rows = modulate(hidden_items, shifts[0], scales[0])
    low_own = stored(product(u_rows, down_weight))
    joined = jnp.concatenate([u_rows, low_own], axis=1)
    portion = lax.all_gather(joined, "tp", axis=0, tiled=True)
    features = portion[:, :width]
    gathered = jnp.concatenate(
        [
            stored(product(features, receiver_matrix)),
            stored(product(features, address_matrix)),
            stored(product(features, payload_matrix)),
            portion[:, width:],
        ],
        axis=1,
    )
    head_cols = receiver_matrix.shape[1]
    head_count = head_cols // ATTEND_WIDTH
    ctx_mod = modulate(prompt_items, shifts[1], scales[1])
    ctx_keys, ctx_values, ctx_low = in_one_piece(
        (
            stored(product(ctx_mod, address_matrix)),
            stored(product(ctx_mod, payload_matrix)),
            stored(product(ctx_mod, down_weight)),
        ),
        "sp",
        0,
        1,
    )
    ctx_inputs = chain_inputs(
        ctx_keys,
        ctx_values,
        ctx_low,
        ctx_keys,
        fading_raise_matrix,
        step_raise_matrix,
        feature_fading,
        0.0,
    )
    zeroed = jnp.zeros((2, head_count, ATTEND_WIDTH, ATTEND_WIDTH), jnp.float32)
    ctx_state, _ = run_chain(zeroed, ctx_inputs, False)
    surplus_entries = jnp.repeat(spike_logfade, ATTEND_WIDTH, axis=1)
    lat_inputs = chain_inputs(
        gathered[:, head_cols : 2 * head_cols],
        gathered[:, 2 * head_cols : 3 * head_cols],
        gathered[:, 3 * head_cols :],
        gathered[:, :head_cols],
        fading_raise_matrix,
        step_raise_matrix,
        feature_fading,
        surplus_entries,
    )
    identity_maps = jnp.broadcast_to(
        jnp.eye(ATTEND_WIDTH, dtype=jnp.float32), (2, head_count, ATTEND_WIDTH, ATTEND_WIDTH)
    )
    augmented = jnp.concatenate([jnp.zeros_like(identity_maps), identity_maps], axis=2)
    padded_values = jnp.concatenate([lat_inputs[2], jnp.zeros_like(lat_inputs[2])], axis=3)
    ending, _ = run_chain(augmented, lat_inputs[:2] + (padded_values,) + lat_inputs[3:], False)
    offsets = ending[:, :, :ATTEND_WIDTH]
    factors = ending[:, :, ATTEND_WIDTH:]

    def compose(early, later):
        return (batch_dot(early[0], later[0]), batch_dot(early[1], later[0]) + later[1])

    unit_map = (identity_maps[0], jnp.zeros_like(identity_maps[0]))
    ahead = entering((factors[0], offsets[0]), "sp", compose, unit_map)
    behind = entering_2((factors[1], offsets[1]), "sp", compose, unit_map)
    starting = jnp.stack(
        [
            batch_dot(ctx_state[0], ahead[0]) + ahead[1],
            batch_dot(ctx_state[1], behind[0]) + behind[1],
        ]
    )
    _, outputs = run_chain(starting, lat_inputs, True)
    combined = outputs[0] + jnp.flip(outputs[1], axis=1)
    centre = jnp.mean(combined, -1, keepdims=True)
    spread = jnp.mean(jnp.square(combined - centre), -1, keepdims=True)
    gains = group_standard_factor.reshape(head_count, 1, ATTEND_WIDTH)
    normed = (combined - centre) * lax.rsqrt(spread + EPS_HEAD) * gains
    row_total = combined.shape[1]
    normed = jnp.transpose(normed, (1, 0, 2)).reshape(row_total, head_cols).astype(jnp.bfloat16)
    mixed_sum = sent_and_summed(product(normed, out_weight).astype(jnp.bfloat16), "tp", 0)
    return (hidden_items.astype(jnp.float32) + gates[0] * mixed_sum).astype(jnp.bfloat16)


def solution(mesh):
    placed = (
        P(("grp", "sp", "tp"), None),
        P("grp"),
        P(("grp", "sp"), None),
        P(),
        P("sp", "tp"),
        P("sp", "tp"),
        P("sp", "tp"),
        P(None, "tp"),
        P(None, "tp"),
        P(None, "tp"),
        P("sp", None),
        P(None, "tp"),
        P(None, "tp"),
        P("tp"),
        P(("grp", "sp"), "tp"),
        P("tp"),
        P("tp", "sp"),
    )
    return jax.shard_map(
        shards, mesh=mesh, in_specs=placed, out_specs=P(("grp", "sp", "tp"), None), check_vma=False
    )
```

profile of v0, /device:TPU:65, one launch (start us, length us, event | category | flops | bytes accessed | tf_op | source)
XLA Modules:
  0.0 458.1 jit_solution(16582487184394105169)
XLA Ops:
  8.2 1.0 fusion.132
  9.2 1.1 convolution_bitcast_fusion.3
  10.4 1.1 convolution_bitcast_fusion.4
  12.1 44.2 %all-to-all-start = ((f32[16,1,1280]{2,1,0:T(1,128)}), f32[16,1,1280]{2,1,0:T(1,128)S(1)}, u32[]{:S(2)}, u32[]{:S(2)}) async-start(f32[16,1,1280]{2,1,0:T(1,128)} %broadcast_in_dim.39), calls=%async_computation | async-start | bytes 163840 | tf_op jit(solution)/shard_map/all_to_all | solution.py:19
  56.4 1.5 pad_maximum_fusion.2
  60.3 7.6 %all-to-all-done = f32[16,1,1280]{2,1,0:T(1,128)S(1)} async-done(((f32[16,1,1280]{2,1,0:T(1,128)}), f32[16,1,1280]{2,1,0:T(1,128)S(1)}, u32[]{:S(2)}, u32[]{:S(2)}) %all-to-all-start) | async-done | bytes 81952 | tf_op jit(solution)/shard_map/all_to_all | solution.py:19
  68.0 20.4 %all_gather.18 = f32[5,4096]{1,0:T(8,128)S(1)} all-gather(f32[5,256]{1,0:T(8,128)S(1)} %pad_maximum_fusion.7), channel_id=1, replica_groups=mesh['grp'=2,'sp'=16,'tp'=16] {'tp'}, dimensions={1}, use_global_device_ids=true | all-gather | bytes 87040 | tf_op jit(solution)/shard_map/all_gather | solution.py:43
  89.3 38.7 %all-gather.4.cloned.1.call-done = bf16[4096,192]{0,1:T(8,128)(2,1)} async-done(((bf16[256,192]{0,1:T(8,128)(2,1)}), bf16[4096,192]{0,1:T(8,128)(2,1)}) %all-gather.4.cloned.1.call-update) | async-done | bytes 1572880 | tf_op jit(solution)/shard_map/all_gather | solution.py:49
  128.0 1.3 convolution_convert_fusion.5
  129.3 21.7 %all_gather.20 = bf16[128,320]{1,0:T(8,128)(2,1)S(1)} all-gather(bf16[8,320]{1,0:T(8,128)(2,1)S(1)} %pad_maximum_fusion.8), channel_id=1, replica_groups=mesh['grp'=2,'sp'=16,'tp'=16] {'sp'}, dimensions={0}, use_global_device_ids=true | all-gather | bytes 87040 | tf_op jit(solution)/shard_map/all_gather | solution.py:43
  152.9 1.3 convolution_convert_fusion.4
  155.7 1.0 maximum_bitcast_fusion
  157.0 46.8 %while.51 = (s32[]{:T(128)}, f32[2,2,64,64]{3,2,1,0:T(8,128)S(1)}, f32[2,2,2,64,64]{3,0,4,2,1:T(2,128)}, f32[2,2,2,64,64]{3,0,4,2,1:T(2,128)S(1)}, f32[2,2,2,64,...) while((s32[]{:T(128)}, f32[2,2,64,64]{3,2,1,0:T(8,128)S(1)}, ...), condition=%wide.region_6.8_spmd.clone, body=%wide.region_4.7_spmd.clone.sunk | while | flops 26669124 | bytes 3338888 | solution.py:268
  157.3 1.1 constant_dynamic-slice_fusion.16
  160.1 19.7 %custom-call.18 = f32[2,2,1,64,64]{3,4,2,1,0:T(8,128)S(1)} custom-call(f32[2,2,1,64,64]{4,3,2,1,0:T(8,128)S(1)} %fusion.288), custom_call_target="InvertDiagBlocksLowerTriangular" | custom-call | tf_op jit(solution)/shard_map/while/body/eval_jaxpr/jit(_solve_triangular)/vmap(vmap())/triangular_solve | solution.py:237
  180.7 1.1 constant_dynamic-slice_fusion.16
  183.5 19.7 %custom-call.18 = f32[2,2,1,64,64]{3,4,2,1,0:T(8,128)S(1)} custom-call(f32[2,2,1,64,64]{4,3,2,1,0:T(8,128)S(1)} %fusion.288), custom_call_target="InvertDiagBlocksLowerTriangular" | custom-call | tf_op jit(solution)/shard_map/while/body/eval_jaxpr/jit(_solve_triangular)/vmap(vmap())/triangular_solve | solution.py:237
  203.8 10.1 %all-gather.6.cloned.1.call-done = bf16[128,4160]{1,0:T(8,128)(2,1)} async-done(((bf16[8,4160]{1,0:T(8,128)(2,1)}), bf16[128,4160]{1,0:T(8,128)(2,1)}) %all-gather.6.cloned.1.call-update) | async-done | bytes 1064976 | tf_op jit(solution)/shard_map/all_gather | solution.py:308
  213.9 1.0 fusion.83
  215.2 1.7 convolution_convert_fusion.2
  217.2 1.0 fusion.78
  220.3 1.6 convolution_convert_fusion.3
  224.1 42.9 %while.49 = (s32[]{:T(128)}, f32[2,2,128,64]{2,3,1,0:T(8,128)S(1)}, f32[2,2,2,64,64]{4,3,2,1,0:T(8,128)S(1)}, bf16[2,2,2,64,128]{4,3,0,2,1:T(8,128)(2,1)S(1)}, f...) while((s32[]{:T(128)}, f32[2,2,128,64]{2,3,1,0:T(8,128)S(1)}, ...), condition=%wide.region_12.14_spmd, body=%wide.region_10.13_spmd.sunk | while | flops 47673408 | bytes 4268149 | solution.py:268
  225.3 19.7 %custom-call.16 = f32[2,2,1,64,64]{3,4,2,1,0:T(8,128)S(1)} custom-call(f32[2,2,1,64,64]{4,3,2,1,0:T(8,128)S(1)} %fusion.251), custom_call_target="InvertDiagBlocksLowerTriangular" | custom-call | tf_op jit(solution)/shard_map/while/body/eval_jaxpr/jit(_solve_triangular)/vmap(vmap())/triangular_solve | solution.py:237
  246.7 19.7 %custom-call.16 = f32[2,2,1,64,64]{3,4,2,1,0:T(8,128)S(1)} custom-call(f32[2,2,1,64,64]{4,3,2,1,0:T(8,128)S(1)} %fusion.251), custom_call_target="InvertDiagBlocksLowerTriangular" | custom-call | tf_op jit(solution)/shard_map/while/body/eval_jaxpr/jit(_solve_triangular)/vmap(vmap())/triangular_solve | solution.py:237
  267.4 0.8 broadcast_in_dim.44
  268.3 12.5 %all-to-all-start.1 = ((bf16[16,256,64]{1,2,0:T(8,128)(2,1)}), bf16[16,256,64]{1,2,0:T(8,128)(2,1)S(1)}, u32[]{:S(2)}, u32[]{:S(2)}) async-start(bf16[16,256,64]{1,2,0:T(8,128)(2,1)} %broadcast_in_dim.44), calls=%async_computation.1 | async-start | bytes 1048576 | tf_op jit(solution)/shard_map/all_to_all | solution.py:19
  281.1 45.0 %all-gather = bf16[4096,64]{0,1:T(8,128)(2,1)S(1)} all-gather(bf16[256,64]{0,1:T(8,128)(2,1)S(1)} %pad_maximum_fusion.4), channel_id=2, replica_groups=mesh['grp'=2,'sp'=16,'tp'=16] {'sp'}, dimensions={0}, use_global_device_ids=true | all-gather | bytes 557056 | tf_op jit(solution)/shard_map/all_gather | solution.py:65
  326.4 1.1 reshape_reshape.8
  327.5 1.1 reshape_reshape.9
  328.6 18.0 %while.52 = (s32[]{:T(128)}, bf16[2,64,64]{1,2,0:T(8,128)(2,1)S(1)}, f32[2,64,64]{1,2,0:T(8,128)S(1)}, s32[]{:T(128)}, bf16[16,2,64,64]{2,1,3,0:T(2,128)(2,1)}, ...) while((s32[]{:T(128)}, bf16[2,64,64]{1,2,0:T(8,128)(2,1)S(1)}, ...), condition=%wide.region_14.16_spmd.clone, body=%wide.region_13.15_spmd.clone.sunk | while | flops 2146308 | bytes 311414 | solution.py:93
  328.7 0.8 constant_dynamic-slice_fusion.18
  329.8 0.8 constant_dynamic-slice_fusion.18
  330.9 0.8 constant_dynamic-slice_fusion.18
  332.0 0.8 constant_dynamic-slice_fusion.18
  333.2 0.8 constant_dynamic-slice_fusion.18
  334.3 0.8 constant_dynamic-slice_fusion.18
  346.9 2.0 convolution_convert_fusion.1
  350.2 1.1 maximum_bitcast_fusion.9
  351.3 1.0 fusion.140
  352.3 1.4 copy.217
  358.2 49.5 %while.50 = (s32[]{:T(128)}, f32[2,2,64,64]{3,2,1,0:T(8,128)S(1)}, f32[2,2,2,64,64]{4,3,2,1,0:T(8,128)}, f32[2,2,2,64,64]{4,3,2,1,0:T(8,128)S(1)}, f32[2,2,2,64,...) while((s32[]{:T(128)}, f32[2,2,64,64]{3,2,1,0:T(8,128)S(1)}, ...), condition=%wide.region_17.19_spmd, body=%wide.region_15.18_spmd.sunk | while | flops 37163072 | bytes 5173957 | solution.py:268
  358.2 1.3 constant_dynamic-slice_fusion.14
  360.9 19.7 %custom-call.17 = f32[2,2,1,64,64]{3,4,2,1,0:T(8,128)S(1)} custom-call(f32[2,2,1,64,64]{4,3,2,1,0:T(8,128)S(1)} %fusion.273), custom_call_target="InvertDiagBlocksLowerTriangular" | custom-call | tf_op jit(solution)/shard_map/while/body/eval_jaxpr/jit(_solve_triangular)/vmap(vmap())/triangular_solve | solution.py:237
  383.0 1.3 constant_dynamic-slice_fusion.14
  385.7 19.7 %custom-call.17 = f32[2,2,1,64,64]{3,4,2,1,0:T(8,128)S(1)} custom-call(f32[2,2,1,64,64]{4,3,2,1,0:T(8,128)S(1)} %fusion.273), custom_call_target="InvertDiagBlocksLowerTriangular" | custom-call | tf_op jit(solution)/shard_map/while/body/eval_jaxpr/jit(_solve_triangular)/vmap(vmap())/triangular_solve | solution.py:237
  407.7 1.1 fusion.141
  410.0 39.7 %all_to_all.16 = bf16[16,8,4096]{2,1,0:T(8,128)(2,1)S(1)} all-to-all(bf16[16,8,4096]{2,1,0:T(8,128)(2,1)S(1)} %fusion.70), channel_id=1, replica_groups=mesh['grp'=2,'sp'=16,'tp'=16] {'tp'}, dimensions={0} | all-to-all | bytes 2097152 | tf_op jit(solution)/shard_map/all_to_all | solution.py:148
  (386 shorter events, 51.7 us)
Async XLA Ops:
  6.5 82.3 %copy-start = (bf16[4096,128]{1,0:T(8,128)(2,1)S(1)}, bf16[4096,128]{1,0:T(8,128)(2,1)}, u32[]{:S(2)}) copy-start(bf16[4096,128]{1,0:T(8,128)(2,1)} %param.35) | copy-start | bytes 3145732
  6.6 51.5 %copy-start.3 = (bf16[8,4096]{1,0:T(8,128)(2,1)S(1)}, bf16[8,4096]{1,0:T(8,128)(2,1)}, u32[]{:S(2)}) copy-start(bf16[8,4096]{1,0:T(8,128)(2,1)} %param.27) | copy-start | bytes 196612
  6.6 51.9 %copy-start.7 = (bf16[8,4096]{1,0:T(8,128)(2,1)S(1)}, bf16[8,4096]{1,0:T(8,128)(2,1)}, u32[]{:S(2)}) copy-start(bf16[8,4096]{1,0:T(8,128)(2,1)} %param.29) | copy-start | bytes 196612
  6.6 53.0 %copy-start.27 = (f32[128]{0:T(128)S(1)}, f32[128]{0:T(128)}, u32[]{:S(2)}) copy-start(f32[128]{0:T(128)} %param.40) | copy-start | bytes 1540
  6.6 53.0 %copy-start.28 = (f32[128]{0:T(128)S(1)}, f32[128]{0:T(128)}, u32[]{:S(2)}) copy-start(f32[128]{0:T(128)} %param.42) | copy-start | bytes 1540
  9.2 79.3 %copy-start.5 = (bf16[4096,128]{1,0:T(8,128)(2,1)S(1)}, bf16[4096,128]{1,0:T(8,128)(2,1)}, u32[]{:S(2)}) copy-start(bf16[4096,128]{1,0:T(8,128)(2,1)} %param.36) | copy-start | bytes 3145732
  12.1 55.8 %all-to-all-start = ((f32[16,1,1280]{2,1,0:T(1,128)}), f32[16,1,1280]{2,1,0:T(1,128)S(1)}, u32[]{:S(2)}, u32[]{:S(2)}) async-start(f32[16,1,1280]{2,1,0:T(1,128)} %broadcast_in_dim.39), calls=%async_computation | async-start | bytes 163840 | tf_op jit(solution)/shard_map/all_to_all | solution.py:19
  56.3 71.6 %all-gather.4.cloned.1.call-start = ((), (), s32[]{:S(2)}) async-start(), calls=%async_computation.3 | async-start | bytes 1671168 | tf_op jit(solution)/shard_map/all_gather | solution.py:49
  58.0 155.9 %all-gather.6.cloned.1.call-start = ((), (), s32[]{:S(2)}) async-start(), calls=%async_computation.4 | async-start | bytes 1148928 | tf_op jit(solution)/shard_map/all_gather | solution.py:308
  58.1 2.1 copy-start.11
  59.5 0.7 copy-start.13
  88.9 62.2 %copy-start.24 = (bf16[64,128]{1,0:T(8,128)(2,1)S(1)}, bf16[64,128]{1,0:T(8,128)(2,1)}, u32[]{:S(2)}) copy-start(bf16[64,128]{1,0:T(8,128)(2,1)} %param.38) | copy-start | bytes 49156
  129.3 22.9 %copy-start.25 = (bf16[64,128]{1,0:T(8,128)(2,1)S(1)}, bf16[64,128]{1,0:T(8,128)(2,1)}, u32[]{:S(2)}) copy-start(bf16[64,128]{1,0:T(8,128)(2,1)} %param.39) | copy-start | bytes 49156
  157.0 56.9 %copy-start.22 = (f32[128,2]{0,1:T(2,128)S(1)}, f32[128,2]{0,1:T(2,128)}, u32[]{:S(2)}) copy-start(f32[128,2]{0,1:T(2,128)} %param.41) | copy-start | bytes 3076
  215.1 2.0 copy-start.26
  218.2 2.2 copy-start.6
  222.0 1.1 copy-start.16
  222.2 0.6 copy-start.8
  222.8 0.8 copy-start.15
  268.3 83.0 %all-to-all-start.1 = ((bf16[16,256,64]{1,2,0:T(8,128)(2,1)}), bf16[16,256,64]{1,2,0:T(8,128)(2,1)S(1)}, u32[]{:S(2)}, u32[]{:S(2)}) async-start(bf16[16,256,64]{1,2,0:T(8,128)(2,1)} %broadcast_in_dim.44), calls=%async_computation.1 | async-start | bytes 1048576 | tf_op jit(solution)/shard_map/all_to_all | solution.py:19
  326.4 2.2 copy-start.14
  328.6 18.1 %copy-start.9 = (f32[2,128,64]{1,2,0:T(8,128)S(1)}, f32[2,128,64]{1,2,0:T(8,128)}, u32[]{:S(2)}) copy-start(f32[2,128,64]{1,2,0:T(8,128)} %copy-done.8) | copy-start | bytes 196612
  352.3 1.4 copy-start.21
  353.9 1.6 copy-start.2
  353.9 1.9 copy-start.12
  356.0 1.0 copy-start.10
  356.0 1.1 copy-start.19
  357.3 0.9 copy-start.20
  381.0 1.0 copy-start.17
  382.2 0.7 copy-start.18
  405.7 1.0 copy-start.17
  407.0 0.7 copy-start.18
  407.7 1.8 copy-start.23
  407.7 1.9 copy-start.1
  449.8 0.8 copy-start.4
Sparse Core Ops, SparseCore 0:
  59.2 68.7 all-gather.3
  155.0 58.8 all-gather.5
where the time goes:
time: 460 us; the launch traced here: 458 us
  other arithmetic  129 us (28%)
  blocking collectives  127 us (28%)
  starting transfers between devices  56.9 us (12%)
  waiting for transfers between devices  56.5 us (12%)
  local copies, waits for them, and re-layouts  42.8 us (9%)
  matrix products  30.6 us (7%)
  between operations  14.5 us (3%)
    another operation x18, other arithmetic, sub_block(): jax.scipy.linalg.solve_triangular(system, right_side, lower=True, unit_di...  119 us
    all_to_all x2, starting transfers between devices, copy_for_each(): lax.all_to_all(jnp.broadcast_to(shard[None], (peers, *shard.shape)), axis...  56.7 us
    all_gather x1, blocking collectives, collected_together(): both, at, found = (lax.all_gather(jnp.concatenate(lines), axis), 0, {})  45 us
    all_gather x2, blocking collectives, in_one_piece(): lax.all_gather(both, axis, axis=dim, tiled=True)  42.1 us
    all_to_all x1, blocking collectives, sent_and_summed(): tiles = lax.all_to_all(cut_along(shard, dim, peers), axis, 0, 0, tiled=True)  39.7 us
    all_gather x1, waiting for transfers between devices, rows_first(): lax.all_gather(both, axis, axis=0, tiled=True)  38.7 us
    dot_general x15, matrix products, product(): return jnp.dot(left, right, preferred_element_type=jnp.float32)  14.6 us
    dot_general x77, matrix products, batch_dot(): return jnp.matmul(left, right)  13.7 us
  transfers between devices with their start and end apart: 4, of which 3 were waited for; matrix products, arithmetic and copies ran while one was open for 17% of the time, Pallas kernels for 0%

commit v1 on v0

v1 whole, which is shorter than its diff:
```python
import jax
import jax.numpy as jnp
from jax import lax
from jax.experimental import pallas as pl
from jax.experimental.pallas import tpu as pltpu
from jax.sharding import PartitionSpec as P

HEAD = 64
EPS_ROW = 1e-05
EPS_HEAD = 0.00064
EPS_KEY = 1e-06
RATE_SHIFT = 5.0
NEVER = -1e30
BF16, F32 = jnp.bfloat16, jnp.float32

VMEM = pl.BlockSpec(memory_space=pltpu.VMEM)
SMEM = pl.BlockSpec(memory_space=pltpu.SMEM)


def call(body, outs, *args, flops=0, scalars=0, scratch=()):
    many = isinstance(outs, list)
    shapes = [jax.ShapeDtypeStruct(s, d) for s, d in (outs if many else [outs])]
    got = pl.pallas_call(
        body,
        out_shape=shapes,
        in_specs=[SMEM] * scalars + [VMEM] * (len(args) - scalars),
        out_specs=[VMEM] * len(shapes),
        scratch_shapes=list(scratch),
        compiler_params=pltpu.CompilerParams(vmem_limit_bytes=48 * 1024 * 1024),
        cost_estimate=pl.CostEstimate(
            flops=flops, transcendentals=0, bytes_accessed=sum(a.size * a.dtype.itemsize for a in args)
        ),
    )(*args)
    return got if many else got[0]


def dot(left, right, dims=((1,), (0,))):
    return lax.dot_general(
        left.astype(BF16), right.astype(BF16), (dims, ((), ())), preferred_element_type=F32
    )


def iota(shape, dim):
    return lax.broadcasted_iota(jnp.int32, shape, dim)


def partials_kernel(place, sample, prompt, shifting, stretch, valve, out):
    peers, rows, _ = out.shape
    mine = iota(sample.shape, 0) == place[0]

    def own(cond):
        return jnp.sum(jnp.where(mine, cond[...].astype(F32), 0.0), axis=0, keepdims=True)

    row = iota((rows, sample.shape[1]), 0)
    first, second = jax.nn.silu(own(sample)), jax.nn.silu(own(prompt))

    def at(k, both):
        left = jnp.where(row == k, first, 0.0)
        return jnp.where(row == k + 1, second, left) if both else left

    total = dot(at(0, True), shifting[...]) + dot(at(2, True), stretch[...])
    total = total + dot(at(4, False), valve[...])
    out[...] = jnp.broadcast_to(total[None], out.shape)


def sum_kernel(parts, out):
    total = parts[0]
    for k in range(1, parts.shape[0]):
        total = total + parts[k]
    out[...] = jnp.broadcast_to(total[None], out.shape)


def rows_kernel(latent, context, vectors, wq, wk, wv, u, q, k, v):
    count, width = latent.shape
    extra = context.shape[0]
    lane = vectors.shape[2]

    def moments(ref):
        total = jnp.zeros((ref.shape[0], lane), F32)
        for c in range(0, width, lane):
            total = total + ref[:, c : c + lane].astype(F32)
        centre = jnp.sum(total, -1, keepdims=True) * (1.0 / width)
        total = jnp.zeros((ref.shape[0], lane), F32)
        for c in range(0, width, lane):
            off = ref[:, c : c + lane].astype(F32) - centre
            total = total + off * off
        spread = jnp.sum(total, -1, keepdims=True) * (1.0 / width)
        return centre, lax.rsqrt(spread + EPS_ROW)

    lat, ctx = moments(latent), moments(context)
    pad = jnp.zeros((u.shape[0] - count - extra, lane), F32)
    for t in range(width // lane):
        cols = slice(t * lane, (t + 1) * lane)

        def one(ref, stats, i):
            normed = (ref[:, cols].astype(F32) - stats[0]) * stats[1]
            return normed * (1.0 + vectors[t, 2 + i : 3 + i, :]) + vectors[t, i : i + 1, :]

        u[:count, cols] = one(latent, lat, 0).astype(BF16)
        u[count:, cols] = jnp.concatenate([one(context, ctx, 1), pad], axis=0).astype(BF16)
    q[...] = dot(u[:count], wq[...]).astype(BF16)
    k[...] = dot(u[...], wk[...]).astype(BF16)
    v[...] = dot(u[...], wv[...]).astype(BF16)


def low_kernel(u, pieces, k, v, low, payload, down):
    _, blocks, rows, lane = pieces.shape
    span = pieces.shape[0] * rows
    for s in range(blocks):
        piece = pieces[:, s].astype(F32).reshape(span, lane)
        down[2 * s * span : (2 * s + 1) * span] = piece.astype(BF16)
        down[(2 * s + 1) * span : (2 * s + 2) * span] = pltpu.roll(piece, HEAD, 1).astype(BF16)
    result = dot(u[...], down[...])
    result = jnp.where(iota(result.shape, 1) < HEAD, result, 0.0)
    count = low.shape[0]
    low[...] = result[:count].astype(BF16)
    extra = payload.shape[1]
    for at, part in enumerate((k[count:].astype(F32), v[count:].astype(F32), result[count:])):
        part = part[:extra].astype(BF16)
        payload[:, :, at * lane : (at + 1) * lane] = jnp.broadcast_to(part[None], (payload.shape[0], extra, lane))


def inverse(mixing, row, col, upper):
    size = mixing[0].shape[0]
    eye = (row == col).astype(F32)
    width = 1
    found = None
    while width < size:
        here, there = (col, row) if upper else (row, col)
        shared = (row // (2 * width)) == (col // (2 * width))
        corner = shared & ((here // width) % 2 == 1) & ((there // width) % 2 == 0)
        parts = [jnp.where(corner, m, 0.0) for m in mixing]
        if found is None:
            found = [eye - p for p in parts]
        else:
            lefts = [dot(p, f) for p, f in zip(parts, found)]
            found = [f - dot(f, g) for f, g in zip(found, lefts)]
        width *= 2
    return found


def block_terms(k, v, low, fading, step, rates, spikes=None, q=None):
    count, lanes = k.shape
    row, col = iota((count, lanes), 0), iota((count, lanes), 1)
    heads = lanes // HEAD
    owns = [(col // HEAD) == h for h in range(heads)]

    squashed = jnp.tanh(low.astype(F32)).astype(BF16)
    feature = -rates * jax.nn.sigmoid(dot(squashed, fading))
    learned = jax.nn.sigmoid(dot(squashed, step) - RATE_SHIFT)
    key = k.astype(F32)
    norms = jnp.zeros_like(key)
    for own in owns:
        total = jnp.sum(jnp.where(own, key * key, 0.0), -1, keepdims=True)
        norms = jnp.where(own, lax.rsqrt(total + EPS_KEY), norms)
    unit = key * norms
    removal = unit * learned

    upto = (row >= col).astype(F32)

    def running(part):
        return lax.dot_general(
            upto, part, (((1,), (0,)), ((), ())), preferred_element_type=F32, precision=lax.Precision.HIGHEST
        )

    after = running(feature)
    before = after - feature
    grow, shrink = jnp.exp(after), jnp.exp(-after)
    grow_x, shrink_x = jnp.exp(before), jnp.exp(-before)
    end = after[count - 1 : count]
    if spikes is None:
        b_end = b_after = b_before = None
    else:
        jump = jnp.zeros_like(key)
        for h, own in enumerate(owns):
            jump = jnp.where(own, -spikes[:, h : h + 1], jump)
        b_after = running(jump)
        b_before = b_after - jump
        b_end = b_after[count - 1 : count]
        across_after, across_before = b_after.T, b_before.T

    def pair(h, upper, strict):
        inside = ((col > row) if strict else (col >= row)) if upper else ((col < row) if strict else (col <= row))
        if spikes is None:
            return inside.astype(F32)
        at = h * HEAD
        down_after, down_before = b_after[:, at : at + 1], b_before[:, at : at + 1]
        side_after, side_before = across_after[at : at + 1], across_before[at : at + 1]
        if upper:
            power = side_before - (down_after if strict else down_before)
        else:
            power = (down_before if strict else down_after) - side_after
        return jnp.where(inside, jnp.exp(jnp.where(inside, power, NEVER)), 0.0)

    def scaled(tensor, power):
        return tensor if spikes is None else tensor * jnp.exp(power)

    probes = (unit * grow_x, unit * shrink)
    removals = (removal * shrink, removal * grow_x)
    keys = (key * shrink, key * grow_x)
    asks = None if q is None else (q.astype(F32) * grow, q.astype(F32) * shrink_x)

    scores = []
    for d in range(2):
        right = jnp.concatenate([removals[d], keys[d]], axis=0)
        for own in owns:
            left = jnp.where(own, probes[d], 0.0)
            if q is not None:
                left = jnp.concatenate([left, jnp.where(own, asks[d], 0.0)], axis=0)
            scores.append(dot(left, right, ((1,), (1,))))
    chains = [(d, h) for d in range(2) for h in range(heads)]
    masks = {(d, h): pair(h, d == 1, True) for d, h in chains}
    mixing = {c: scores[n][:count, :count] * masks[c] for n, c in enumerate(chains)}
    seen = {c: dot(scores[n][:count, count:] * masks[c], v) for n, c in enumerate(chains)}
    solved = {}
    for d in range(2):
        found = inverse([mixing[d, h] for h in range(heads)], row, col, d == 1)
        for h in range(heads):
            solved[d, h] = found[h]

    whole = jnp.exp(end)
    starts = (
        scaled(probes[0], b_before),
        scaled(probes[1] * whole, None if spikes is None else b_end - b_after),
    )

    def gathered(parts):
        total = parts[0]
        for own, part in zip(owns[1:], parts[1:]):
            total = jnp.where(own, part, total)
        return total

    results = []
    for d in range(2):
        x, y = [], []
        for h in range(heads):
            both = dot(solved[d, h], jnp.concatenate([starts[d], seen[d, h]], axis=1))
            x.append(both[:, :lanes])
            y.append(both[:, lanes:])
        x, y = gathered(x), gathered(y)
        if d == 0:
            weigh = whole if spikes is None else whole * jnp.exp(b_end - b_after)
        else:
            weigh = jnp.ones_like(whole) if spikes is None else jnp.exp(b_before)
        last_keys, last_removals = keys[d] * weigh, removals[d] * weigh
        offset = dot(
            jnp.concatenate([v.astype(F32), -y], axis=0),
            jnp.concatenate([last_keys, last_removals], axis=0),
            ((0,), (0,)),
        )
        if q is None:
            results.append((None, offset, None, None))
            continue
        decay = whole if spikes is None else jnp.exp(end + b_end)
        factor = jnp.where(row == col, decay, 0.0) - dot(x, last_removals, ((0,), (0,)))
        if d == 0:
            query = scaled(asks[0], b_after)
        else:
            query = scaled(asks[1] * whole, None if spikes is None else b_end - b_before)
        wx, base = [], []
        for h in range(heads):
            n = chains.index((d, h))
            mask = pair(h, d == 1, False)
            reads = scores[n][count:] * jnp.concatenate([mask, mask], axis=1)
            both = dot(reads[:, :count], jnp.concatenate([x, y], axis=1))
            wx.append(both[:, :lanes])
            base.append(dot(reads[:, count:], v) - both[:, lanes:])
        results.append((factor, offset, query - gathered(wx), gathered(base)))
    return results


def same_head(shape):
    return (iota(shape, 0) // HEAD) == (iota(shape, 1) // HEAD)


def maps_kernel(place, q, k, v, low, fading, step, rates, spikes, sent, asked, base):
    count = q.shape[0]
    ahead, behind = block_terms(
        k[:count], v[:count], low[:, :HEAD], fading[...], step[...], rates[...], spikes[...], q[...]
    )
    same = same_head(ahead[0].shape)
    packed = [
        jnp.where(same, factor, pltpu.roll(offset, HEAD, 0)).astype(BF16)
        for factor, offset in (ahead[:2], behind[:2])
    ]
    for j in range(sent.shape[0]):
        sent[j] = jnp.where(place[0] < j, packed[0], packed[1])
    asked[0], asked[1] = ahead[2].astype(BF16), behind[2].astype(BF16)
    base[...] = ahead[3] + behind[3]


def context_kernel(got, fading, step, rates, state):
    blocks, extra, lanes = got.shape[0], got.shape[1], got.shape[2] // 3
    parts = [
        got[:, :, n * lanes : (n + 1) * lanes].astype(F32).reshape(blocks * extra, lanes).astype(BF16)
        for n in range(3)
    ]
    ahead, behind = block_terms(parts[0], parts[1], parts[2][:, :HEAD], fading[...], step[...], rates[...])
    same = same_head(ahead[1].shape)
    state[0], state[1] = jnp.where(same, ahead[1], 0.0), jnp.where(same, behind[1], 0.0)


def read_kernel(place, maps, state, asked, base, gains, emit, keep, give):
    peers, size, _ = maps.shape
    same = same_head((size, size))
    me, core = place[0], place[1]
    states = [state[0], state[1]]
    for n in range(peers - 1):
        for d, j, reached in ((0, n, n < me), (1, peers - 1 - n, peers - 1 - n > me)):
            packed = maps[j].astype(F32)
            factor = jnp.where(same, packed, 0.0)
            offset = jnp.where(same, pltpu.roll(packed, HEAD, 0), 0.0)
            states[d] = jnp.where(reached, dot(states[d], factor) + offset, states[d])
    out = base[...]
    for d in range(2):
        out = out + dot(asked[d], states[d], ((1,), (1,)))
    first = iota(out.shape, 1) < HEAD

    def mean(value):
        left = jnp.sum(jnp.where(first, value, 0.0), -1, keepdims=True)
        right = jnp.sum(jnp.where(first, 0.0, value), -1, keepdims=True)
        return jnp.where(first, left, right) * (1.0 / HEAD)

    out = out - mean(out)
    normed = out * lax.rsqrt(mean(out * out) + EPS_HEAD) * gains[...]
    chips, rows, width = keep.shape
    split = normed.reshape(chips, 2, rows, size)
    even, odd = split[:, 0].reshape(chips * rows, size), split[:, 1].reshape(chips * rows, size)
    mine = jnp.where(core == 0, even, odd)
    other = jnp.where(core == 0, odd, even)
    left = jnp.concatenate([mine, other], axis=0).astype(BF16)
    lane = emit.shape[2]
    for s in range(emit.shape[0]):
        part = dot(left, emit[s]).reshape(2, chips, rows, lane).astype(BF16)
        keep[:, :, s * lane : (s + 1) * lane] = part[0]
        give[:, :, s * lane : (s + 1) * lane] = part[1]


def last_kernel(parts, hidden, vectors, out):
    lane = vectors.shape[2]
    for t in range(vectors.shape[0]):
        cols = slice(t * lane, (t + 1) * lane)
        total = parts[0, :, cols].astype(F32)
        for n in range(1, parts.shape[0]):
            total = total + parts[n, :, cols].astype(F32)
        out[:, cols] = (hidden[:, cols].astype(F32) + vectors[t, 4:5, :] * total).astype(BF16)


def exchange(blocks, axis, groups=None):
    return lax.all_to_all(blocks, axis, 0, 0, tiled=True, axis_index_groups=groups)


def spread(shard, axis):
    return exchange(jnp.broadcast_to(shard[None], (lax.axis_size(axis), *shard.shape)), axis)


def shards(
    hidden_items,
    sample_cond,
    prompt_items,
    prompt_cond,
    adjust_shifting,
    adjust_stretch,
    skip_valve,
    receiver_matrix,
    address_matrix,
    payload_matrix,
    joint_lower_projector,
    fading_raise_matrix,
    step_raise_matrix,
    feature_fading,
    spike_logfade,
    group_standard_factor,
    emit_matrix,
):
    n_sp, n_tp = lax.axis_size("sp"), lax.axis_size("tp")
    me, tp = lax.axis_index("sp"), lax.axis_index("tp")
    rows, width = hidden_items.shape
    extra = prompt_items.shape[0]
    count = rows * n_tp
    lanes = receiver_matrix.shape[1]
    span, chunk = adjust_shifting.shape
    place = jnp.stack([me, tp % 2]).astype(jnp.int32)

    parts = call(
        partials_kernel,
        ((n_sp, 8, chunk), F32),
        place,
        sample_cond.reshape(-1, span),
        prompt_cond.reshape(-1, span),
        adjust_shifting,
        adjust_stretch,
        skip_valve,
        scalars=1,
        flops=8 * span * chunk * 6,
    )
    parts = exchange(parts, "sp")
    latent = spread(hidden_items, "tp").reshape(count, width)
    half = joint_lower_projector.shape[0] // 2
    packed = jnp.concatenate([joint_lower_projector[:half], joint_lower_projector[half:]], axis=1)
    piece = half // n_tp
    pieces = spread(lax.dynamic_slice_in_dim(packed, tp * piece, piece, 0), "sp")
    emit = spread(emit_matrix, "sp")

    vectors = exchange(call(sum_kernel, ((n_tp, 8, chunk), F32), parts), "tp")
    pieces = spread(pieces, "tp")

    padded = count + -(-extra // 16) * 16
    u, q, k, v = call(
        rows_kernel,
        [((padded, width), BF16), ((count, lanes), BF16), ((padded, lanes), BF16), ((padded, lanes), BF16)],
        latent,
        prompt_items,
        vectors,
        receiver_matrix,
        address_matrix,
        payload_matrix,
        flops=2 * padded * width * lanes * 3,
    )
    low, payload = call(
        low_kernel,
        [((count, lanes), BF16), ((n_sp, extra, 3 * lanes), BF16)],
        u,
        pieces,
        k,
        v,
        flops=2 * padded * width * lanes,
        scratch=[pltpu.VMEM((width, lanes), BF16)],
    )
    ctx = exchange(payload, "sp")
    rates = feature_fading.reshape(1, lanes)
    sent, asked, base = call(
        maps_kernel,
        [((n_sp, lanes, lanes), BF16), ((2, count, lanes), BF16), ((count, lanes), F32)],
        place,
        q,
        k,
        v,
        low,
        fading_raise_matrix,
        step_raise_matrix,
        rates,
        spike_logfade,
        scalars=1,
        flops=2 * 128**3 * 100,
    )
    maps = exchange(sent, "sp")
    state = call(
        context_kernel,
        ((2, lanes, lanes), F32),
        ctx,
        fading_raise_matrix,
        step_raise_matrix,
        rates,
        flops=2 * 128**3 * 80,
    )
    chips = n_tp // 2
    keep, give = call(
        read_kernel,
        [((chips, rows, width), BF16)] * 2,
        place,
        maps,
        state,
        asked,
        base,
        group_standard_factor.reshape(1, lanes),
        emit,
        scalars=1,
        flops=2 * count * lanes * width,
    )
    given = lax.ppermute(give, "tp", [(i, i ^ 1) for i in range(n_tp)])
    both = (keep.astype(F32) + given.astype(F32)).astype(BF16)
    final = exchange(both, "tp", [[2 * i + c for i in range(chips)] for c in range(2)])
    return call(last_kernel, ((rows, width), BF16), final, hidden_items, vectors)


def solution(mesh):
    placed = (
        P(("grp", "sp", "tp"), None),
        P("grp"),
        P(("grp", "sp"), None),
        P(),
        P("sp", "tp"),
        P("sp", "tp"),
        P("sp", "tp"),
        P(None, "tp"),
        P(None, "tp"),
        P(None, "tp"),
        P("sp", None),
        P(None, "tp"),
        P(None, "tp"),
        P("tp"),
        P(("grp", "sp"), "tp"),
        P("tp"),
        P("tp", "sp"),
    )
    return jax.shard_map(
        shards, mesh=mesh, in_specs=placed, out_specs=P(("grp", "sp", "tp"), None), check_vma=False
    )
```

time: 460 us -> 289 us (0.63)
  other arithmetic: 129 us -> 0.28 us
  local copies, waits for them, and re-layouts: 42.8 us -> 11.5 us
  matrix products: 30.6 us -> 0 us
  blocking collectives: 127 us -> 96.9 us
  waiting for transfers between devices: 56.5 us -> 82 us
  starting transfers between devices: 56.9 us -> 79.1 us
  Pallas kernels: 0 us -> 17.8 us
  between operations: 14.5 us -> 0.2 us
    another operation x27 -> x1, other arithmetic: 119 us -> 0.07 us  [shards(): place = jnp.stack([me, tp % 2]).astype(jnp.int32)]
    all_gather x3 -> x0, blocking collectives: 87.1 us -> none  [the longest x1 45 us: collected_together(): both, at, found = (lax.all_gather(jnp.concatenate(lines), axis), 0, {})]
    all_to_all x2 -> x5, waiting for transfers between devices: 7.61 us -> 80.5 us  [exchange(): lax.all_to_all(blocks, axis, 0, 0, tiled=True, axis_index_groups=groups)]
    all_to_all x1 -> x4, blocking collectives: 39.7 us -> 96.9 us  [exchange(): lax.all_to_all(blocks, axis, 0, 0, tiled=True, axis_index_groups=groups)]
    all_gather x2 -> x0, waiting for transfers between devices: 48.8 us -> none  [the longest x1 38.7 us: rows_first(): lax.all_gather(both, axis, axis=0, tiled=True)]
    dot_general x92 -> x0, matrix products: 28.2 us -> none  [the longest x15 14.6 us: product(): return jnp.dot(left, right, preferred_element_type=jnp.float32)]
    dynamic_slice x34 -> x1, local copies, waits for them, and re-layouts: 20.1 us -> 0.06 us  [shards(): lax.dynamic_slice_in_dim(packed, tp * piece, piece, 0)]
    pallas_call x0 -> x8, Pallas kernels: none -> 17.8 us  [call(): pl.pallas_call(body, out_shape=shapes, in_specs=[SMEM] * scalars + [VMEM]...]
  transfers between devices with their start and end apart: 4 -> 6, of which waited for: 3 -> 6; matrix products, arithmetic and copies ran while one was open for 17% -> 0% of each run, Pallas kernels for 0% -> 4%
where the time goes in v1:
time: 289 us; the launch traced here: 288 us
  blocking collectives  96.9 us (34%)
  waiting for transfers between devices  82 us (28%)
  starting transfers between devices  79.1 us (27%)
  Pallas kernels  17.8 us (6%)
  local copies, waits for them, and re-layouts  11.5 us (4%)
    all_to_all x4, blocking collectives, exchange(): lax.all_to_all(blocks, axis, 0, 0, tiled=True, axis_index_groups=groups)  96.9 us
    all_to_all x5, waiting for transfers between devices, exchange(): lax.all_to_all(blocks, axis, 0, 0, tiled=True, axis_index_groups=groups)  80.5 us
    all_to_all x5, starting transfers between devices, exchange(): lax.all_to_all(blocks, axis, 0, 0, tiled=True, axis_index_groups=groups)  71.5 us
    pallas_call x8, Pallas kernels, call(): pl.pallas_call(body, out_shape=shapes, in_specs=[SMEM] * scalars + [VMEM]...  17.8 us
    ppermute x1, starting transfers between devices, shards(): given = lax.ppermute(give, 'tp', [(i, i ^ 1) for i in range(n_tp)])  7.55 us
    unnamed x29, local copies, waits for them, and re-layouts  6.54 us
  transfers between devices with their start and end apart: 6, of which 6 were waited for; matrix products, arithmetic and copies ran while one was open for 0% of the time, Pallas kernels for 4%

profile of v1, /device:TPU:65, one launch (start us, length us, event | category | flops | bytes accessed | tf_op | source)
XLA Modules:
  0.0 287.7 jit_solution(3945971984406031874)
XLA Ops:
  0.0 0.7 reshape.20.sample
  0.7 0.7 reshape.21.prompt
  1.4 0.1 pad_add_fusion.place
  1.5 0.9 copy-done.4
  2.4 0.9 copy-done.5
  3.3 0.9 copy-done.6
  4.2 1.4 shard_map.163
  5.6 44.2 %all-to-all-start.1 = ((f32[16,8,256]{2,1,0:T(8,128)}), f32[16,8,256]{2,1,0:T(8,128)S(1)}, u32[]{:S(2)}, u32[]{:S(2)}) async-start(f32[16,8,256]{2,1,0:T(8,128)} %shard_map.163), calls=%async_computation.1 | async-start | bytes 262144 | tf_op jit(solution)/shard_map/all_to_all | solution.py:350
  49.8 0.7 fusion
  50.6 0.1 dynamic-slice_maximum_fusion
  50.7 0.1 copy.18
  50.7 10.9 %all-to-all-done.1.parts = f32[16,8,256]{2,1,0:T(8,128)S(1)} async-done(((f32[16,8,256]{2,1,0:T(8,128)}), f32[16,8,256]{2,1,0:T(8,128)S(1)}, u32[]{:S(2)}, u32[]{:S(2)}) %all-to-all-start.1) | async-done | bytes 131104 | tf_op jit(solution)/shard_map/all_to_all | solution.py:350
  61.6 0.6 broadcast_in_dim.9
  62.2 6.4 %all-to-all-start.3 = ((bf16[16,8,128]{2,1,0:T(8,128)(2,1)}), bf16[16,8,128]{2,1,0:T(8,128)(2,1)S(1)}, u32[]{:S(2)}, u32[]{:S(2)}) async-start(bf16[16,8,128]{2,1,0:T(8,128)(2,1)} %broadcast_in_dim.9), calls=%async_computation.3 | async-start | bytes 65536 | tf_op jit(solution)/shard_map/all_to_all | solution.py:350
  68.7 11.3 %all-to-all-done.3 = bf16[16,8,128]{2,1,0:T(8,128)(2,1)S(1)} async-done(((bf16[16,8,128]{2,1,0:T(8,128)(2,1)}), bf16[16,8,128]{2,1,0:T(8,128)(2,1)S(1)}, u32[]{:S(2)}, u32[]{:S(2)}) %all-to-all-start.3) | async-done | bytes 32800 | tf_op jit(solution)/shard_map/all_to_all | solution.py:350
  80.0 18.4 %all_to_all.45.vectors = f32[16,8,256]{2,1,0:T(8,128)S(1)} all-to-all(f32[16,8,256]{2,1,0:T(8,128)S(1)} %shard_map.164), channel_id=1, replica_groups=mesh['grp'=2,'sp'=16,'tp'=16] {'tp'}, dimensions={0} | all-to-all | bytes 262144 | tf_op jit(solution)/shard_map/all_to_all | solution.py:350
  98.4 0.1 broadcast_in_dim.8
  98.5 31.1 %all_to_all.46 = bf16[16,8,4096]{2,1,0:T(8,128)(2,1)S(1)} all-to-all(bf16[16,8,4096]{2,1,0:T(8,128)(2,1)S(1)} %broadcast_in_dim.8), channel_id=1, replica_groups=mesh['grp'=2,'sp'=16,'tp'=16] {'tp'}, dimensions={0} | all-to-all | bytes 2097152 | tf_op jit(solution)/shard_map/all_to_all | solution.py:350
  129.6 0.9 broadcast_in_dim.10
  130.5 3.7 %all-to-all-start.4 = ((bf16[16,16,8,128]{3,2,1,0:T(8,128)(2,1)}), bf16[16,16,8,128]{3,2,1,0:T(8,128)(2,1)S(1)}, u32[]{:S(2)}, u32[]{:S(2)}) async-start(bf16[16,16,8,128]{3,2,1,0:T(8,128)(2,1)} %broadcast_in_dim.10), calls=%async_computation.4 | async-start | bytes 1048576 | tf_op jit(solution)/shard_map/all_to_all | solution.py:350
  134.3 0.0 copy-start
  134.3 1.2 copy-done
  135.5 1.2 copy-done.1
  136.7 1.2 copy-done.2
  138.0 1.9 shard_map.165
  139.8 0.0 copy-start.13
  139.8 0.0 copy-start.9
  139.9 0.0 copy-start.10
  139.9 0.0 copy-start.11
  139.9 10.8 %all-to-all-done.4.pieces = bf16[16,16,8,128]{3,2,1,0:T(8,128)(2,1)S(1)} async-done(((bf16[16,16,8,128]{3,2,1,0:T(8,128)(2,1)}), bf16[16,16,8,128]{3,2,1,0:T(8,128)(2,1)S(1)}, u32[]{:S(2)}, u32[]{:S(2)}) %all-to-all-start.4) | async-done | bytes 524320 | tf_op jit(solution)/shard_map/all_to_all | solution.py:350
  150.7 1.2 shard_map.166
  151.9 3.9 %all-to-all-start.6 = ((bf16[16,8,384]{2,1,0:T(8,128)(2,1)}), bf16[16,8,384]{2,1,0:T(8,128)(2,1)S(1)}, u32[]{:S(2)}, u32[]{:S(2)}) async-start(bf16[16,8,384]{2,1,0:T(8,128)(2,1)} %get-tuple-element.22), calls=%async_computation.6 | async-start | bytes 196608 | tf_op jit(solution)/shard_map/all_to_all | solution.py:350
  155.9 0.1 copy.19.spikes
  156.0 0.0 copy-done.10
  156.0 0.0 copy-start.12
  156.0 5.2 %shard_map.167 = (bf16[16,128,128]{2,1,0:T(8,128)(2,1)S(1)}, bf16[2,128,128]{2,1,0:T(8,128)(2,1)S(1)}, f32[128,128]{1,0:T(8,128)S(1)}) custom-call(s32[2]{0:T(128)S(1)} %pad_add_fusion.place, bf16[128,128]{1,0:T(8,128)(2,1)S(1)} %get-tuple-element.16.q, bf16[144,128]{1,0:T(8,128)(2,1)S(1)} %get-tuple-element.17.k, bf16[144,128]{1,0:T(8,128)(2,1)S(1)} %get-tuple-element.18.v, ...), custom_call_target="tpu_custom_call" | custom-call | flops 419430400 | bytes 173576 | tf_op jit(solution)/shard_map/pallas_call | solution.py:23
  161.2 6.6 %all-to-all-done.6.got = bf16[16,8,384]{2,1,0:T(8,128)(2,1)S(1)} async-done(((bf16[16,8,384]{2,1,0:T(8,128)(2,1)}), bf16[16,8,384]{2,1,0:T(8,128)(2,1)S(1)}, u32[]{:S(2)}, u32[]{:S(2)}) %all-to-all-start.6) | async-done | bytes 98336 | tf_op jit(solution)/shard_map/all_to_all | solution.py:350
  167.8 27.0 %all_to_all.47.maps = bf16[16,128,128]{2,1,0:T(8,128)(2,1)S(1)} all-to-all(bf16[16,128,128]{2,1,0:T(8,128)(2,1)S(1)} %get-tuple-element.21), channel_id=1, replica_groups=mesh['grp'=2,'sp'=16,'tp'=16] {'sp'}, dimensions={0} | all-to-all | bytes 1048576 | tf_op jit(solution)/shard_map/all_to_all | solution.py:350
  194.8 1.1 broadcast_in_dim.11
  195.9 13.2 %all-to-all-start.7 = ((bf16[16,128,256]{2,1,0:T(8,128)(2,1)}), bf16[16,128,256]{2,1,0:T(8,128)(2,1)S(1)}, u32[]{:S(2)}, u32[]{:S(2)}) async-start(bf16[16,128,256]{2,1,0:T(8,128)(2,1)} %broadcast_in_dim.11), calls=%async_computation.7 | async-start | bytes 2097152 | tf_op jit(solution)/shard_map/all_to_all | solution.py:350
  209.1 4.2 %shard_map.168.state = f32[2,128,128]{2,1,0:T(8,128)S(1)} custom-call(bf16[16,8,384]{2,1,0:T(8,128)(2,1)S(1)} %all-to-all-done.6.got, bf16[64,128]{1,0:T(8,128)(2,1)S(1)} %copy-done.9, bf16[64,128]{1,0:T(8,128)(2,1)S(1)} %copy-done.10, f32[1,128]{1,0:T(1,128)S(1)} %bitcast.8), custom_call_target="tpu_custom_call" | custom-call | flops 335544320 | bytes 131584 | tf_op jit(solution)/shard_map/pallas_call | solution.py:23
  213.3 40.8 %all-to-all-done.7.emit = bf16[16,128,256]{2,1,0:T(8,128)(2,1)S(1)} async-done(((bf16[16,128,256]{2,1,0:T(8,128)(2,1)}), bf16[16,128,256]{2,1,0:T(8,128)(2,1)S(1)}, u32[]{:S(2)}, u32[]{:S(2)}) %all-to-all-start.7) | async-done | bytes 1048608 | tf_op jit(solution)/shard_map/all_to_all | solution.py:350
  254.1 3.2 %shard_map.169 = (bf16[8,8,4096]{2,1,0:T(8,128)(2,1)S(1)}, bf16[8,8,4096]{2,1,0:T(8,128)(2,1)S(1)}) custom-call(s32[2]{0:T(128)S(1)} %pad_add_fusion.place, bf16[16,128,128]{2,1,0:T(8,128)(2,1)S(1)} %all_to_all.47.maps, f32[2,128,128]{2,1,0:T(8,128)S(1)} %shard_map.168.state, bf16[2,128,128]{2,1,0:T(8,128)(2,1)S(1)} %get-tuple-element.23.asked, ...), custom_call_target="tpu_custom_call" | custom-call | flops 134217728 | bytes 1835528 | tf_op jit(solution)/shard_map/pallas_call | solution.py:23
  257.3 7.5 %collective-permute-start = (bf16[8,8,4096]{2,1,0:T(8,128)(2,1)S(1)}, bf16[8,8,4096]{2,1,0:T(8,128)(2,1)S(1)}, u32[]{:S(2)}, u32[]{:S(2)}) collective-permute-start(bf16[8,8,4096]{2,1,0:T(8,128)(2,1)S(1)} %get-tuple-element.26), channel_id=1, source_target_pairs={{0,1},{1,0},{2,3},{3,2},{4,5},{5,4},{6,7},{7,6},{8,9},{9,8},{10,11... | collective-permute-start | bytes 1572872 | tf_op jit(solution)/shard_map/ppermute | solution.py:471
  264.9 1.5 collective-permute-done
  266.4 0.1 add_convert_fusion
  266.5 20.4 %all_to_all.48.parts = bf16[8,8,4096]{2,1,0:T(8,128)(2,1)S(1)} all-to-all(bf16[8,8,4096]{2,1,0:T(8,128)(2,1)S(1)} %add_convert_fusion), channel_id=1, replica_groups={{0,2,4,6,8,10,12,14},{1,3,5,7,9,11,13,15},{16,18,20,22,24,26,28,30},{17..., dimensions={0} | all-to-all | bytes 1048576 | tf_op jit(solution)/shard_map/all_to_all | solution.py:350
  286.9 0.7 shard_map.170
  (16 shorter events, 0.1 us)
Async XLA Ops:
  0.0 98.4 %copy-start.3 = (bf16[8,4096]{1,0:T(8,128)(2,1)S(1)}, bf16[8,4096]{1,0:T(8,128)(2,1)}, u32[]{:S(2)}) copy-start(bf16[8,4096]{1,0:T(8,128)(2,1)} %hidden.1) | copy-start | bytes 196612
  1.5 0.9 copy-start.4
  2.4 0.9 copy-start.5
  3.3 0.9 copy-start.6
  5.6 56.0 %all-to-all-start.1 = ((f32[16,8,256]{2,1,0:T(8,128)}), f32[16,8,256]{2,1,0:T(8,128)S(1)}, u32[]{:S(2)}, u32[]{:S(2)}) async-start(f32[16,8,256]{2,1,0:T(8,128)} %shard_map.163), calls=%async_computation.1 | async-start | bytes 262144 | tf_op jit(solution)/shard_map/all_to_all | solution.py:350
  62.2 17.8 %all-to-all-start.3 = ((bf16[16,8,128]{2,1,0:T(8,128)(2,1)}), bf16[16,8,128]{2,1,0:T(8,128)(2,1)S(1)}, u32[]{:S(2)}, u32[]{:S(2)}) async-start(bf16[16,8,128]{2,1,0:T(8,128)(2,1)} %broadcast_in_dim.9), calls=%async_computation.3 | async-start | bytes 65536 | tf_op jit(solution)/shard_map/all_to_all | solution.py:350
  129.6 4.7 %copy-start.7 = (bf16[8,4096]{1,0:T(8,128)(2,1)S(1)}, bf16[8,4096]{1,0:T(8,128)(2,1)}, u32[]{:S(2)}) copy-start(bf16[8,4096]{1,0:T(8,128)(2,1)} %context.1) | copy-start | bytes 196612
  130.5 20.2 %all-to-all-start.4 = ((bf16[16,16,8,128]{3,2,1,0:T(8,128)(2,1)}), bf16[16,16,8,128]{3,2,1,0:T(8,128)(2,1)S(1)}, u32[]{:S(2)}, u32[]{:S(2)}) async-start(bf16[16,16,8,128]{3,2,1,0:T(8,128)(2,1)} %broadcast_in_dim.10), calls=%async_computation.4 | async-start | bytes 1048576 | tf_op jit(solution)/shard_map/all_to_all | solution.py:350
  134.3 1.2 copy-start
  135.5 1.2 copy-start.1
  136.7 1.2 copy-start.2
  139.8 16.0 %copy-start.13 = (f32[128,2]{0,1:T(2,128)S(1)}, f32[128,2]{0,1:T(2,128)}, u32[]{:S(2)}) copy-start(f32[128,2]{0,1:T(2,128)} %param.31) | copy-start | bytes 3076
  139.8 16.1 %copy-start.9 = (bf16[64,128]{1,0:T(8,128)(2,1)S(1)}, bf16[64,128]{1,0:T(8,128)(2,1)}, u32[]{:S(2)}) copy-start(bf16[64,128]{1,0:T(8,128)(2,1)} %fading.3) | copy-start | bytes 49156
  139.9 16.1 %copy-start.10 = (bf16[64,128]{1,0:T(8,128)(2,1)S(1)}, bf16[64,128]{1,0:T(8,128)(2,1)}, u32[]{:S(2)}) copy-start(bf16[64,128]{1,0:T(8,128)(2,1)} %step.3) | copy-start | bytes 49156
  139.9 16.1 %copy-start.11 = (f32[128]{0:T(128)S(1)}, f32[128]{0:T(128)}, u32[]{:S(2)}) copy-start(f32[128]{0:T(128)} %param.30) | copy-start | bytes 1540
  151.9 15.9 %all-to-all-start.6 = ((bf16[16,8,384]{2,1,0:T(8,128)(2,1)}), bf16[16,8,384]{2,1,0:T(8,128)(2,1)S(1)}, u32[]{:S(2)}, u32[]{:S(2)}) async-start(bf16[16,8,384]{2,1,0:T(8,128)(2,1)} %get-tuple-element.22), calls=%async_computation.6 | async-start | bytes 196608 | tf_op jit(solution)/shard_map/all_to_all | solution.py:350
  156.0 38.8 %copy-start.12 = (bf16[128,256]{1,0:T(8,128)(2,1)S(1)}, bf16[128,256]{1,0:T(8,128)(2,1)}, u32[]{:S(2)}) copy-start(bf16[128,256]{1,0:T(8,128)(2,1)} %param.33) | copy-start | bytes 196612
  195.9 58.3 %copy-start.8 = (f32[128]{0:T(128)S(1)}, f32[128]{0:T(128)}, u32[]{:S(2)}) copy-start(f32[128]{0:T(128)} %param.32) | copy-start | bytes 1540
  195.9 58.3 %all-to-all-start.7 = ((bf16[16,128,256]{2,1,0:T(8,128)(2,1)}), bf16[16,128,256]{2,1,0:T(8,128)(2,1)S(1)}, u32[]{:S(2)}, u32[]{:S(2)}) async-start(bf16[16,128,256]{2,1,0:T(8,128)(2,1)} %broadcast_in_dim.11), calls=%async_computation.7 | async-start | bytes 2097152 | tf_op jit(solution)/shard_map/all_to_all | solution.py:350
  257.3 9.1 %collective-permute-start = (bf16[8,8,4096]{2,1,0:T(8,128)(2,1)S(1)}, bf16[8,8,4096]{2,1,0:T(8,128)(2,1)S(1)}, u32[]{:S(2)}, u32[]{:S(2)}) collective-permute-start(bf16[8,8,4096]{2,1,0:T(8,128)(2,1)S(1)} %get-tuple-element.26), channel_id=1, source_target_pairs={{0,1},{1,0},{2,3},{3,2},{4,5},{5,4},{6,7},{7,6},{8,9},{9,8},{10,11... | collective-permute-start | bytes 1572872 | tf_op jit(solution)/shard_map/ppermute | solution.py:471

commit v2 on v1

--- a/solution.py
+++ b/solution.py
@@ -1,9 +1,12 @@
+import math
+
 import jax
 import jax.numpy as jnp
 from jax import lax
 from jax.experimental import pallas as pl
 from jax.experimental.pallas import tpu as pltpu
 from jax.sharding import PartitionSpec as P
+
 
 HEAD = 64
 EPS_ROW = 1e-05
@@ -15,15 +18,16 @@
 
 VMEM = pl.BlockSpec(memory_space=pltpu.VMEM)
 SMEM = pl.BlockSpec(memory_space=pltpu.SMEM)
-
-
-def call(body, outs, *args, flops=0, scalars=0, scratch=()):
+ANY = pl.BlockSpec(memory_space=pl.ANY)
+
+
+def call(body, outs, *args, flops=0, scalars=0, scratch=(), fetched=0):
     many = isinstance(outs, list)
     shapes = [jax.ShapeDtypeStruct(s, d) for s, d in (outs if many else [outs])]
     got = pl.pallas_call(
         body,
         out_shape=shapes,
-        in_specs=[SMEM] * scalars + [VMEM] * (len(args) - scalars),
+        in_specs=[SMEM] * scalars + [VMEM] * (len(args) - scalars - fetched) + [ANY] * fetched,
         out_specs=[VMEM] * len(shapes),
         scratch_shapes=list(scratch),
         compiler_params=pltpu.CompilerParams(vmem_limit_bytes=48 * 1024 * 1024),
@@ -44,36 +48,95 @@
     return lax.broadcasted_iota(jnp.int32, shape, dim)
 
 
-def partials_kernel(place, sample, prompt, shifting, stretch, valve, out):
-    peers, rows, _ = out.shape
-    mine = iota(sample.shape, 0) == place[0]
+def partials_kernel(place, sample, prompt, lower, shifting, stretch, valve, out, held, sems):
+    copies = [
+        pltpu.make_async_copy(ref, held.at[n], sems.at[n]) for n, ref in enumerate((shifting, stretch, valve))
+    ]
+    for copy in copies:
+        copy.start()
+    _, rows, _ = out.shape
+    chunk = held.shape[2]
+    wide = chunk // sample.shape[1]
+    line = iota(sample.shape, 0)
 
     def own(cond):
-        return jnp.sum(jnp.where(mine, cond[...].astype(F32), 0.0), axis=0, keepdims=True)
-
-    row = iota((rows, sample.shape[1]), 0)
-    first, second = jax.nn.silu(own(sample)), jax.nn.silu(own(prompt))
+        full = cond[...].astype(F32)
+        cut = [
+            jnp.sum(jnp.where(line == place[0] * wide + n, full, 0.0), axis=0, keepdims=True) for n in range(wide)
+        ]
+        return jax.nn.silu(jnp.concatenate(cut, axis=1))
+
+    row = iota((rows, chunk), 0)
+    first, second = own(sample), own(prompt)
 
     def at(k, both):
         left = jnp.where(row == k, first, 0.0)
         return jnp.where(row == k + 1, second, left) if both else left
 
-    total = dot(at(0, True), shifting[...]) + dot(at(2, True), stretch[...])
-    total = total + dot(at(4, False), valve[...])
-    out[...] = jnp.broadcast_to(total[None], out.shape)
+    half = lower.shape[0] // 2
+    blocks = lower[...].astype(F32).reshape(2 * half // rows, rows, lower.shape[1])
+    number = iota(blocks.shape, 0)
+    halves = [
+        jnp.sum(jnp.where(number == place[2] + n * (half // rows), blocks, 0.0), axis=0) for n in range(2)
+    ]
+    piece = jnp.concatenate(halves, axis=1)
+    for copy in copies:
+        copy.wait()
+    total = dot(at(0, True), held[0]) + dot(at(2, True), held[1]) + dot(at(4, False), held[2])
+    out[...] = jnp.broadcast_to(jnp.concatenate([total, piece], axis=1)[None], out.shape)
 
 
 def sum_kernel(parts, out):
-    total = parts[0]
+    chunk = parts.shape[2] - out.shape[3]
+    lanes = out.shape[3]
+    total = parts[0, :, :chunk]
     for k in range(1, parts.shape[0]):
-        total = total + parts[k]
-    out[...] = jnp.broadcast_to(total[None], out.shape)
-
-
-def rows_kernel(latent, context, vectors, wq, wk, wv, u, q, k, v):
-    count, width = latent.shape
-    extra = context.shape[0]
+        total = total + parts[k, :, :chunk]
+    high = total.astype(BF16)
+    rest = (total - high.astype(F32)).astype(BF16)
+    blocks = [parts[k, :, chunk:].astype(BF16) for k in range(parts.shape[0])]
+    for value in (high, rest):
+        blocks += [value[:, n : n + lanes] for n in range(0, chunk, lanes)]
+    for p in range(out.shape[0]):
+        for n, block in enumerate(blocks):
+            out[p, n] = block
+
+
+def by_core(core, own, other):
+    return jnp.where(core == 0, own, other), jnp.where(core == 0, other, own)
+
+
+def placed_rows(value, tp, held):
+    count = held.shape[0]
+    for n in range(count):
+        held[tp ^ mask_of(n, count)] = value[n * held.shape[1] : (n + 1) * held.shape[1]]
+    return held[...].reshape(count * held.shape[1], held.shape[2])
+
+
+def mask_of(n, count):
+    half = count // 2
+    bits = half.bit_length() - 1
+    inner = n % half
+    mask = sum(((inner >> b) & 1) << (bits - b) for b in range(bits))
+    return mask | (n // half)
+
+
+def rows_kernel(place, near, far, context, mine, theirs, wq, wk, wv, u, q, k, v, vectors, held, moved, sems):
+    copies = [pltpu.make_async_copy(ref, held.at[n], sems.at[n]) for n, ref in enumerate((wq, wk, wv))]
+    for copy in copies:
+        copy.start()
+    half, width = near.shape
+    count, extra = 2 * half, context.shape[0]
     lane = vectors.shape[2]
+    lanes = mine.shape[3]
+    spans = lane // lanes
+    first = mine.shape[1] - 2 * spans
+    for x in range(mine.shape[0]):
+        found = []
+        for ref in (mine, theirs):
+            cut = [ref[x, first + n].astype(F32) + ref[x, first + spans + n].astype(F32) for n in range(spans)]
+            found.append(jnp.concatenate(cut, axis=1))
+        vectors[2 * x], vectors[2 * x + 1] = by_core(place[1], *found)
 
     def moments(ref):
         total = jnp.zeros((ref.shape[0], lane), F32)
@@ -87,37 +150,41 @@
         spread = jnp.sum(total, -1, keepdims=True) * (1.0 / width)
         return centre, lax.rsqrt(spread + EPS_ROW)
 
-    lat, ctx = moments(latent), moments(context)
+    stats = [moments(ref) for ref in (near, far, context)]
     pad = jnp.zeros((u.shape[0] - count - extra, lane), F32)
     for t in range(width // lane):
         cols = slice(t * lane, (t + 1) * lane)
 
-        def one(ref, stats, i):
-            normed = (ref[:, cols].astype(F32) - stats[0]) * stats[1]
+        def one(n, ref, i):
+            normed = (ref[:, cols].astype(F32) - stats[n][0]) * stats[n][1]
             return normed * (1.0 + vectors[t, 2 + i : 3 + i, :]) + vectors[t, i : i + 1, :]
 
-        u[:count, cols] = one(latent, lat, 0).astype(BF16)
-        u[count:, cols] = jnp.concatenate([one(context, ctx, 1), pad], axis=0).astype(BF16)
-    q[...] = dot(u[:count], wq[...]).astype(BF16)
-    k[...] = dot(u[...], wk[...]).astype(BF16)
-    v[...] = dot(u[...], wv[...]).astype(BF16)
-
-
-def low_kernel(u, pieces, k, v, low, payload, down):
-    _, blocks, rows, lane = pieces.shape
-    span = pieces.shape[0] * rows
+        u[:half, cols] = one(0, near, 0).astype(BF16)
+        u[half:count, cols] = one(1, far, 0).astype(BF16)
+        u[count:, cols] = jnp.concatenate([one(2, context, 1), pad], axis=0).astype(BF16)
+    for copy in copies:
+        copy.wait()
+    q[...] = placed_rows(dot(u[:count], held[0]), place[2], moved).astype(BF16)
+    for out, n in ((k, 1), (v, 2)):
+        found = dot(u[...], held[n])
+        out[:count] = placed_rows(found[:count], place[2], moved).astype(BF16)
+        out[count:] = found[count:].astype(BF16)
+
+
+def low_kernel(place, u, mine, theirs, k, v, low, payload, down, moved):
+    lane = mine.shape[3]
+    blocks = down.shape[0] // (2 * lane)
     for s in range(blocks):
-        piece = pieces[:, s].astype(F32).reshape(span, lane)
-        down[2 * s * span : (2 * s + 1) * span] = piece.astype(BF16)
-        down[(2 * s + 1) * span : (2 * s + 2) * span] = pltpu.roll(piece, HEAD, 1).astype(BF16)
+        even, odd = by_core(place[1], mine[:, s].astype(F32), theirs[:, s].astype(F32))
+        piece = jnp.stack([even, odd], axis=1).reshape(lane, lane)
+        down[2 * s * lane : (2 * s + 1) * lane] = piece.astype(BF16)
+        down[(2 * s + 1) * lane : (2 * s + 2) * lane] = pltpu.roll(piece, HEAD, 1).astype(BF16)
     result = dot(u[...], down[...])
     result = jnp.where(iota(result.shape, 1) < HEAD, result, 0.0)
-    count = low.shape[0]
-    low[...] = result[:count].astype(BF16)
-    extra = payload.shape[1]
+    count, extra = low.shape[0], payload.shape[0]
+    low[...] = placed_rows(result[:count], place[2], moved).astype(BF16)
     for at, part in enumerate((k[count:].astype(F32), v[count:].astype(F32), result[count:])):
-        part = part[:extra].astype(BF16)
-        payload[:, :, at * lane : (at + 1) * lane] = jnp.broadcast_to(part[None], (payload.shape[0], extra, lane))
+        payload[:, at * lane : (at + 1) * lane] = part[:extra].astype(BF16)
 
 
 def inverse(mixing, row, col, upper):
@@ -289,18 +356,19 @@
     base[...] = ahead[3] + behind[3]
 
 
-def context_kernel(got, fading, step, rates, state):
+def context_kernel(place, got, fading, step, rates, state, moved):
     blocks, extra, lanes = got.shape[0], got.shape[1], got.shape[2] // 3
+    for n in range(blocks):
+        moved[place[0] ^ n] = got[n].astype(F32)
     parts = [
-        got[:, :, n * lanes : (n + 1) * lanes].astype(F32).reshape(blocks * extra, lanes).astype(BF16)
-        for n in range(3)
+        moved[:, :, n * lanes : (n + 1) * lanes].reshape(blocks * extra, lanes).astype(BF16) for n in range(3)
     ]
     ahead, behind = block_terms(parts[0], parts[1], parts[2][:, :HEAD], fading[...], step[...], rates[...])
     same = same_head(ahead[1].shape)
     state[0], state[1] = jnp.where(same, ahead[1], 0.0), jnp.where(same, behind[1], 0.0)
 
 
-def read_kernel(place, maps, state, asked, base, gains, emit, keep, give):
+def read_kernel(place, maps, state, asked, base, gains, emit_0, emit_1, emit_2, emit_3, keep, give):
     peers, size, _ = maps.shape
     same = same_head((size, size))
     me, core = place[0], place[1]
@@ -323,17 +391,21 @@
 
     out = out - mean(out)
     normed = out * lax.rsqrt(mean(out * out) + EPS_HEAD) * gains[...]
-    chips, rows, width = keep.shape
+    chips, rows, _ = keep.shape
     split = normed.reshape(chips, 2, rows, size)
     even, odd = split[:, 0].reshape(chips * rows, size), split[:, 1].reshape(chips * rows, size)
     mine = jnp.where(core == 0, even, odd)
     other = jnp.where(core == 0, odd, even)
     left = jnp.concatenate([mine, other], axis=0).astype(BF16)
-    lane = emit.shape[2]
-    for s in range(emit.shape[0]):
-        part = dot(left, emit[s]).reshape(2, chips, rows, lane).astype(BF16)
-        keep[:, :, s * lane : (s + 1) * lane] = part[0]
-        give[:, :, s * lane : (s + 1) * lane] = part[1]
+    lane = emit_0.shape[2]
+    fours = emit_0.shape[0]
+    for b, emit in enumerate((emit_0, emit_1, emit_2, emit_3)):
+        for a in range(fours):
+            block = fours * ((me // fours - a + fours) % fours) + (me - b + fours) % fours
+            cols = pl.ds(pl.multiple_of(block * lane, lane), lane)
+            part = dot(left, emit[a]).reshape(2, chips, rows, lane).astype(BF16)
+            keep[:, :, cols] = part[0]
+            give[:, :, cols] = part[1]
 
 
 def last_kernel(parts, hidden, vectors, out):
@@ -350,8 +422,8 @@
     return lax.all_to_all(blocks, axis, 0, 0, tiled=True, axis_index_groups=groups)
 
 
-def spread(shard, axis):
-    return exchange(jnp.broadcast_to(shard[None], (lax.axis_size(axis), *shard.shape)), axis)
+def swapped(value, axis, bit):
+    return lax.ppermute(value, axis, [(i, i ^ bit) for i in range(lax.axis_size(axis))])
 
 
 def shards(
@@ -380,54 +452,93 @@
     count = rows * n_tp
     lanes = receiver_matrix.shape[1]
     span, chunk = adjust_shifting.shape
-    place = jnp.stack([me, tp % 2]).astype(jnp.int32)
+    chips = n_tp // 2
+    same_core = [[2 * i + c for i in range(chips)] for c in range(2)]
+    place = jnp.stack([me, tp % 2, tp]).astype(jnp.int32)
 
     parts = call(
         partials_kernel,
-        ((n_sp, 8, chunk), F32),
+        ((n_sp, 8, chunk + lanes), F32),
         place,
-        sample_cond.reshape(-1, span),
-        prompt_cond.reshape(-1, span),
+        sample_cond.reshape(-1, lanes),
+        prompt_cond.reshape(-1, lanes),
+        joint_lower_projector,
         adjust_shifting,
         adjust_stretch,
         skip_valve,
         scalars=1,
+        fetched=3,
         flops=8 * span * chunk * 6,
+        scratch=[pltpu.VMEM((3, span, chunk), BF16), pltpu.SemaphoreType.DMA((3,))],
     )
     parts = exchange(parts, "sp")
-    latent = spread(hidden_items, "tp").reshape(count, width)
-    half = joint_lower_projector.shape[0] // 2
-    packed = jnp.concatenate([joint_lower_projector[:half], joint_lower_projector[half:]], axis=1)
-    piece = half // n_tp
-    pieces = spread(lax.dynamic_slice_in_dim(packed, tp * piece, piece, 0), "sp")
-    emit = spread(emit_matrix, "sp")
-
-    vectors = exchange(call(sum_kernel, ((n_tp, 8, chunk), F32), parts), "tp")
-    pieces = spread(pieces, "tp")
+
+    near, bit = hidden_items[None], n_tp // 2
+    while bit > 1:
+        near = jnp.concatenate([near, swapped(near, "tp", bit)], axis=0)
+        bit //= 2
+    far = swapped(near, "tp", 1)
+
+    fours = math.isqrt(n_sp)
+    emits = jnp.stack(
+        [emit_matrix]
+        + [lax.ppermute(emit_matrix, "sp", [(i, (i + fours * a) % n_sp) for i in range(n_sp)]) for a in range(1, fours)]
+    )
+    emits = [emits] + [
+        lax.ppermute(emits, "sp", [(i, i // fours * fours + (i + b) % fours) for i in range(n_sp)])
+        for b in range(1, fours)
+    ]
+
+    spans = chunk // lanes
+    mine = call(sum_kernel, ((chips, n_sp + 2 * spans, 8, lanes), BF16), parts)
+    mine = exchange(mine, "tp", same_core)
+    theirs = swapped(mine, "tp", 1)
 
     padded = count + -(-extra // 16) * 16
-    u, q, k, v = call(
+    u, q, k, v, vectors = call(
         rows_kernel,
-        [((padded, width), BF16), ((count, lanes), BF16), ((padded, lanes), BF16), ((padded, lanes), BF16)],
-        latent,
+        [
+            ((padded, width), BF16),
+            ((count, lanes), BF16),
+            ((padded, lanes), BF16),
+            ((padded, lanes), BF16),
+            ((n_tp, 8, chunk), F32),
+        ],
+        place,
+        near.reshape(count // 2, width),
+        far.reshape(count // 2, width),
         prompt_items,
-        vectors,
+        mine,
+        theirs,
         receiver_matrix,
         address_matrix,
         payload_matrix,
+        scalars=1,
+        fetched=3,
         flops=2 * padded * width * lanes * 3,
+        scratch=[
+            pltpu.VMEM((3, width, lanes), BF16),
+            pltpu.VMEM((n_tp, rows, lanes), F32),
+            pltpu.SemaphoreType.DMA((3,)),
+        ],
     )
     low, payload = call(
         low_kernel,
-        [((count, lanes), BF16), ((n_sp, extra, 3 * lanes), BF16)],
+        [((count, lanes), BF16), ((extra, 3 * lanes), BF16)],
+        place,
         u,
-        pieces,
+        mine,
+        theirs,
         k,
         v,
+        scalars=1,
         flops=2 * padded * width * lanes,
-        scratch=[pltpu.VMEM((width, lanes), BF16)],
-    )
-    ctx = exchange(payload, "sp")
+        scratch=[pltpu.VMEM((width, lanes), BF16), pltpu.VMEM((n_tp, rows, lanes), F32)],
+    )
+    ctx, bit = payload[None], 1
+    while bit < n_sp:
+        ctx = jnp.concatenate([ctx, swapped(ctx, "sp", bit)], axis=0)
+        bit *= 2
     rates = feature_fading.reshape(1, lanes)
     sent, asked, base = call(
         maps_kernel,
@@ -448,13 +559,15 @@
     state = call(
         context_kernel,
         ((2, lanes, lanes), F32),
+        place,
         ctx,
         fading_raise_matrix,
         step_raise_matrix,
         rates,
+        scalars=1,
         flops=2 * 128**3 * 80,
-    )
-    chips = n_tp // 2
+        scratch=[pltpu.VMEM((n_sp, extra, 3 * lanes), F32)],
+    )
     keep, give = call(
         read_kernel,
         [((chips, rows, width), BF16)] * 2,
@@ -464,13 +577,13 @@
         asked,
         base,
         group_standard_factor.reshape(1, lanes),
-        emit,
+        *emits,
         scalars=1,
         flops=2 * count * lanes * width,
     )
-    given = lax.ppermute(give, "tp", [(i, i ^ 1) for i in range(n_tp)])
+    given = swapped(give, "tp", 1)
     both = (keep.astype(F32) + given.astype(F32)).astype(BF16)
-    final = exchange(both, "tp", [[2 * i + c for i in range(chips)] for c in range(2)])
+    final = exchange(both, "tp", same_core)
     return call(last_kernel, ((rows, width), BF16), final, hidden_items, vectors)
 
 
@@ -494,6 +607,5 @@
         P("tp"),
         P("tp", "sp"),
     )
-    return jax.shard_map(
-        shards, mesh=mesh, in_specs=placed, out_specs=P(("grp", "sp", "tp"), None), check_vma=False
-    )
+
+    return jax.shard_map(shards, mesh=mesh, in_specs=placed, out_specs=P(("grp", "sp", "tp"), None), check_vma=False)

time: 289 us -> 254 us (0.88)
  blocking collectives: 96.9 us -> 20.4 us
  starting transfers between devices: 79.1 us -> 144 us
  waiting for transfers between devices: 82 us -> 53.5 us
  Pallas kernels: 17.8 us -> 22.7 us
  local copies, waits for them, and re-layouts: 11.5 us -> 8.31 us
    ppermute x1 -> x16, starting transfers between devices: 7.55 us -> 88.7 us  [the longest x10 53.3 us: swapped(): lax.ppermute(value, axis, [(i, i ^ bit) for i in range(lax.axis_size(axis...]
    all_to_all x4 -> x1, blocking collectives: 96.9 us -> 20.4 us  [exchange(): lax.all_to_all(blocks, axis, 0, 0, tiled=True, axis_index_groups=groups)]
    all_to_all x5 -> x3, waiting for transfers between devices: 80.5 us -> 11.1 us  [exchange(): lax.all_to_all(blocks, axis, 0, 0, tiled=True, axis_index_groups=groups)]
    ppermute x1 -> x16, waiting for transfers between devices: 1.51 us -> 42.4 us  [the longest x10 26.5 us: swapped(): lax.ppermute(value, axis, [(i, i ^ bit) for i in range(lax.axis_size(axis...]
    all_to_all x5 -> x3, starting transfers between devices: 71.5 us -> 55.5 us  [exchange(): lax.all_to_all(blocks, axis, 0, 0, tiled=True, axis_index_groups=groups)]
    pallas_call x8, Pallas kernels: 17.8 us -> 22.7 us  [call(): pl.pallas_call(body, out_shape=shapes, in_specs=[SMEM] * scalars + [VMEM]...]
    unnamed x29 -> x46, local copies, waits for them, and re-layouts: 6.54 us -> 8.3 us
  transfers between devices with their start and end apart: 6 -> 19, of which waited for: 6 -> 11; matrix products, arithmetic and copies ran while one was open for 0% -> 1% of each run, Pallas kernels for 4% -> 3%
where the time goes in v2:
time: 254 us; the launch traced here: 253 us
  starting transfers between devices  144 us (57%)
  waiting for transfers between devices  53.5 us (21%)
  Pallas kernels  22.7 us (9%)
  blocking collectives  20.4 us (8%)
  local copies, waits for them, and re-layouts  8.31 us (3%)
  other arithmetic  2.98 us (1%)
    all_to_all x3, starting transfers between devices, exchange(): lax.all_to_all(blocks, axis, 0, 0, tiled=True, axis_index_groups=groups)  55.5 us
    ppermute x10, starting transfers between devices, swapped(): lax.ppermute(value, axis, [(i, i ^ bit) for i in range(lax.axis_size(axis...  53.3 us
    ppermute x10, waiting for transfers between devices, swapped(): lax.ppermute(value, axis, [(i, i ^ bit) for i in range(lax.axis_size(axis...  26.5 us
    pallas_call x8, Pallas kernels, call(): pl.pallas_call(body, out_shape=shapes, in_specs=[SMEM] * scalars + [VMEM]...  22.7 us
    ppermute x3, starting transfers between devices, shards(): lax.ppermute(emit_matrix, 'sp', [(i, (i + fours * a) % n_sp) for i in ran...  21.1 us
    all_to_all x1, blocking collectives, exchange(): lax.all_to_all(blocks, axis, 0, 0, tiled=True, axis_index_groups=groups)  20.4 us
    ppermute x3, waiting for transfers between devices, shards(): lax.ppermute(emit_matrix, 'sp', [(i, (i + fours * a) % n_sp) for i in ran...  15.9 us
    ppermute x3, starting transfers between devices, shards(): lax.ppermute(emits, 'sp', [(i, i // fours * fours + (i + b) % fours) for...  14.4 us
  transfers between devices with their start and end apart: 19, of which 11 were waited for; matrix products, arithmetic and copies ran while one was open for 1% of the time, Pallas kernels for 3%

profile of v2, /device:TPU:65, one launch (start us, length us, event | category | flops | bytes accessed | tf_op | source)
XLA Modules:
  0.0 252.6 jit_solution(398317999333828888)
XLA Ops:
  0.0 8.6 %collective-permute-start = (bf16[1,8,4096]{2,1,0:T(8,128)(2,1)}, bf16[1,8,4096]{2,1,0:T(8,128)(2,1)S(1)}, u32[]{:S(2)}, u32[]{:S(2)}) collective-permute-start(bf16[1,8,4096]{2,1,0:T(8,128)(2,1)} %bitcast.17), channel_id=1, source_target_pairs={{0,8},{1,9},{2,10},{3,11},{4,12},{5,13},{6,14},{7,15},{8,0},{9,1},... | collective-permute-start | bytes 196616 | tf_op jit(solution)/shard_map/ppermute | solution.py:426
  8.6 0.9 copy.18.lower
  9.5 1.1 collective-permute-done
  10.6 0.9 pad_maximum_fusion.3
  11.4 5.2 %collective-permute-start.1 = (bf16[2,8,4096]{2,1,0:T(8,128)(2,1)S(1)}, bf16[2,8,4096]{2,1,0:T(8,128)(2,1)S(1)}, u32[]{:S(2)}, u32[]{:S(2)}) collective-permute-start(bf16[2,8,4096]{2,1,0:T(8,128)(2,1)S(1)} %pad_maximum_fusion.3), channel_id=1, source_target_pairs={{0,4},{1,5},{2,6},{3,7},{4,0},{5,1},{6,2},{7,3},{8,12},{9,13},{10,... | collective-permute-start | bytes 393224 | tf_op jit(solution)/shard_map/ppermute | solution.py:426
  16.7 0.9 copy-done.5
  17.6 0.9 copy-done.6
  18.5 0.9 copy-done.7
  20.1 0.7 copy-done.11
  20.8 2.1 shard_map.163
  22.9 44.3 %all-to-all-start = ((f32[16,8,384]{2,1,0:T(8,128)}), f32[16,8,384]{2,1,0:T(8,128)S(1)}, u32[]{:S(2)}, u32[]{:S(2)}) async-start(f32[16,8,384]{2,1,0:T(8,128)} %shard_map.163), calls=%async_computation | async-start | bytes 393216 | tf_op jit(solution)/shard_map/all_to_all | solution.py:422
  67.3 2.0 collective-permute-start.2
  69.3 10.1 %all-to-all-done.parts = f32[16,8,384]{2,1,0:T(8,128)S(1)} async-done(((f32[16,8,384]{2,1,0:T(8,128)}), f32[16,8,384]{2,1,0:T(8,128)S(1)}, u32[]{:S(2)}, u32[]{:S(2)}) %all-to-all-start) | async-done | bytes 196640 | tf_op jit(solution)/shard_map/all_to_all | solution.py:422
  79.4 0.8 shard_map.164
  80.2 4.3 %all-to-all-start.1 = ((bf16[8,20,8,128]{3,2,1,0:T(8,128)(2,1)}), bf16[8,20,8,128]{3,2,1,0:T(8,128)(2,1)S(1)}, u32[]{:S(2)}, u32[]{:S(2)}) async-start(bf16[8,20,8,128]{3,2,1,0:T(8,128)(2,1)} %shard_map.164), calls=%async_computation.1 | async-start | bytes 655360 | tf_op jit(solution)/shard_map/all_to_all | solution.py:422
  84.5 1.8 pad_maximum_fusion
  86.3 7.3 %collective-permute-start.3 = (bf16[8,8,4096]{2,1,0:T(8,128)(2,1)}, bf16[8,8,4096]{2,1,0:T(8,128)(2,1)}, u32[]{:S(2)}, u32[]{:S(2)}) collective-permute-start(bf16[8,8,4096]{2,1,0:T(8,128)(2,1)} %get-tuple-element.29), channel_id=1, source_target_pairs={{0,1},{1,0},{2,3},{3,2},{4,5},{5,4},{6,7},{7,6},{8,9},{9,8},{10,11... | collective-permute-start | bytes 1572872 | tf_op jit(solution)/shard_map/ppermute | solution.py:426
  93.6 1.0 all-to-all-done.1.mine
  94.6 8.3 %collective-permute-start.4 = (bf16[8,20,8,128]{3,2,1,0:T(8,128)(2,1)S(1)}, bf16[8,20,8,128]{3,2,1,0:T(8,128)(2,1)S(1)}, u32[]{:S(2)}, u32[]{:S(2)}) collective-permute-start(bf16[8,20,8,128]{3,2,1,0:T(8,128)(2,1)S(1)} %all-to-all-done.1.mine), channel_id=1, source_target_pairs={{0,1},{1,0},{2,3},{3,2},{4,5},{5,4},{6,7},{7,6},{8,9},{9,8},{10,11... | collective-permute-start | bytes 983048 | tf_op jit(solution)/shard_map/ppermute | solution.py:426
  103.0 0.7 copy.19.spikes
  104.2 1.2 copy-done.3
  105.5 4.1 %shard_map.165 = (bf16[144,4096]{1,0:T(8,128)(2,1)}, bf16[128,128]{1,0:T(8,128)(2,1)S(1)}, bf16[144,128]{1,0:T(8,128)(2,1)S(1)}, bf16[144,128]{1,0:T(8,128)(2,1)S(1)}, f32[16,8,256]{2,1,0:T(8,128)S(1)}) custom-call(s32[3]{0:T(128)S(1)} %pad_add_fusion.place, bf16[64,4096]{1,0:T(8,128)(2,1)S(1)} %get-tuple-element.30.near, bf16[64,4096]{1,0:T(8,128)(2,1)} %bitcast.5.far, ...), custom_call_target="tpu_custom_call" | custom-call | flops 452984832 | bytes 4915212 | tf_op jit(solution)/shard_map/pallas_call | solution.py:27
  109.6 1.3 copy-done
  110.8 1.1 shard_map.166
  112.0 5.9 %shard_map.167 = (bf16[16,128,128]{2,1,0:T(8,128)(2,1)}, bf16[2,128,128]{2,1,0:T(8,128)(2,1)S(1)}, f32[128,128]{1,0:T(8,128)S(1)}) custom-call(s32[3]{0:T(128)S(1)} %pad_add_fusion.place, bf16[128,128]{1,0:T(8,128)(2,1)S(1)} %get-tuple-element.17.q, bf16[144,128]{1,0:T(8,128)(2,1)S(1)} %get-tuple-element.18.k, bf16[144,128]{1,0:T(8,128)(2,1)S(1)} %get-tuple-element.19.v, ...), custom_call_target="tpu_custom_call" | custom-call | flops 419430400 | bytes 173580 | tf_op jit(solution)/shard_map/pallas_call | solution.py:27
  118.0 6.9 %all-to-all-start.2 = ((bf16[16,128,128]{2,1,0:T(8,128)(2,1)}), bf16[16,128,128]{2,1,0:T(8,128)(2,1)S(1)}, u32[]{:S(2)}, u32[]{:S(2)}) async-start(bf16[16,128,128]{2,1,0:T(8,128)(2,1)} %get-tuple-element.22), calls=%async_computation.2 | async-start | bytes 1048576 | tf_op jit(solution)/shard_map/all_to_all | solution.py:422
  124.8 7.0 %collective-permute-start.9 = (bf16[128,256]{1,0:T(8,128)(2,1)S(1)}, bf16[128,256]{1,0:T(8,128)(2,1)S(1)}, u32[]{:S(2)}, u32[]{:S(2)}) collective-permute-start(bf16[128,256]{1,0:T(8,128)(2,1)S(1)} %copy-done.18), channel_id=1, source_target_pairs={{0,64},{16,80},{32,96},{48,112},{64,128},{80,144},{96,160},{112,17... | collective-permute-start | bytes 196616 | tf_op jit(solution)/shard_map/ppermute | solution.py:485
  131.9 7.0 %collective-permute-start.10 = (bf16[128,256]{1,0:T(8,128)(2,1)S(1)}, bf16[128,256]{1,0:T(8,128)(2,1)S(1)}, u32[]{:S(2)}, u32[]{:S(2)}) collective-permute-start(bf16[128,256]{1,0:T(8,128)(2,1)S(1)} %copy-done.18), channel_id=1, source_target_pairs={{0,128},{16,144},{32,160},{48,176},{64,192},{80,208},{96,224},{112... | collective-permute-start | bytes 196616 | tf_op jit(solution)/shard_map/ppermute | solution.py:485
  138.9 7.0 %collective-permute-start.11 = (bf16[128,256]{1,0:T(8,128)(2,1)S(1)}, bf16[128,256]{1,0:T(8,128)(2,1)S(1)}, u32[]{:S(2)}, u32[]{:S(2)}) collective-permute-start(bf16[128,256]{1,0:T(8,128)(2,1)S(1)} %copy-done.18), channel_id=1, source_target_pairs={{0,192},{16,208},{32,224},{48,240},{64,0},{80,16},{96,32},{112,48}... | collective-permute-start | bytes 196616 | tf_op jit(solution)/shard_map/ppermute | solution.py:485
  145.9 4.1 %collective-permute-done.9 = bf16[128,256]{1,0:T(8,128)(2,1)S(1)} collective-permute-done((bf16[128,256]{1,0:T(8,128)(2,1)S(1)}, bf16[128,256]{1,0:T(8,128)(2,1)S(1)}, u32[]{:S(2)}, u32[]{:S(2)}) %collective-permute-start.9) | collective-permute-done | bytes 65568 | tf_op jit(solution)/shard_map/ppermute | solution.py:485
  150.0 11.8 %collective-permute-done.10 = bf16[128,256]{1,0:T(8,128)(2,1)S(1)} collective-permute-done((bf16[128,256]{1,0:T(8,128)(2,1)S(1)}, bf16[128,256]{1,0:T(8,128)(2,1)S(1)}, u32[]{:S(2)}, u32[]{:S(2)}) %collective-permute-start.10) | collective-permute-done | bytes 65568 | tf_op jit(solution)/shard_map/ppermute | solution.py:485
  161.9 8.4 %collective-permute-start.12 = (bf16[4,128,256]{2,1,0:T(8,128)(2,1)S(1)}, bf16[4,128,256]{2,1,0:T(8,128)(2,1)S(1)}, u32[]{:S(2)}, u32[]{:S(2)}) collective-permute-start(bf16[4,128,256]{2,1,0:T(8,128)(2,1)S(1)} %pad_maximum_fusion.2.emit_0), channel_id=1, source_target_pairs={{0,16},{16,32},{32,48},{48,0},{64,80},{80,96},{96,112},{112,64},{1... | collective-permute-start | bytes 786440 | tf_op jit(solution)/shard_map/ppermute | solution.py:488
  170.3 2.0 collective-permute-start.13
  172.3 4.0 %collective-permute-start.14 = (bf16[4,128,256]{2,1,0:T(8,128)(2,1)S(1)}, bf16[4,128,256]{2,1,0:T(8,128)(2,1)S(1)}, u32[]{:S(2)}, u32[]{:S(2)}) collective-permute-start(bf16[4,128,256]{2,1,0:T(8,128)(2,1)S(1)} %pad_maximum_fusion.2.emit_0), channel_id=1, source_target_pairs={{0,48},{16,0},{32,16},{48,32},{64,112},{80,64},{96,80},{112,96},{1... | collective-permute-start | bytes 786440 | tf_op jit(solution)/shard_map/ppermute | solution.py:488
  176.3 2.0 collective-permute-start.5
  178.3 8.5 %collective-permute-done.5 = bf16[1,8,384]{2,1,0:T(8,128)(2,1)S(1)} collective-permute-done((bf16[1,8,384]{2,1,0:T(8,128)(2,1)S(1)}, bf16[1,8,384]{2,1,0:T(8,128)(2,1)S(1)}, u32[]{:S(2)}, u32[]{:S(2)}) %collective-permute-start.5) | collective-permute-done | bytes 6176 | tf_op jit(solution)/shard_map/ppermute | solution.py:426
  186.8 1.9 collective-permute-start.6
  188.7 3.6 %collective-permute-done.6 = bf16[2,8,384]{2,1,0:T(8,128)(2,1)S(1)} collective-permute-done((bf16[2,8,384]{2,1,0:T(8,128)(2,1)S(1)}, bf16[2,8,384]{2,1,0:T(8,128)(2,1)S(1)}, u32[]{:S(2)}, u32[]{:S(2)}) %collective-permute-start.6) | collective-permute-done | bytes 12320 | tf_op jit(solution)/shard_map/ppermute | solution.py:426
  192.3 3.7 %collective-permute-start.7 = (bf16[4,8,384]{2,1,0:T(8,128)(2,1)S(1)}, bf16[4,8,384]{2,1,0:T(8,128)(2,1)S(1)}, u32[]{:S(2)}, u32[]{:S(2)}) collective-permute-start(bf16[4,8,384]{2,1,0:T(8,128)(2,1)S(1)} %pad_maximum_fusion.5), channel_id=1, source_target_pairs={{0,64},{16,80},{32,96},{48,112},{64,0},{80,16},{96,32},{112,48},{1... | collective-permute-start | bytes 73736 | tf_op jit(solution)/shard_map/ppermute | solution.py:426
  196.0 4.8 %collective-permute-done.7 = bf16[4,8,384]{2,1,0:T(8,128)(2,1)S(1)} collective-permute-done((bf16[4,8,384]{2,1,0:T(8,128)(2,1)S(1)}, bf16[4,8,384]{2,1,0:T(8,128)(2,1)S(1)}, u32[]{:S(2)}, u32[]{:S(2)}) %collective-permute-start.7) | collective-permute-done | bytes 24608 | tf_op jit(solution)/shard_map/ppermute | solution.py:426
  200.9 7.0 %collective-permute-start.8 = (bf16[8,8,384]{2,1,0:T(8,128)(2,1)S(1)}, bf16[8,8,384]{2,1,0:T(8,128)(2,1)S(1)}, u32[]{:S(2)}, u32[]{:S(2)}) collective-permute-start(bf16[8,8,384]{2,1,0:T(8,128)(2,1)S(1)} %pad_maximum_fusion.4), channel_id=1, source_target_pairs={{0,128},{16,144},{32,160},{48,176},{64,192},{80,208},{96,224},{112... | collective-permute-start | bytes 147464 | tf_op jit(solution)/shard_map/ppermute | solution.py:426
  207.9 6.5 %collective-permute-done.8 = bf16[8,8,384]{2,1,0:T(8,128)(2,1)S(1)} collective-permute-done((bf16[8,8,384]{2,1,0:T(8,128)(2,1)S(1)}, bf16[8,8,384]{2,1,0:T(8,128)(2,1)S(1)}, u32[]{:S(2)}, u32[]{:S(2)}) %collective-permute-start.8) | collective-permute-done | bytes 49184 | tf_op jit(solution)/shard_map/ppermute | solution.py:426
  214.5 4.8 %shard_map.168.state = f32[2,128,128]{2,1,0:T(8,128)S(1)} custom-call(s32[3]{0:T(128)S(1)} %pad_add_fusion.place, bf16[16,8,384]{2,1,0:T(8,128)(2,1)S(1)} %constant_dynamic-update-slice_fusion.got, bf16[64,128]{1,0:T(8,128)(2,1)S(1)} %copy-done.14, bf16[64,128]{1,0:T(8,128)(2,1)S(1)} %copy-done.16, f32[1,128]{1,0:T(1,128)S(1)} %bitcast.29), custom_call_target="tpu_custom_call" | custom-call | flops 335544320 | bytes 131596 | tf_op jit(solution)/shard_map/pallas_call | solution.py:27
  219.3 3.2 %shard_map.169 = (bf16[8,8,4096]{2,1,0:T(8,128)(2,1)S(1)}, bf16[8,8,4096]{2,1,0:T(8,128)(2,1)S(1)}) custom-call(s32[3]{0:T(128)S(1)} %pad_add_fusion.place, bf16[16,128,128]{2,1,0:T(8,128)(2,1)S(1)} %all-to-all-done.2.maps, f32[2,128,128]{2,1,0:T(8,128)S(1)} %shard_map.168.state, bf16[2,128,128]{2,1,0:T(8,128)(2,1)S(1)} %get-tuple-element.24.asked, ...), custom_call_target="tpu_custom_call" | custom-call | flops 134217728 | bytes 1835532 | tf_op jit(solution)/shard_map/pallas_call | solution.py:27
  222.5 7.3 %collective-permute-start.15 = (bf16[8,8,4096]{2,1,0:T(8,128)(2,1)S(1)}, bf16[8,8,4096]{2,1,0:T(8,128)(2,1)S(1)}, u32[]{:S(2)}, u32[]{:S(2)}) collective-permute-start(bf16[8,8,4096]{2,1,0:T(8,128)(2,1)S(1)} %get-tuple-element.27), channel_id=1, source_target_pairs={{0,1},{1,0},{2,3},{3,2},{4,5},{5,4},{6,7},{7,6},{8,9},{9,8},{10,11... | collective-permute-start | bytes 1572872 | tf_op jit(solution)/shard_map/ppermute | solution.py:426
  229.8 1.5 collective-permute-done.15
  231.5 20.4 %all_to_all.20.parts = bf16[8,8,4096]{2,1,0:T(8,128)(2,1)S(1)} all-to-all(bf16[8,8,4096]{2,1,0:T(8,128)(2,1)S(1)} %add_convert_fusion), channel_id=1, replica_groups={{0,2,4,6,8,10,12,14},{1,3,5,7,9,11,13,15},{16,18,20,22,24,26,28,30},{17..., dimensions={0} | all-to-all | bytes 1048576 | tf_op jit(solution)/shard_map/all_to_all | solution.py:422
  251.9 0.7 shard_map.170
  (55 shorter events, 1.6 us)
Async XLA Ops:
  0.0 67.3 %copy-start.4 = (bf16[8,4096]{1,0:T(8,128)(2,1)S(1)}, bf16[8,4096]{1,0:T(8,128)(2,1)}, u32[]{:S(2)}) copy-start(bf16[8,4096]{1,0:T(8,128)(2,1)} %hidden.1) | copy-start | bytes 196612
  0.0 10.6 %collective-permute-start = (bf16[1,8,4096]{2,1,0:T(8,128)(2,1)}, bf16[1,8,4096]{2,1,0:T(8,128)(2,1)S(1)}, u32[]{:S(2)}, u32[]{:S(2)}) collective-permute-start(bf16[1,8,4096]{2,1,0:T(8,128)(2,1)} %bitcast.17), channel_id=1, source_target_pairs={{0,8},{1,9},{2,10},{3,11},{4,12},{5,13},{6,14},{7,15},{8,0},{9,1},... | collective-permute-start | bytes 196616 | tf_op jit(solution)/shard_map/ppermute | solution.py:426
  11.4 55.8 %collective-permute-start.1 = (bf16[2,8,4096]{2,1,0:T(8,128)(2,1)S(1)}, bf16[2,8,4096]{2,1,0:T(8,128)(2,1)S(1)}, u32[]{:S(2)}, u32[]{:S(2)}) collective-permute-start(bf16[2,8,4096]{2,1,0:T(8,128)(2,1)S(1)} %pad_maximum_fusion.3), channel_id=1, source_target_pairs={{0,4},{1,5},{2,6},{3,7},{4,0},{5,1},{6,2},{7,3},{8,12},{9,13},{10,... | collective-permute-start | bytes 393224 | tf_op jit(solution)/shard_map/ppermute | solution.py:426
  16.7 0.9 copy-start.5
  17.6 0.9 copy-start.6
  18.5 0.9 copy-start.7
  19.4 0.7 copy-start.10
  20.1 0.7 copy-start.11
  22.9 56.4 %all-to-all-start = ((f32[16,8,384]{2,1,0:T(8,128)}), f32[16,8,384]{2,1,0:T(8,128)S(1)}, u32[]{:S(2)}, u32[]{:S(2)}) async-start(f32[16,8,384]{2,1,0:T(8,128)} %shard_map.163), calls=%async_computation | async-start | bytes 393216 | tf_op jit(solution)/shard_map/all_to_all | solution.py:422
  67.3 17.2 %collective-permute-start.2 = (bf16[4,8,4096]{2,1,0:T(8,128)(2,1)S(1)}, bf16[4,8,4096]{2,1,0:T(8,128)(2,1)}, u32[]{:S(2)}, u32[]{:S(2)}) collective-permute-start(bf16[4,8,4096]{2,1,0:T(8,128)(2,1)S(1)} %pad_maximum_fusion.1), channel_id=1, source_target_pairs={{0,2},{1,3},{2,0},{3,1},{4,6},{5,7},{6,4},{7,5},{8,10},{9,11},{10,... | collective-permute-start | bytes 786440 | tf_op jit(solution)/shard_map/ppermute | solution.py:426
  80.1 22.8 %copy-start.19 = (f32[128,2]{0,1:T(2,128)S(1)}, f32[128,2]{0,1:T(2,128)}, u32[]{:S(2)}) copy-start(f32[128,2]{0,1:T(2,128)} %param.31) | copy-start | bytes 3076
  80.1 24.1 %copy-start.1 = (bf16[4096,128]{1,0:T(8,128)(2,1)S(1)}, bf16[4096,128]{1,0:T(8,128)(2,1)}, u32[]{:S(2)}) copy-start(bf16[4096,128]{1,0:T(8,128)(2,1)} %wq.1) | copy-start | bytes 3145732
  80.1 24.1 %copy-start.2 = (bf16[4096,128]{1,0:T(8,128)(2,1)S(1)}, bf16[4096,128]{1,0:T(8,128)(2,1)}, u32[]{:S(2)}) copy-start(bf16[4096,128]{1,0:T(8,128)(2,1)} %wk.1) | copy-start | bytes 3145732
  80.1 24.1 %copy-start.8 = (bf16[8,4096]{1,0:T(8,128)(2,1)S(1)}, bf16[8,4096]{1,0:T(8,128)(2,1)}, u32[]{:S(2)}) copy-start(bf16[8,4096]{1,0:T(8,128)(2,1)} %context.1) | copy-start | bytes 196612
  80.2 14.5 %all-to-all-start.1 = ((bf16[8,20,8,128]{3,2,1,0:T(8,128)(2,1)}), bf16[8,20,8,128]{3,2,1,0:T(8,128)(2,1)S(1)}, u32[]{:S(2)}, u32[]{:S(2)}) async-start(bf16[8,20,8,128]{3,2,1,0:T(8,128)(2,1)} %shard_map.164), calls=%async_computation.1 | async-start | bytes 655360 | tf_op jit(solution)/shard_map/all_to_all | solution.py:422
  86.3 17.4 %collective-permute-start.3 = (bf16[8,8,4096]{2,1,0:T(8,128)(2,1)}, bf16[8,8,4096]{2,1,0:T(8,128)(2,1)}, u32[]{:S(2)}, u32[]{:S(2)}) collective-permute-start(bf16[8,8,4096]{2,1,0:T(8,128)(2,1)} %get-tuple-element.29), channel_id=1, source_target_pairs={{0,1},{1,0},{2,3},{3,2},{4,5},{5,4},{6,7},{7,6},{8,9},{9,8},{10,11... | collective-permute-start | bytes 1572872 | tf_op jit(solution)/shard_map/ppermute | solution.py:426
  94.6 9.6 %collective-permute-start.4 = (bf16[8,20,8,128]{3,2,1,0:T(8,128)(2,1)S(1)}, bf16[8,20,8,128]{3,2,1,0:T(8,128)(2,1)S(1)}, u32[]{:S(2)}, u32[]{:S(2)}) collective-permute-start(bf16[8,20,8,128]{3,2,1,0:T(8,128)(2,1)S(1)} %all-to-all-done.1.mine), channel_id=1, source_target_pairs={{0,1},{1,0},{2,3},{3,2},{4,5},{5,4},{6,7},{7,6},{8,9},{9,8},{10,11... | collective-permute-start | bytes 983048 | tf_op jit(solution)/shard_map/ppermute | solution.py:426
  104.2 1.2 copy-start.3
  105.5 6.5 %copy-start.9 = (f32[128,2]{1,0:T(8,128)S(1)}, f32[128,2]{1,0:T(8,128)}, u32[]{:S(2)}) copy-start(f32[128,2]{1,0:T(8,128)} %copy.19.spikes) | copy-start | bytes 3076
  105.5 6.5 %copy-start.13 = (bf16[64,128]{1,0:T(8,128)(2,1)S(1)}, bf16[64,128]{1,0:T(8,128)(2,1)}, u32[]{:S(2)}) copy-start(bf16[64,128]{1,0:T(8,128)(2,1)} %fading.3) | copy-start | bytes 49156
  105.5 6.5 %copy-start.15 = (bf16[64,128]{1,0:T(8,128)(2,1)S(1)}, bf16[64,128]{1,0:T(8,128)(2,1)}, u32[]{:S(2)}) copy-start(bf16[64,128]{1,0:T(8,128)(2,1)} %step.3) | copy-start | bytes 49156
  109.6 2.4 copy-start.17
  109.6 1.3 copy-start
  112.0 12.8 %copy-start.18 = (bf16[128,256]{1,0:T(8,128)(2,1)S(1)}, bf16[128,256]{1,0:T(8,128)(2,1)}, u32[]{:S(2)}) copy-start(bf16[128,256]{1,0:T(8,128)(2,1)} %param.33) | copy-start | bytes 196612
  118.0 96.5 %copy-start.14 = (bf16[64,128]{1,0:T(8,128)(2,1)S(1)}, bf16[64,128]{1,0:T(8,128)(2,1)}, u32[]{:S(2)}) copy-start(bf16[64,128]{1,0:T(8,128)(2,1)} %fading.3) | copy-start | bytes 49156
  118.0 96.5 %copy-start.16 = (bf16[64,128]{1,0:T(8,128)(2,1)S(1)}, bf16[64,128]{1,0:T(8,128)(2,1)}, u32[]{:S(2)}) copy-start(bf16[64,128]{1,0:T(8,128)(2,1)} %step.3) | copy-start | bytes 49156
  118.0 101.3 %all-to-all-start.2 = ((bf16[16,128,128]{2,1,0:T(8,128)(2,1)}), bf16[16,128,128]{2,1,0:T(8,128)(2,1)S(1)}, u32[]{:S(2)}, u32[]{:S(2)}) async-start(bf16[16,128,128]{2,1,0:T(8,128)(2,1)} %get-tuple-element.22), calls=%async_computation.2 | async-start | bytes 1048576 | tf_op jit(solution)/shard_map/all_to_all | solution.py:422
  124.8 94.5 %copy-start.12 = (f32[128]{0:T(128)S(1)}, f32[128]{0:T(128)}, u32[]{:S(2)}) copy-start(f32[128]{0:T(128)} %param.32) | copy-start | bytes 1540
  124.8 25.2 %collective-permute-start.9 = (bf16[128,256]{1,0:T(8,128)(2,1)S(1)}, bf16[128,256]{1,0:T(8,128)(2,1)S(1)}, u32[]{:S(2)}, u32[]{:S(2)}) collective-permute-start(bf16[128,256]{1,0:T(8,128)(2,1)S(1)} %copy-done.18), channel_id=1, source_target_pairs={{0,64},{16,80},{32,96},{48,112},{64,128},{80,144},{96,160},{112,17... | collective-permute-start | bytes 196616 | tf_op jit(solution)/shard_map/ppermute | solution.py:485
  131.9 30.0 %collective-permute-start.10 = (bf16[128,256]{1,0:T(8,128)(2,1)S(1)}, bf16[128,256]{1,0:T(8,128)(2,1)S(1)}, u32[]{:S(2)}, u32[]{:S(2)}) collective-permute-start(bf16[128,256]{1,0:T(8,128)(2,1)S(1)} %copy-done.18), channel_id=1, source_target_pairs={{0,128},{16,144},{32,160},{48,176},{64,192},{80,208},{96,224},{112... | collective-permute-start | bytes 196616 | tf_op jit(solution)/shard_map/ppermute | solution.py:485
  138.9 22.9 %collective-permute-start.11 = (bf16[128,256]{1,0:T(8,128)(2,1)S(1)}, bf16[128,256]{1,0:T(8,128)(2,1)S(1)}, u32[]{:S(2)}, u32[]{:S(2)}) collective-permute-start(bf16[128,256]{1,0:T(8,128)(2,1)S(1)} %copy-done.18), channel_id=1, source_target_pairs={{0,192},{16,208},{32,224},{48,240},{64,0},{80,16},{96,32},{112,48}... | collective-permute-start | bytes 196616 | tf_op jit(solution)/shard_map/ppermute | solution.py:485
  161.9 57.4 %collective-permute-start.12 = (bf16[4,128,256]{2,1,0:T(8,128)(2,1)S(1)}, bf16[4,128,256]{2,1,0:T(8,128)(2,1)S(1)}, u32[]{:S(2)}, u32[]{:S(2)}) collective-permute-start(bf16[4,128,256]{2,1,0:T(8,128)(2,1)S(1)} %pad_maximum_fusion.2.emit_0), channel_id=1, source_target_pairs={{0,16},{16,32},{32,48},{48,0},{64,80},{80,96},{96,112},{112,64},{1... | collective-permute-start | bytes 786440 | tf_op jit(solution)/shard_map/ppermute | solution.py:488
  170.3 49.0 %collective-permute-start.13 = (bf16[4,128,256]{2,1,0:T(8,128)(2,1)S(1)}, bf16[4,128,256]{2,1,0:T(8,128)(2,1)S(1)}, u32[]{:S(2)}, u32[]{:S(2)}) collective-permute-start(bf16[4,128,256]{2,1,0:T(8,128)(2,1)S(1)} %pad_maximum_fusion.2.emit_0), channel_id=1, source_target_pairs={{0,32},{16,48},{32,0},{48,16},{64,96},{80,112},{96,64},{112,80},{1... | collective-permute-start | bytes 786440 | tf_op jit(solution)/shard_map/ppermute | solution.py:488
  172.3 47.0 %collective-permute-start.14 = (bf16[4,128,256]{2,1,0:T(8,128)(2,1)S(1)}, bf16[4,128,256]{2,1,0:T(8,128)(2,1)S(1)}, u32[]{:S(2)}, u32[]{:S(2)}) collective-permute-start(bf16[4,128,256]{2,1,0:T(8,128)(2,1)S(1)} %pad_maximum_fusion.2.emit_0), channel_id=1, source_target_pairs={{0,48},{16,0},{32,16},{48,32},{64,112},{80,64},{96,80},{112,96},{1... | collective-permute-start | bytes 786440 | tf_op jit(solution)/shard_map/ppermute | solution.py:488
  176.3 10.5 %collective-permute-start.5 = (bf16[1,8,384]{2,1,0:T(8,128)(2,1)S(1)}, bf16[1,8,384]{2,1,0:T(8,128)(2,1)S(1)}, u32[]{:S(2)}, u32[]{:S(2)}) collective-permute-start(bf16[1,8,384]{2,1,0:T(8,128)(2,1)S(1)} %bitcast.21), channel_id=1, source_target_pairs={{0,16},{16,0},{32,48},{48,32},{64,80},{80,64},{96,112},{112,96},{1... | collective-permute-start | bytes 18440 | tf_op jit(solution)/shard_map/ppermute | solution.py:426
  186.8 5.5 %collective-permute-start.6 = (bf16[2,8,384]{2,1,0:T(8,128)(2,1)S(1)}, bf16[2,8,384]{2,1,0:T(8,128)(2,1)S(1)}, u32[]{:S(2)}, u32[]{:S(2)}) collective-permute-start(bf16[2,8,384]{2,1,0:T(8,128)(2,1)S(1)} %pad_maximum_fusion.6), channel_id=1, source_target_pairs={{0,32},{16,48},{32,0},{48,16},{64,96},{80,112},{96,64},{112,80},{1... | collective-permute-start | bytes 36872 | tf_op jit(solution)/shard_map/ppermute | solution.py:426
  192.3 8.5 %collective-permute-start.7 = (bf16[4,8,384]{2,1,0:T(8,128)(2,1)S(1)}, bf16[4,8,384]{2,1,0:T(8,128)(2,1)S(1)}, u32[]{:S(2)}, u32[]{:S(2)}) collective-permute-start(bf16[4,8,384]{2,1,0:T(8,128)(2,1)S(1)} %pad_maximum_fusion.5), channel_id=1, source_target_pairs={{0,64},{16,80},{32,96},{48,112},{64,0},{80,16},{96,32},{112,48},{1... | collective-permute-start | bytes 73736 | tf_op jit(solution)/shard_map/ppermute | solution.py:426
  200.9 13.6 %collective-permute-start.8 = (bf16[8,8,384]{2,1,0:T(8,128)(2,1)S(1)}, bf16[8,8,384]{2,1,0:T(8,128)(2,1)S(1)}, u32[]{:S(2)}, u32[]{:S(2)}) collective-permute-start(bf16[8,8,384]{2,1,0:T(8,128)(2,1)S(1)} %pad_maximum_fusion.4), channel_id=1, source_target_pairs={{0,128},{16,144},{32,160},{48,176},{64,192},{80,208},{96,224},{112... | collective-permute-start | bytes 147464 | tf_op jit(solution)/shard_map/ppermute | solution.py:426
  222.5 8.8 %collective-permute-start.15 = (bf16[8,8,4096]{2,1,0:T(8,128)(2,1)S(1)}, bf16[8,8,4096]{2,1,0:T(8,128)(2,1)S(1)}, u32[]{:S(2)}, u32[]{:S(2)}) collective-permute-start(bf16[8,8,4096]{2,1,0:T(8,128)(2,1)S(1)} %get-tuple-element.27), channel_id=1, source_target_pairs={{0,1},{1,0},{2,3},{3,2},{4,5},{5,4},{6,7},{7,6},{8,9},{9,8},{10,11... | collective-permute-start | bytes 1572872 | tf_op jit(solution)/shard_map/ppermute | solution.py:426

commit v3 on v2

--- a/solution.py
+++ b/solution.py
@@ -1,5 +1,3 @@
-import math
-
 import jax
 import jax.numpy as jnp
 from jax import lax
@@ -18,7 +16,7 @@
 
 VMEM = pl.BlockSpec(memory_space=pltpu.VMEM)
 SMEM = pl.BlockSpec(memory_space=pltpu.SMEM)
-ANY = pl.BlockSpec(memory_space=pl.ANY)
+HBM = pl.BlockSpec(memory_space=pltpu.HBM)
 
 
 def call(body, outs, *args, flops=0, scalars=0, scratch=(), fetched=0):
@@ -27,7 +25,7 @@
     got = pl.pallas_call(
         body,
         out_shape=shapes,
-        in_specs=[SMEM] * scalars + [VMEM] * (len(args) - scalars - fetched) + [ANY] * fetched,
+        in_specs=[SMEM] * scalars + [VMEM] * (len(args) - scalars - fetched) + [HBM] * fetched,
         out_specs=[VMEM] * len(shapes),
         scratch_shapes=list(scratch),
         compiler_params=pltpu.CompilerParams(vmem_limit_bytes=48 * 1024 * 1024),
@@ -48,39 +46,42 @@
     return lax.broadcasted_iota(jnp.int32, shape, dim)
 
 
-def partials_kernel(place, sample, prompt, lower, shifting, stretch, valve, out, held, sems):
-    copies = [
-        pltpu.make_async_copy(ref, held.at[n], sems.at[n]) for n, ref in enumerate((shifting, stretch, valve))
-    ]
+def partials_kernel(place, sample, prompt, lower, shifting, stretch, valve, out, conds, low_rows, held, sems):
+    pairs = [(sample, conds.at[0]), (prompt, conds.at[1]), (lower, low_rows)]
+    pairs += [(ref, held.at[n]) for n, ref in enumerate((shifting, stretch, valve))]
+    copies = [pltpu.make_async_copy(ref, to, sems.at[n]) for n, (ref, to) in enumerate(pairs)]
     for copy in copies:
         copy.start()
+    for copy in copies[:3]:
+        copy.wait()
     _, rows, _ = out.shape
     chunk = held.shape[2]
     wide = chunk // sample.shape[1]
     line = iota(sample.shape, 0)
 
-    def own(cond):
-        full = cond[...].astype(F32)
+    def own(n):
+        full = conds[n].astype(F32)
         cut = [
             jnp.sum(jnp.where(line == place[0] * wide + n, full, 0.0), axis=0, keepdims=True) for n in range(wide)
         ]
         return jax.nn.silu(jnp.concatenate(cut, axis=1))
 
     row = iota((rows, chunk), 0)
-    first, second = own(sample), own(prompt)
+    first, second = own(0), own(1)
 
     def at(k, both):
         left = jnp.where(row == k, first, 0.0)
         return jnp.where(row == k + 1, second, left) if both else left
 
-    half = lower.shape[0] // 2
-    blocks = lower[...].astype(F32).reshape(2 * half // rows, rows, lower.shape[1])
+    upright = low_rows[...].astype(F32).T
+    count = upright.shape[0] // rows
+    blocks = upright.reshape(count, rows, upright.shape[1])
     number = iota(blocks.shape, 0)
     halves = [
-        jnp.sum(jnp.where(number == place[2] + n * (half // rows), blocks, 0.0), axis=0) for n in range(2)
+        jnp.sum(jnp.where(number == place[2] + n * (count // 2), blocks, 0.0), axis=0) for n in range(2)
     ]
     piece = jnp.concatenate(halves, axis=1)
-    for copy in copies:
+    for copy in copies[3:]:
         copy.wait()
     total = dot(at(0, True), held[0]) + dot(at(2, True), held[1]) + dot(at(4, False), held[2])
     out[...] = jnp.broadcast_to(jnp.concatenate([total, piece], axis=1)[None], out.shape)
@@ -106,30 +107,26 @@
     return jnp.where(core == 0, own, other), jnp.where(core == 0, other, own)
 
 
-def placed_rows(value, tp, held):
-    count = held.shape[0]
-    for n in range(count):
-        held[tp ^ mask_of(n, count)] = value[n * held.shape[1] : (n + 1) * held.shape[1]]
-    return held[...].reshape(count * held.shape[1], held.shape[2])
-
-
-def mask_of(n, count):
-    half = count // 2
-    bits = half.bit_length() - 1
-    inner = n % half
-    mask = sum(((inner >> b) & 1) << (bits - b) for b in range(bits))
-    return mask | (n // half)
-
-
-def rows_kernel(place, near, far, context, mine, theirs, wq, wk, wv, u, q, k, v, vectors, held, moved, sems):
-    copies = [pltpu.make_async_copy(ref, held.at[n], sems.at[n]) for n, ref in enumerate((wq, wk, wv))]
-    for copy in copies:
-        copy.start()
-    half, width = near.shape
-    count, extra = 2 * half, context.shape[0]
-    lane = vectors.shape[2]
-    lanes = mine.shape[3]
+def moments(ref, lane):
+    width = ref.shape[1]
+    total = jnp.zeros((ref.shape[0], lane), F32)
+    for c in range(0, width, lane):
+        total = total + ref[:, c : c + lane].astype(F32)
+    centre = jnp.sum(total, -1, keepdims=True) * (1.0 / width)
+    total = jnp.zeros((ref.shape[0], lane), F32)
+    for c in range(0, width, lane):
+        off = ref[:, c : c + lane].astype(F32) - centre
+        total = total + off * off
+    spread = jnp.sum(total, -1, keepdims=True) * (1.0 / width)
+    return centre, lax.rsqrt(spread + EPS_ROW)
+
+
+def modulated(place, latent, context, mine, theirs, u, vectors, down):
+    count, width = latent.shape
+    extra = context.shape[0]
+    lane, lanes = vectors.shape[2], mine.shape[3]
     spans = lane // lanes
+    stats = [moments(ref, lane) for ref in (latent, context)]
     first = mine.shape[1] - 2 * spans
     for x in range(mine.shape[0]):
         found = []
@@ -137,20 +134,6 @@
             cut = [ref[x, first + n].astype(F32) + ref[x, first + spans + n].astype(F32) for n in range(spans)]
             found.append(jnp.concatenate(cut, axis=1))
         vectors[2 * x], vectors[2 * x + 1] = by_core(place[1], *found)
-
-    def moments(ref):
-        total = jnp.zeros((ref.shape[0], lane), F32)
-        for c in range(0, width, lane):
-            total = total + ref[:, c : c + lane].astype(F32)
-        centre = jnp.sum(total, -1, keepdims=True) * (1.0 / width)
-        total = jnp.zeros((ref.shape[0], lane), F32)
-        for c in range(0, width, lane):
-            off = ref[:, c : c + lane].astype(F32) - centre
-            total = total + off * off
-        spread = jnp.sum(total, -1, keepdims=True) * (1.0 / width)
-        return centre, lax.rsqrt(spread + EPS_ROW)
-
-    stats = [moments(ref) for ref in (near, far, context)]
     pad = jnp.zeros((u.shape[0] - count - extra, lane), F32)
     for t in range(width // lane):
         cols = slice(t * lane, (t + 1) * lane)
@@ -159,32 +142,13 @@
             normed = (ref[:, cols].astype(F32) - stats[n][0]) * stats[n][1]
             return normed * (1.0 + vectors[t, 2 + i : 3 + i, :]) + vectors[t, i : i + 1, :]
 
-        u[:half, cols] = one(0, near, 0).astype(BF16)
-        u[half:count, cols] = one(1, far, 0).astype(BF16)
-        u[count:, cols] = jnp.concatenate([one(2, context, 1), pad], axis=0).astype(BF16)
-    for copy in copies:
-        copy.wait()
-    q[...] = placed_rows(dot(u[:count], held[0]), place[2], moved).astype(BF16)
-    for out, n in ((k, 1), (v, 2)):
-        found = dot(u[...], held[n])
-        out[:count] = placed_rows(found[:count], place[2], moved).astype(BF16)
-        out[count:] = found[count:].astype(BF16)
-
-
-def low_kernel(place, u, mine, theirs, k, v, low, payload, down, moved):
-    lane = mine.shape[3]
-    blocks = down.shape[0] // (2 * lane)
-    for s in range(blocks):
+        u[:count, cols] = one(0, latent, 0).astype(BF16)
+        u[count:, cols] = jnp.concatenate([one(1, context, 1), pad], axis=0).astype(BF16)
+    for s in range(down.shape[0] // (2 * lanes)):
         even, odd = by_core(place[1], mine[:, s].astype(F32), theirs[:, s].astype(F32))
-        piece = jnp.stack([even, odd], axis=1).reshape(lane, lane)
-        down[2 * s * lane : (2 * s + 1) * lane] = piece.astype(BF16)
-        down[(2 * s + 1) * lane : (2 * s + 2) * lane] = pltpu.roll(piece, HEAD, 1).astype(BF16)
-    result = dot(u[...], down[...])
-    result = jnp.where(iota(result.shape, 1) < HEAD, result, 0.0)
-    count, extra = low.shape[0], payload.shape[0]
-    low[...] = placed_rows(result[:count], place[2], moved).astype(BF16)
-    for at, part in enumerate((k[count:].astype(F32), v[count:].astype(F32), result[count:])):
-        payload[:, at * lane : (at + 1) * lane] = part[:extra].astype(BF16)
+        piece = jnp.stack([even, odd], axis=1).reshape(lanes, lanes)
+        down[2 * s * lanes : (2 * s + 1) * lanes] = piece.astype(BF16)
+        down[(2 * s + 1) * lanes : (2 * s + 2) * lanes] = pltpu.roll(piece, HEAD, 1).astype(BF16)
 
 
 def inverse(mixing, row, col, upper):
@@ -238,9 +202,10 @@
     if spikes is None:
         b_end = b_after = b_before = None
     else:
-        jump = jnp.zeros_like(key)
-        for h, own in enumerate(owns):
-            jump = jnp.where(own, -spikes[:, h : h + 1], jump)
+        across = jnp.zeros((lanes, count), F32)
+        for h in range(heads):
+            across = jnp.where(iota(across.shape, 0) // HEAD == h, -spikes[h : h + 1], across)
+        jump = across.T
         b_after = running(jump)
         b_before = b_after - jump
         b_end = b_after[count - 1 : count]
@@ -340,48 +305,81 @@
     return (iota(shape, 0) // HEAD) == (iota(shape, 1) // HEAD)
 
 
-def maps_kernel(place, q, k, v, low, fading, step, rates, spikes, sent, asked, base):
-    count = q.shape[0]
+def block_kernel(
+    place, mine, theirs, latent_, context_, wq, wk, wv, fading_, step_, rates_, spikes_,
+    sent, asked, base, vectors,
+    latent, context, held, fading, step, rates, spikes, u, down, sems,
+):
+    pairs = [(latent_, latent), (context_, context)]
+    pairs += [(ref, held.at[n]) for n, ref in enumerate((wq, wk, wv))]
+    pairs += [(fading_, fading), (step_, step), (rates_, rates), (spikes_, spikes)]
+    copies = [pltpu.make_async_copy(ref, to, sems.at[n]) for n, (ref, to) in enumerate(pairs)]
+    for copy in copies:
+        copy.start()
+    for copy in copies[:2]:
+        copy.wait()
+    modulated(place, latent, context, mine, theirs, u, vectors, down)
+    for copy in copies[2:]:
+        copy.wait()
+    count, extra = latent.shape[0], context.shape[0]
+    q = dot(u[:count], held[0]).astype(BF16)
+    k, v = dot(u[...], held[1]).astype(BF16), dot(u[...], held[2]).astype(BF16)
+    low = dot(u[...], down[...])
+    low = jnp.where(iota(low.shape, 1) < HEAD, low, 0.0).astype(BF16)
     ahead, behind = block_terms(
-        k[:count], v[:count], low[:, :HEAD], fading[...], step[...], rates[...], spikes[...], q[...]
+        k[:count], v[:count], low[:count, :HEAD], fading[...], step[...], rates[...], spikes[...], q
     )
     same = same_head(ahead[0].shape)
     packed = [
         jnp.where(same, factor, pltpu.roll(offset, HEAD, 0)).astype(BF16)
         for factor, offset in (ahead[:2], behind[:2])
     ]
+    tail = [part[count:].astype(F32)[:extra] for part in (k, v, low)]
+    tail = jnp.concatenate(tail + [jnp.zeros_like(tail[0])] * (-len(tail) % 2), axis=0).astype(BF16)
+    size = packed[0].shape[0]
     for j in range(sent.shape[0]):
-        sent[j] = jnp.where(place[0] < j, packed[0], packed[1])
+        sent[j, :size] = jnp.where(place[0] < j, packed[0], packed[1])
+        sent[j, size:] = tail
     asked[0], asked[1] = ahead[2].astype(BF16), behind[2].astype(BF16)
     base[...] = ahead[3] + behind[3]
 
 
-def context_kernel(place, got, fading, step, rates, state, moved):
-    blocks, extra, lanes = got.shape[0], got.shape[1], got.shape[2] // 3
-    for n in range(blocks):
-        moved[place[0] ^ n] = got[n].astype(F32)
-    parts = [
-        moved[:, :, n * lanes : (n + 1) * lanes].reshape(blocks * extra, lanes).astype(BF16) for n in range(3)
-    ]
-    ahead, behind = block_terms(parts[0], parts[1], parts[2][:, :HEAD], fading[...], step[...], rates[...])
-    same = same_head(ahead[1].shape)
-    state[0], state[1] = jnp.where(same, ahead[1], 0.0), jnp.where(same, behind[1], 0.0)
-
-
-def read_kernel(place, maps, state, asked, base, gains, emit_0, emit_1, emit_2, emit_3, keep, give):
-    peers, size, _ = maps.shape
+def read_kernel(
+    place, maps, asked, base, fading_, step_, rates_, gains_, emit_,
+    keep, give,
+    fading, step, rates, gains, emit, sems,
+):
+    pairs = [(fading_, fading), (step_, step), (rates_, rates), (gains_, gains), (emit_, emit)]
+    copies = [pltpu.make_async_copy(ref, to, sems.at[n]) for n, (ref, to) in enumerate(pairs)]
+    for copy in copies:
+        copy.start()
+    peers, _, size = maps.shape
+    extra = keep.shape[1]
     same = same_head((size, size))
     me, core = place[0], place[1]
-    states = [state[0], state[1]]
+    for copy in copies[:4]:
+        copy.wait()
+    parts = [
+        jnp.concatenate([maps[j, size + n * extra : size + (n + 1) * extra].astype(F32) for j in range(peers)], axis=0)
+        for n in range(3)
+    ]
+    parts = [part.astype(BF16) for part in parts]
+    context = block_terms(parts[0], parts[1], parts[2][:, :HEAD], fading[...], step[...], rates[...])
+    eye = (iota((size, size), 0) == iota((size, size), 1)).astype(F32)
+    composed = [jnp.concatenate([eye, jnp.zeros_like(eye)], axis=0) for _ in range(2)]
     for n in range(peers - 1):
         for d, j, reached in ((0, n, n < me), (1, peers - 1 - n, peers - 1 - n > me)):
-            packed = maps[j].astype(F32)
+            packed = maps[j, :size].astype(F32)
             factor = jnp.where(same, packed, 0.0)
             offset = jnp.where(same, pltpu.roll(packed, HEAD, 0), 0.0)
-            states[d] = jnp.where(reached, dot(states[d], factor) + offset, states[d])
+            new = dot(composed[d], factor)
+            new = jnp.concatenate([new[:size], new[size:] + offset], axis=0)
+            composed[d] = jnp.where(reached, new, composed[d])
     out = base[...]
     for d in range(2):
-        out = out + dot(asked[d], states[d], ((1,), (1,)))
+        start = jnp.where(same, context[d][1], 0.0)
+        state = dot(start, composed[d][:size]) + composed[d][size:]
+        out = out + dot(asked[d], state, ((1,), (1,)))
     first = iota(out.shape, 1) < HEAD
 
     def mean(value):
@@ -397,15 +395,12 @@
     mine = jnp.where(core == 0, even, odd)
     other = jnp.where(core == 0, odd, even)
     left = jnp.concatenate([mine, other], axis=0).astype(BF16)
-    lane = emit_0.shape[2]
-    fours = emit_0.shape[0]
-    for b, emit in enumerate((emit_0, emit_1, emit_2, emit_3)):
-        for a in range(fours):
-            block = fours * ((me // fours - a + fours) % fours) + (me - b + fours) % fours
-            cols = pl.ds(pl.multiple_of(block * lane, lane), lane)
-            part = dot(left, emit[a]).reshape(2, chips, rows, lane).astype(BF16)
-            keep[:, :, cols] = part[0]
-            give[:, :, cols] = part[1]
+    copies[4].wait()
+    lane = emit.shape[2]
+    for s in range(emit.shape[0]):
+        part = dot(left, emit[s]).reshape(2, chips, rows, lane).astype(BF16)
+        keep[:, :, s * lane : (s + 1) * lane] = part[0]
+        give[:, :, s * lane : (s + 1) * lane] = part[1]
 
 
 def last_kernel(parts, hidden, vectors, out):
@@ -462,32 +457,23 @@
         place,
         sample_cond.reshape(-1, lanes),
         prompt_cond.reshape(-1, lanes),
-        joint_lower_projector,
+        joint_lower_projector.T,
         adjust_shifting,
         adjust_stretch,
         skip_valve,
         scalars=1,
-        fetched=3,
+        fetched=6,
         flops=8 * span * chunk * 6,
-        scratch=[pltpu.VMEM((3, span, chunk), BF16), pltpu.SemaphoreType.DMA((3,))],
-    )
+        scratch=[
+            pltpu.VMEM((2, width // lanes, lanes), BF16),
+            pltpu.VMEM(joint_lower_projector.shape[::-1], BF16),
+            pltpu.VMEM((3, span, chunk), BF16),
+            pltpu.SemaphoreType.DMA((6,)),
+        ],
+    )
+    latent = lax.all_gather(hidden_items, "tp", axis=0, tiled=True)
+    emit = lax.all_gather(emit_matrix, "sp", axis=0)
     parts = exchange(parts, "sp")
-
-    near, bit = hidden_items[None], n_tp // 2
-    while bit > 1:
-        near = jnp.concatenate([near, swapped(near, "tp", bit)], axis=0)
-        bit //= 2
-    far = swapped(near, "tp", 1)
-
-    fours = math.isqrt(n_sp)
-    emits = jnp.stack(
-        [emit_matrix]
-        + [lax.ppermute(emit_matrix, "sp", [(i, (i + fours * a) % n_sp) for i in range(n_sp)]) for a in range(1, fours)]
-    )
-    emits = [emits] + [
-        lax.ppermute(emits, "sp", [(i, i // fours * fours + (i + b) % fours) for i in range(n_sp)])
-        for b in range(1, fours)
-    ]
 
     spans = chunk // lanes
     mine = call(sum_kernel, ((chips, n_sp + 2 * spans, 8, lanes), BF16), parts)
@@ -495,91 +481,68 @@
     theirs = swapped(mine, "tp", 1)
 
     padded = count + -(-extra // 16) * 16
-    u, q, k, v, vectors = call(
-        rows_kernel,
+    rates = feature_fading.reshape(1, lanes)
+    small = [
+        pltpu.VMEM(fading_raise_matrix.shape, BF16),
+        pltpu.VMEM(step_raise_matrix.shape, BF16),
+        pltpu.VMEM(rates.shape, F32),
+    ]
+    sent, asked, base, vectors = call(
+        block_kernel,
         [
-            ((padded, width), BF16),
-            ((count, lanes), BF16),
-            ((padded, lanes), BF16),
-            ((padded, lanes), BF16),
+            ((n_sp, lanes + 4 * extra, lanes), BF16),
+            ((2, count, lanes), BF16),
+            ((count, lanes), F32),
             ((n_tp, 8, chunk), F32),
         ],
         place,
-        near.reshape(count // 2, width),
-        far.reshape(count // 2, width),
-        prompt_items,
         mine,
         theirs,
+        latent,
+        prompt_items,
         receiver_matrix,
         address_matrix,
         payload_matrix,
-        scalars=1,
-        fetched=3,
-        flops=2 * padded * width * lanes * 3,
-        scratch=[
-            pltpu.VMEM((3, width, lanes), BF16),
-            pltpu.VMEM((n_tp, rows, lanes), F32),
-            pltpu.SemaphoreType.DMA((3,)),
-        ],
-    )
-    low, payload = call(
-        low_kernel,
-        [((count, lanes), BF16), ((extra, 3 * lanes), BF16)],
-        place,
-        u,
-        mine,
-        theirs,
-        k,
-        v,
-        scalars=1,
-        flops=2 * padded * width * lanes,
-        scratch=[pltpu.VMEM((width, lanes), BF16), pltpu.VMEM((n_tp, rows, lanes), F32)],
-    )
-    ctx, bit = payload[None], 1
-    while bit < n_sp:
-        ctx = jnp.concatenate([ctx, swapped(ctx, "sp", bit)], axis=0)
-        bit *= 2
-    rates = feature_fading.reshape(1, lanes)
-    sent, asked, base = call(
-        maps_kernel,
-        [((n_sp, lanes, lanes), BF16), ((2, count, lanes), BF16), ((count, lanes), F32)],
-        place,
-        q,
-        k,
-        v,
-        low,
         fading_raise_matrix,
         step_raise_matrix,
         rates,
-        spike_logfade,
+        spike_logfade.T,
         scalars=1,
-        flops=2 * 128**3 * 100,
+        fetched=9,
+        flops=2 * padded * width * lanes * 4,
+        scratch=[
+            pltpu.VMEM((count, width), BF16),
+            pltpu.VMEM((extra, width), BF16),
+            pltpu.VMEM((3, width, lanes), BF16),
+            *small,
+            pltpu.VMEM(spike_logfade.shape[::-1], F32),
+            pltpu.VMEM((padded, width), BF16),
+            pltpu.VMEM((width, lanes), BF16),
+            pltpu.SemaphoreType.DMA((9,)),
+        ],
     )
     maps = exchange(sent, "sp")
-    state = call(
-        context_kernel,
-        ((2, lanes, lanes), F32),
-        place,
-        ctx,
-        fading_raise_matrix,
-        step_raise_matrix,
-        rates,
-        scalars=1,
-        flops=2 * 128**3 * 80,
-        scratch=[pltpu.VMEM((n_sp, extra, 3 * lanes), F32)],
-    )
     keep, give = call(
         read_kernel,
         [((chips, rows, width), BF16)] * 2,
         place,
         maps,
-        state,
         asked,
         base,
+        fading_raise_matrix,
+        step_raise_matrix,
+        rates,
         group_standard_factor.reshape(1, lanes),
-        *emits,
+        emit,
         scalars=1,
+        fetched=5,
         flops=2 * count * lanes * width,
+        scratch=[
+            *small,
+            pltpu.VMEM((1, lanes), F32),
+            pltpu.VMEM((n_sp, *emit_matrix.shape), BF16),
+            pltpu.SemaphoreType.DMA((5,)),
+        ],
     )
     given = swapped(give, "tp", 1)
     both = (keep.astype(F32) + given.astype(F32)).astype(BF16)

time: 254 us -> 238 us (0.937)
  starting transfers between devices: 144 us -> 27.1 us
  blocking collectives: 20.4 us -> 96.4 us
  waiting for transfers between devices: 53.5 us -> 71.7 us
  between operations: 0.43 us -> 15 us
  Pallas kernels: 22.7 us -> 18.8 us
  other arithmetic: 2.98 us -> 0.21 us
    all_to_all x1 -> x3, blocking collectives: 20.4 us -> 96.4 us  [exchange(): lax.all_to_all(blocks, axis, 0, 0, tiled=True, axis_index_groups=groups)]
    all_gather x0 -> x2, waiting for transfers between devices: none -> 67.7 us  [the longest x1 67.7 us: shards(): emit = lax.all_gather(emit_matrix, 'sp', axis=0)]
    all_to_all x3 -> x1, starting transfers between devices: 55.5 us -> 8.58 us  [exchange(): lax.all_to_all(blocks, axis, 0, 0, tiled=True, axis_index_groups=groups)]
    ppermute x6 -> x0, starting transfers between devices: 35.5 us -> none  [the longest x3 21.1 us: shards(): lax.ppermute(emit_matrix, 'sp', [(i, (i + fours * a) % n_sp) for i in ran...]
    ppermute x10 -> x2, starting transfers between devices: 53.3 us -> 18.4 us  [swapped(): lax.ppermute(value, axis, [(i, i ^ bit) for i in range(lax.axis_size(axis...]
    ppermute x10 -> x2, waiting for transfers between devices: 26.5 us -> 2.75 us  [swapped(): lax.ppermute(value, axis, [(i, i ^ bit) for i in range(lax.axis_size(axis...]
    ppermute x6 -> x0, waiting for transfers between devices: 15.9 us -> none  [the longest x3 15.9 us: shards(): lax.ppermute(emit_matrix, 'sp', [(i, (i + fours * a) % n_sp) for i in ran...]
    all_to_all x3 -> x1, waiting for transfers between devices: 11.1 us -> 0.01 us  [exchange(): lax.all_to_all(blocks, axis, 0, 0, tiled=True, axis_index_groups=groups)]
  transfers between devices with their start and end apart: 19 -> 5, of which waited for: 11 -> 3; matrix products, arithmetic and copies ran while one was open for 1% -> 0% of each run, Pallas kernels for 3% -> 1%
where the time goes in v3:
time: 238 us
  blocking collectives  96.4 us (41%)
  waiting for transfers between devices  71.7 us (30%)
  starting transfers between devices  27.1 us (11%)
  Pallas kernels  18.8 us (8%)
  between operations  15 us (6%)
  local copies, waits for them, and re-layouts  8.38 us (4%)
    all_to_all x3, blocking collectives, exchange(): lax.all_to_all(blocks, axis, 0, 0, tiled=True, axis_index_groups=groups)  96.4 us
    all_gather x1, waiting for transfers between devices, shards(): emit = lax.all_gather(emit_matrix, 'sp', axis=0)  67.7 us
    pallas_call x5, Pallas kernels, call(): pl.pallas_call(body, out_shape=shapes, in_specs=[SMEM] * scalars + [VMEM]...  18.8 us
    ppermute x2, starting transfers between devices, swapped(): lax.ppermute(value, axis, [(i, i ^ bit) for i in range(lax.axis_size(axis...  18.4 us
    all_to_all x1, starting transfers between devices, exchange(): lax.all_to_all(blocks, axis, 0, 0, tiled=True, axis_index_groups=groups)  8.58 us
    unnamed x36, local copies, waits for them, and re-layouts  8.38 us
  transfers between devices with their start and end apart: 5, of which 3 were waited for; matrix products, arithmetic and copies ran while one was open for 0% of the time, Pallas kernels for 1%

profile of v3, /device:TPU:65, one launch (start us, length us, event | category | flops | bytes accessed | tf_op | source)
XLA Modules:
  0.0 237.7 jit_solution(16576995670946824630)
XLA Ops:
  7.4 0.0 all-gather.4.cloned.1.call-start
  7.4 0.0 copy-start.14
  7.4 0.7 all-gather.4.cloned.1.call-update
  8.2 0.0 copy-start.12
  8.2 0.0 copy-start.13
  8.2 0.1 pad_add_fusion.place
  8.3 0.0 copy-done.14
  8.3 0.6 copy-done.12
  8.9 0.0 copy-done.13
  8.9 0.0 copy-start.6
  8.9 0.9 copy-done.6
  9.8 0.0 copy-start.7
  9.8 0.9 copy-done.7
  10.7 0.0 copy-start.8
  10.7 0.9 copy-done.8
  11.6 1.6 shard_map.163
  13.2 56.3 %all_to_all.20.parts = f32[16,8,384]{2,1,0:T(8,128)S(1)} all-to-all(f32[16,8,384]{2,1,0:T(8,128)S(1)} %shard_map.163), channel_id=1, replica_groups=mesh['grp'=2,'sp'=16,'tp'=16] {'sp'}, dimensions={0} | all-to-all | bytes 393216 | tf_op jit(solution)/shard_map/all_to_all | solution.py:417
  69.6 0.0 copy-start.9
  69.6 0.0 copy-start.10
  69.6 0.0 copy-start.11
  69.6 17.7 %all_to_all.21.mine = bf16[8,20,8,128]{3,2,1,0:T(8,128)(2,1)S(1)} all-to-all(bf16[8,20,8,128]{3,2,1,0:T(8,128)(2,1)S(1)} %shard_map.164), channel_id=1, replica_groups={{0,2,4,6,8,10,12,14},{1,3,5,7,9,11,13,15},{16,18,20,22,24,26,28,30},{17..., dimensions={0} | all-to-all | bytes 655360 | tf_op jit(solution)/shard_map/all_to_all | solution.py:417
  87.3 7.4 %collective-permute-start = (bf16[8,20,8,128]{3,2,1,0:T(8,128)(2,1)S(1)}, bf16[8,20,8,128]{3,2,1,0:T(8,128)(2,1)S(1)}, u32[]{:S(2)}, u32[]{:S(2)}) collective-permute-start(bf16[8,20,8,128]{3,2,1,0:T(8,128)(2,1)S(1)} %all_to_all.21.mine), channel_id=1, source_target_pairs={{0,1},{1,0},{2,3},{3,2},{4,5},{5,4},{6,7},{7,6},{8,9},{9,8},{10,11... | collective-permute-start | bytes 983048 | tf_op jit(solution)/shard_map/ppermute | solution.py:421
  94.6 1.2 collective-permute-done.theirs
  95.9 0.0 copy-done.1
  95.9 0.0 copy-done.2
  95.9 0.0 copy-done.9
  95.9 0.0 copy-done.10
  95.9 0.0 copy-done.11
  95.9 0.6 copy-done.15
  96.5 0.0 copy-done.16
  96.6 1.2 copy-done.3
  97.8 1.2 copy-done.4
  99.0 9.0 %shard_map.165 = (bf16[16,160,128]{2,1,0:T(8,128)(2,1)}, bf16[2,128,128]{2,1,0:T(8,128)(2,1)S(1)}, f32[128,128]{1,0:T(8,128)S(1)}, f32[16,8,256]{2,1,0:T(8,128)S(1)}) custom-call(s32[3]{0:T(128)S(1)} %pad_add_fusion.place, bf16[8,20,8,128]{3,2,1,0:T(8,128)(2,1)S(1)} %all_to_all.21.mine, bf16[8,20,8,128]{3,2,1,0:T(8,128)(2,1)S(1)} %collective-permute-done.theirs, ...), custom_call_target="tpu_custom_call" | custom-call | flops 603979776 | bytes 4949516 | tf_op jit(solution)/shard_map/pallas_call | solution.py:25
  108.0 8.6 %all-to-all-start.2 = ((bf16[16,160,128]{2,1,0:T(8,128)(2,1)}), bf16[16,160,128]{2,1,0:T(8,128)(2,1)S(1)}, u32[]{:S(2)}, u32[]{:S(2)}) async-start(bf16[16,160,128]{2,1,0:T(8,128)(2,1)} %get-tuple-element.11), calls=%async_computation.2 | async-start | bytes 1310720 | tf_op jit(solution)/shard_map/all_to_all | solution.py:417
  116.6 0.1 all-gather.6.cloned.1.call-start
  116.7 0.6 all-gather.6.cloned.1.call-update
  117.3 67.7 %all-gather.6.cloned.1.call-done = bf16[2048,256]{1,0:T(8,128)(2,1)} async-done(((bf16[128,256]{1,0:T(8,128)(2,1)}), bf16[2048,256]{1,0:T(8,128)(2,1)}) %all-gather.6.cloned.1.call-update) | async-done | bytes 1048592 | tf_op jit(solution)/shard_map/all_gather | solution.py:475
  184.9 0.0 all-to-all-done.2.maps
  184.9 0.7 copy-done.17
  185.6 1.2 copy-done
  186.8 7.5 %shard_map.166 = (bf16[8,8,4096]{2,1,0:T(8,128)(2,1)S(1)}, bf16[8,8,4096]{2,1,0:T(8,128)(2,1)S(1)}) custom-call(s32[3]{0:T(128)S(1)} %pad_add_fusion.place, bf16[16,160,128]{2,1,0:T(8,128)(2,1)S(1)} %all-to-all-done.2.maps, bf16[2,128,128]{2,1,0:T(8,128)(2,1)S(1)} %get-tuple-element.12.asked, f32[128,128]{1,0:T(8,128)S(1)} %get-tuple-element.13.base, ...), custom_call_target="tpu_custom_call" | custom-call | flops 134217728 | bytes 1868812 | tf_op jit(solution)/shard_map/pallas_call | solution.py:25
  194.4 11.1 %collective-permute-start.1 = (bf16[8,8,4096]{2,1,0:T(8,128)(2,1)S(1)}, bf16[8,8,4096]{2,1,0:T(8,128)(2,1)S(1)}, u32[]{:S(2)}, u32[]{:S(2)}) collective-permute-start(bf16[8,8,4096]{2,1,0:T(8,128)(2,1)S(1)} %get-tuple-element.15), channel_id=1, source_target_pairs={{0,1},{1,0},{2,3},{3,2},{4,5},{5,4},{6,7},{7,6},{8,9},{9,8},{10,11... | collective-permute-start | bytes 1572872 | tf_op jit(solution)/shard_map/ppermute | solution.py:421
  205.4 1.5 collective-permute-done.1
  206.9 0.1 add_convert_fusion
  207.1 0.0 copy-start.5
  207.1 22.4 %all_to_all.22.parts = bf16[8,8,4096]{2,1,0:T(8,128)(2,1)S(1)} all-to-all(bf16[8,8,4096]{2,1,0:T(8,128)(2,1)S(1)} %add_convert_fusion), channel_id=1, replica_groups={{0,2,4,6,8,10,12,14},{1,3,5,7,9,11,13,15},{16,18,20,22,24,26,28,30},{17..., dimensions={0} | all-to-all | bytes 1048576 | tf_op jit(solution)/shard_map/all_to_all | solution.py:417
  229.5 0.0 copy-done.5
  229.5 0.7 shard_map.167
  (10 shorter events, 0.0 us)
Async XLA Ops:
  7.4 88.5 %all-gather.4.cloned.1.call-start = ((), (), s32[]{:S(2)}) async-start(), calls=%async_computation.4 | async-start | bytes 1114112 | tf_op jit(solution)/shard_map/all_gather | solution.py:474
  7.4 0.9 copy-start.14
  8.2 0.8 copy-start.12
  8.2 0.7 copy-start.13
  8.9 0.9 copy-start.6
  9.8 0.9 copy-start.7
  10.7 0.9 copy-start.8
  11.6 84.2 %copy-start.1 = (bf16[4096,128]{1,0:T(8,128)(2,1)S(1)}, bf16[4096,128]{1,0:T(8,128)(2,1)}, u32[]{:S(2)}) copy-start(bf16[4096,128]{1,0:T(8,128)(2,1)} %wq.1) | copy-start | bytes 3145732
  11.6 84.2 %copy-start.2 = (bf16[4096,128]{1,0:T(8,128)(2,1)S(1)}, bf16[4096,128]{1,0:T(8,128)(2,1)}, u32[]{:S(2)}) copy-start(bf16[4096,128]{1,0:T(8,128)(2,1)} %wk.1) | copy-start | bytes 3145732
  69.6 26.3 %copy-start.9 = (bf16[8,4096]{1,0:T(8,128)(2,1)S(1)}, bf16[8,4096]{1,0:T(8,128)(2,1)}, u32[]{:S(2)}) copy-start(bf16[8,4096]{1,0:T(8,128)(2,1)} %context_.1) | copy-start | bytes 196612
  69.6 26.3 %copy-start.10 = (bf16[64,128]{1,0:T(8,128)(2,1)S(1)}, bf16[64,128]{1,0:T(8,128)(2,1)}, u32[]{:S(2)}) copy-start(bf16[64,128]{1,0:T(8,128)(2,1)} %fading_.3) | copy-start | bytes 49156
  69.6 26.3 %copy-start.11 = (bf16[64,128]{1,0:T(8,128)(2,1)S(1)}, bf16[64,128]{1,0:T(8,128)(2,1)}, u32[]{:S(2)}) copy-start(bf16[64,128]{1,0:T(8,128)(2,1)} %step_.3) | copy-start | bytes 49156
  87.3 8.6 %collective-permute-start = (bf16[8,20,8,128]{3,2,1,0:T(8,128)(2,1)S(1)}, bf16[8,20,8,128]{3,2,1,0:T(8,128)(2,1)S(1)}, u32[]{:S(2)}, u32[]{:S(2)}) collective-permute-start(bf16[8,20,8,128]{3,2,1,0:T(8,128)(2,1)S(1)} %all_to_all.21.mine), channel_id=1, source_target_pairs={{0,1},{1,0},{2,3},{3,2},{4,5},{5,4},{6,7},{7,6},{8,9},{9,8},{10,11... | collective-permute-start | bytes 983048 | tf_op jit(solution)/shard_map/ppermute | solution.py:421
  95.9 0.7 copy-start.15
  95.9 0.7 copy-start.16
  96.6 1.2 copy-start.3
  97.8 1.2 copy-start.4
  108.0 76.9 %all-to-all-start.2 = ((bf16[16,160,128]{2,1,0:T(8,128)(2,1)}), bf16[16,160,128]{2,1,0:T(8,128)(2,1)S(1)}, u32[]{:S(2)}, u32[]{:S(2)}) async-start(bf16[16,160,128]{2,1,0:T(8,128)(2,1)} %get-tuple-element.11), calls=%async_computation.2 | async-start | bytes 1310720 | tf_op jit(solution)/shard_map/all_to_all | solution.py:417
  116.6 68.3 %all-gather.6.cloned.1.call-start = ((), (), s32[]{:S(2)}) async-start(), calls=%async_computation.5 | async-start | bytes 1114112 | tf_op jit(solution)/shard_map/all_gather | solution.py:475
  184.9 0.7 copy-start.17
  185.6 1.2 copy-start
  194.4 12.6 %collective-permute-start.1 = (bf16[8,8,4096]{2,1,0:T(8,128)(2,1)S(1)}, bf16[8,8,4096]{2,1,0:T(8,128)(2,1)S(1)}, u32[]{:S(2)}, u32[]{:S(2)}) collective-permute-start(bf16[8,8,4096]{2,1,0:T(8,128)(2,1)S(1)} %get-tuple-element.15), channel_id=1, source_target_pairs={{0,1},{1,0},{2,3},{3,2},{4,5},{5,4},{6,7},{7,6},{8,9},{9,8},{10,11... | collective-permute-start | bytes 1572872 | tf_op jit(solution)/shard_map/ppermute | solution.py:421
  207.1 22.4 %copy-start.5 = (bf16[8,4096]{1,0:T(8,128)(2,1)S(1)}, bf16[8,4096]{1,0:T(8,128)(2,1)}, u32[]{:S(2)}) copy-start(bf16[8,4096]{1,0:T(8,128)(2,1)} %hidden.1) | copy-start | bytes 196612
Sparse Core Ops, SparseCore 0:
  10.3 79.9 all-gather.3
Sparse Core Ops, SparseCore 1:
  119.2 65.7 all-gather.5

commit v4 on v3

--- a/solution.py
+++ b/solution.py
@@ -12,6 +12,7 @@
 EPS_KEY = 1e-06
 RATE_SHIFT = 5.0
 NEVER = -1e30
+SOME, ALL = 32 * 1024 * 1024, 63 * 1024 * 1024
 BF16, F32 = jnp.bfloat16, jnp.float32
 
 VMEM = pl.BlockSpec(memory_space=pltpu.VMEM)
@@ -19,7 +20,7 @@
 HBM = pl.BlockSpec(memory_space=pltpu.HBM)
 
 
-def call(body, outs, *args, flops=0, scalars=0, scratch=(), fetched=0):
+def call(body, outs, *args, flops=0, scalars=0, scratch=(), fetched=0, room=SOME):
     many = isinstance(outs, list)
     shapes = [jax.ShapeDtypeStruct(s, d) for s, d in (outs if many else [outs])]
     got = pl.pallas_call(
@@ -28,7 +29,7 @@
         in_specs=[SMEM] * scalars + [VMEM] * (len(args) - scalars - fetched) + [HBM] * fetched,
         out_specs=[VMEM] * len(shapes),
         scratch_shapes=list(scratch),
-        compiler_params=pltpu.CompilerParams(vmem_limit_bytes=48 * 1024 * 1024),
+        compiler_params=pltpu.CompilerParams(vmem_limit_bytes=room),
         cost_estimate=pl.CostEstimate(
             flops=flops, transcendentals=0, bytes_accessed=sum(a.size * a.dtype.itemsize for a in args)
         ),
@@ -44,6 +45,31 @@
 
 def iota(shape, dim):
     return lax.broadcasted_iota(jnp.int32, shape, dim)
+
+
+USED = 5
+
+
+def packed_lines(total, lanes):
+    high = total.astype(BF16).astype(F32)
+    rest = total - high
+    row = iota((total.shape[0], lanes), 0)
+    last = rest[:, lanes:]
+    free = total.shape[0] - USED
+    return [
+        jnp.where(row < USED, high[:, :lanes], pltpu.roll(last, USED, 0)).astype(BF16),
+        jnp.where(row < USED, high[:, lanes:], pltpu.roll(last, USED - free, 0)).astype(BF16),
+        rest[:, :lanes].astype(BF16),
+    ]
+
+
+def unpacked_lines(first, second, third):
+    first, second, third = (part.astype(F32) for part in (first, second, third))
+    count = first.shape[0]
+    row = iota(first.shape, 0)
+    free = count - USED
+    last = jnp.where(row < free, pltpu.roll(first, count - USED, 0), pltpu.roll(second, count - USED + free, 0))
+    return jnp.concatenate([first + third, second + last], axis=1)
 
 
 def partials_kernel(place, sample, prompt, lower, shifting, stretch, valve, out, conds, low_rows, held, sems):
@@ -54,7 +80,7 @@
         copy.start()
     for copy in copies[:3]:
         copy.wait()
-    _, rows, _ = out.shape
+    peers, _, rows, _ = out.shape
     chunk = held.shape[2]
     wide = chunk // sample.shape[1]
     line = iota(sample.shape, 0)
@@ -84,20 +110,17 @@
     for copy in copies[3:]:
         copy.wait()
     total = dot(at(0, True), held[0]) + dot(at(2, True), held[1]) + dot(at(4, False), held[2])
-    out[...] = jnp.broadcast_to(jnp.concatenate([total, piece], axis=1)[None], out.shape)
+    for n, block in enumerate(packed_lines(total, out.shape[3]) + [piece.astype(BF16)]):
+        for p in range(peers):
+            out[p, n] = block
 
 
 def sum_kernel(parts, out):
-    chunk = parts.shape[2] - out.shape[3]
     lanes = out.shape[3]
-    total = parts[0, :, :chunk]
+    total = unpacked_lines(parts[0, 0], parts[0, 1], parts[0, 2])
     for k in range(1, parts.shape[0]):
-        total = total + parts[k, :, :chunk]
-    high = total.astype(BF16)
-    rest = (total - high.astype(F32)).astype(BF16)
-    blocks = [parts[k, :, chunk:].astype(BF16) for k in range(parts.shape[0])]
-    for value in (high, rest):
-        blocks += [value[:, n : n + lanes] for n in range(0, chunk, lanes)]
+        total = total + unpacked_lines(parts[k, 0], parts[k, 1], parts[k, 2])
+    blocks = [parts[k, 3] for k in range(parts.shape[0])] + packed_lines(total, lanes)
     for p in range(out.shape[0]):
         for n, block in enumerate(blocks):
             out[p, n] = block
@@ -105,6 +128,21 @@
 
 def by_core(core, own, other):
     return jnp.where(core == 0, own, other), jnp.where(core == 0, other, own)
+
+
+def mask_of(n, count):
+    half = count // 2
+    bits = half.bit_length() - 1
+    inner = n % half
+    mask = sum(((inner >> b) & 1) << (bits - b) for b in range(bits))
+    return mask | (n // half)
+
+
+def placed_rows(value, tp, held):
+    count, rows, lanes = held.shape
+    for n in range(count):
+        held[tp ^ mask_of(n, count)] = value[n * rows : (n + 1) * rows]
+    return held[...].reshape(count * rows, lanes)
 
 
 def moments(ref, lane):
@@ -121,18 +159,14 @@
     return centre, lax.rsqrt(spread + EPS_ROW)
 
 
-def modulated(place, latent, context, mine, theirs, u, vectors, down):
-    count, width = latent.shape
-    extra = context.shape[0]
+def modulated(place, near, far, context, mine, theirs, u, vectors, down):
+    half, width = near.shape
+    count, extra = 2 * half, context.shape[0]
     lane, lanes = vectors.shape[2], mine.shape[3]
-    spans = lane // lanes
-    stats = [moments(ref, lane) for ref in (latent, context)]
-    first = mine.shape[1] - 2 * spans
+    stats = [moments(ref, lane) for ref in (near, far, context)]
+    first = mine.shape[1] - 3
     for x in range(mine.shape[0]):
-        found = []
-        for ref in (mine, theirs):
-            cut = [ref[x, first + n].astype(F32) + ref[x, first + spans + n].astype(F32) for n in range(spans)]
-            found.append(jnp.concatenate(cut, axis=1))
+        found = [unpacked_lines(ref[x, first], ref[x, first + 1], ref[x, first + 2]) for ref in (mine, theirs)]
         vectors[2 * x], vectors[2 * x + 1] = by_core(place[1], *found)
     pad = jnp.zeros((u.shape[0] - count - extra, lane), F32)
     for t in range(width // lane):
@@ -142,8 +176,9 @@
             normed = (ref[:, cols].astype(F32) - stats[n][0]) * stats[n][1]
             return normed * (1.0 + vectors[t, 2 + i : 3 + i, :]) + vectors[t, i : i + 1, :]
 
-        u[:count, cols] = one(0, latent, 0).astype(BF16)
-        u[count:, cols] = jnp.concatenate([one(1, context, 1), pad], axis=0).astype(BF16)
+        u[:half, cols] = one(0, near, 0).astype(BF16)
+        u[half:count, cols] = one(1, far, 0).astype(BF16)
+        u[count:, cols] = jnp.concatenate([one(2, context, 1), pad], axis=0).astype(BF16)
     for s in range(down.shape[0] // (2 * lanes)):
         even, odd = by_core(place[1], mine[:, s].astype(F32), theirs[:, s].astype(F32))
         piece = jnp.stack([even, odd], axis=1).reshape(lanes, lanes)
@@ -306,46 +341,68 @@
 
 
 def block_kernel(
-    place, mine, theirs, latent_, context_, wq, wk, wv, fading_, step_, rates_, spikes_,
+    place, mine, theirs, near, far, context_, wq, wk, wv, fading_, step_, rates_, spikes_,
     sent, asked, base, vectors,
-    latent, context, held, fading, step, rates, spikes, u, down, sems,
+    context, held, fading, step, rates, spikes, u, down, moved_q, moved_k, moved_v, moved_low, sems,
 ):
-    pairs = [(latent_, latent), (context_, context)]
+    pairs = [(context_, context)]
     pairs += [(ref, held.at[n]) for n, ref in enumerate((wq, wk, wv))]
     pairs += [(fading_, fading), (step_, step), (rates_, rates), (spikes_, spikes)]
     copies = [pltpu.make_async_copy(ref, to, sems.at[n]) for n, (ref, to) in enumerate(pairs)]
     for copy in copies:
         copy.start()
-    for copy in copies[:2]:
+    copies[0].wait()
+    modulated(place, near, far, context, mine, theirs, u, vectors, down)
+    for copy in copies[1:]:
         copy.wait()
-    modulated(place, latent, context, mine, theirs, u, vectors, down)
-    for copy in copies[2:]:
-        copy.wait()
-    count, extra = latent.shape[0], context.shape[0]
-    q = dot(u[:count], held[0]).astype(BF16)
-    k, v = dot(u[...], held[1]).astype(BF16), dot(u[...], held[2]).astype(BF16)
+    count, extra = asked.shape[1], context.shape[0]
     low = dot(u[...], down[...])
-    low = jnp.where(iota(low.shape, 1) < HEAD, low, 0.0).astype(BF16)
+    low = jnp.where(iota(low.shape, 1) < HEAD, low, 0.0)
+    k, v = dot(u[...], held[1]), dot(u[...], held[2])
+    own = [
+        placed_rows(part[:count], place[2], to).astype(BF16)
+        for part, to in ((low, moved_low), (k, moved_k), (v, moved_v), (dot(u[:count], held[0]), moved_q))
+    ]
     ahead, behind = block_terms(
-        k[:count], v[:count], low[:count, :HEAD], fading[...], step[...], rates[...], spikes[...], q
+        own[1], own[2], own[0][:, :HEAD], fading[...], step[...], rates[...], spikes[...], own[3]
     )
     same = same_head(ahead[0].shape)
-    packed = [
-        jnp.where(same, factor, pltpu.roll(offset, HEAD, 0)).astype(BF16)
-        for factor, offset in (ahead[:2], behind[:2])
-    ]
-    tail = [part[count:].astype(F32)[:extra] for part in (k, v, low)]
-    tail = jnp.concatenate(tail + [jnp.zeros_like(tail[0])] * (-len(tail) % 2), axis=0).astype(BF16)
-    size = packed[0].shape[0]
-    for j in range(sent.shape[0]):
-        sent[j, :size] = jnp.where(place[0] < j, packed[0], packed[1])
-        sent[j, size:] = tail
+    size = same.shape[0]
+    for n, (factor, offset) in enumerate((ahead[:2], behind[:2])):
+        sent[n * size : (n + 1) * size] = jnp.where(same, factor, pltpu.roll(offset, HEAD, 0)).astype(BF16)
+    tail = [part[count : count + extra] for part in (k, v, low)]
+    sent[2 * size :] = jnp.concatenate(tail + [jnp.zeros_like(tail[0])], axis=0).astype(BF16)
     asked[0], asked[1] = ahead[2].astype(BF16), behind[2].astype(BF16)
     base[...] = ahead[3] + behind[3]
 
 
+def opened(packed, same):
+    packed = packed.astype(F32)
+    return jnp.where(same, packed, 0.0), jnp.where(same, pltpu.roll(packed, HEAD, 0), 0.0)
+
+
+def pair_kernel(place, mine, other, out):
+    pairs, _, size = out.shape
+    odd = place[0] % 2
+    same = same_head((size, size))
+    early = jnp.where(odd == 0, mine[...].astype(F32), other[...].astype(F32))
+    late = jnp.where(odd == 0, other[...].astype(F32), mine[...].astype(F32))
+    both = []
+    for first, second, at in ((early, late, 0), (late, early, size)):
+        left, right = (opened(part[at : at + size], same) for part in (first, second))
+        new = dot(jnp.concatenate(left, axis=0), right[0])
+        both.append(jnp.where(same, new[:size], pltpu.roll(new[size:] + right[1], HEAD, 0)).astype(BF16))
+    extra = (early.shape[0] - 2 * size) // 4
+    tails = [[part[2 * size + n * extra : 2 * size + (n + 1) * extra] for part in (early, late)] for n in range(3)]
+    low = tails[2][0] + pltpu.roll(tails[2][1], HEAD, 1)
+    tail = jnp.concatenate(tails[0] + tails[1] + [low, jnp.zeros_like(low)], axis=0).astype(BF16)
+    for j in range(pairs):
+        out[j, :size] = jnp.where(place[0] // 2 < j, both[0], both[1])
+        out[j, size:] = tail
+
+
 def read_kernel(
-    place, maps, asked, base, fading_, step_, rates_, gains_, emit_,
+    place, maps, other, asked, base, fading_, step_, rates_, gains_, emit_,
     keep, give,
     fading, step, rates, gains, emit, sems,
 ):
@@ -357,24 +414,34 @@
     extra = keep.shape[1]
     same = same_head((size, size))
     me, core = place[0], place[1]
+    mine = me // 2
     for copy in copies[:4]:
         copy.wait()
+    wide = 2 * extra
     parts = [
-        jnp.concatenate([maps[j, size + n * extra : size + (n + 1) * extra].astype(F32) for j in range(peers)], axis=0)
-        for n in range(3)
+        jnp.concatenate([maps[j, size + n * wide : size + (n + 1) * wide].astype(F32) for j in range(peers)], axis=0)
+        for n in range(2)
     ]
-    parts = [part.astype(BF16) for part in parts]
+    low = []
+    for j in range(peers):
+        packed = maps[j, size + 2 * wide : size + 2 * wide + extra].astype(F32)
+        low += [packed, pltpu.roll(packed, HEAD, 1)]
+    parts = [part.astype(BF16) for part in (*parts, jnp.concatenate(low, axis=0))]
     context = block_terms(parts[0], parts[1], parts[2][:, :HEAD], fading[...], step[...], rates[...])
     eye = (iota((size, size), 0) == iota((size, size), 1)).astype(F32)
     composed = [jnp.concatenate([eye, jnp.zeros_like(eye)], axis=0) for _ in range(2)]
+
+    def follow(d, packed, reached):
+        factor, offset = opened(packed, same)
+        new = dot(composed[d], factor)
+        new = jnp.concatenate([new[:size], new[size:] + offset], axis=0)
+        composed[d] = jnp.where(reached, new, composed[d])
+
     for n in range(peers - 1):
-        for d, j, reached in ((0, n, n < me), (1, peers - 1 - n, peers - 1 - n > me)):
-            packed = maps[j, :size].astype(F32)
-            factor = jnp.where(same, packed, 0.0)
-            offset = jnp.where(same, pltpu.roll(packed, HEAD, 0), 0.0)
-            new = dot(composed[d], factor)
-            new = jnp.concatenate([new[:size], new[size:] + offset], axis=0)
-            composed[d] = jnp.where(reached, new, composed[d])
+        follow(0, maps[n, :size], n < mine)
+        follow(1, maps[peers - 1 - n, :size], peers - 1 - n > mine)
+    follow(0, other[:size], me % 2 == 1)
+    follow(1, other[size : 2 * size], me % 2 == 0)
     out = base[...]
     for d in range(2):
         start = jnp.where(same, context[d][1], 0.0)
@@ -453,7 +520,7 @@
 
     parts = call(
         partials_kernel,
-        ((n_sp, 8, chunk + lanes), F32),
+        ((n_sp, 4, 8, lanes), BF16),
         place,
         sample_cond.reshape(-1, lanes),
         prompt_cond.reshape(-1, lanes),
@@ -463,6 +530,7 @@
         skip_valve,
         scalars=1,
         fetched=6,
+        room=ALL,
         flops=8 * span * chunk * 6,
         scratch=[
             pltpu.VMEM((2, width // lanes, lanes), BF16),
@@ -471,12 +539,17 @@
             pltpu.SemaphoreType.DMA((6,)),
         ],
     )
-    latent = lax.all_gather(hidden_items, "tp", axis=0, tiled=True)
     emit = lax.all_gather(emit_matrix, "sp", axis=0)
     parts = exchange(parts, "sp")
 
-    spans = chunk // lanes
-    mine = call(sum_kernel, ((chips, n_sp + 2 * spans, 8, lanes), BF16), parts)
+    near, bit = hidden_items[None], n_tp // 2
+    while bit > 1:
+        far = swapped(near, "tp", bit)
+        near = jnp.concatenate([near, far], axis=0)
+        bit //= 2
+    far = swapped(near, "tp", 1)
+
+    mine = call(sum_kernel, ((chips, n_sp + 3, 8, lanes), BF16), parts)
     mine = exchange(mine, "tp", same_core)
     theirs = swapped(mine, "tp", 1)
 
@@ -490,7 +563,7 @@
     sent, asked, base, vectors = call(
         block_kernel,
         [
-            ((n_sp, lanes + 4 * extra, lanes), BF16),
+            ((2 * lanes + 4 * extra, lanes), BF16),
             ((2, count, lanes), BF16),
             ((count, lanes), F32),
             ((n_tp, 8, chunk), F32),
@@ -498,7 +571,8 @@
         place,
         mine,
         theirs,
-        latent,
+        near.reshape(count // 2, width),
+        far.reshape(count // 2, width),
         prompt_items,
         receiver_matrix,
         address_matrix,
@@ -508,25 +582,37 @@
         rates,
         spike_logfade.T,
         scalars=1,
-        fetched=9,
+        fetched=8,
+        room=ALL,
         flops=2 * padded * width * lanes * 4,
         scratch=[
-            pltpu.VMEM((count, width), BF16),
             pltpu.VMEM((extra, width), BF16),
             pltpu.VMEM((3, width, lanes), BF16),
             *small,
             pltpu.VMEM(spike_logfade.shape[::-1], F32),
             pltpu.VMEM((padded, width), BF16),
             pltpu.VMEM((width, lanes), BF16),
-            pltpu.SemaphoreType.DMA((9,)),
+            *[pltpu.VMEM((n_tp, rows, lanes), F32)] * 4,
+            pltpu.SemaphoreType.DMA((8,)),
         ],
     )
-    maps = exchange(sent, "sp")
+    other = swapped(sent, "sp", 1)
+    sent = call(
+        pair_kernel,
+        ((n_sp // 2, lanes + 6 * extra, lanes), BF16),
+        place,
+        sent,
+        other,
+        scalars=1,
+        flops=2 * 128**3 * 8,
+    )
+    maps = exchange(sent, "sp", [[2 * i + c for i in range(n_sp // 2)] for c in range(2)])
     keep, give = call(
         read_kernel,
         [((chips, rows, width), BF16)] * 2,
         place,
         maps,
+        other,
         asked,
         base,
         fading_raise_matrix,
@@ -536,6 +622,7 @@
         emit,
         scalars=1,
         fetched=5,
+        room=ALL,
         flops=2 * count * lanes * width,
         scratch=[
             *small,

time: 238 us -> 202 us (0.85)
  blocking collectives: 96.4 us -> 23.4 us
  starting transfers between devices: 27.1 us -> 89.5 us
  waiting for transfers between devices: 71.7 us -> 43.8 us
  local copies, waits for them, and re-layouts: 8.38 us -> 2.39 us
  Pallas kernels: 18.8 us -> 24.5 us
  other arithmetic: 0.21 us -> 3.58 us
    all_to_all x3 -> x1, blocking collectives: 96.4 us -> 23.4 us  [exchange(): lax.all_to_all(blocks, axis, 0, 0, tiled=True, axis_index_groups=groups)]
    all_gather x1, waiting for transfers between devices: 67.7 us -> 14.4 us  [shards(): emit = lax.all_gather(emit_matrix, 'sp', axis=0)]
    all_to_all x1 -> x3, starting transfers between devices: 8.58 us -> 53.9 us  [exchange(): lax.all_to_all(blocks, axis, 0, 0, tiled=True, axis_index_groups=groups)]
    all_to_all x1 -> x3, waiting for transfers between devices: 0.01 us -> 21.6 us  [exchange(): lax.all_to_all(blocks, axis, 0, 0, tiled=True, axis_index_groups=groups)]
    ppermute x2 -> x7, starting transfers between devices: 18.4 us -> 35.6 us  [swapped(): lax.ppermute(value, axis, [(i, i ^ bit) for i in range(lax.axis_size(axis...]
    unnamed x36 -> x18, local copies, waits for them, and re-layouts: 8.38 us -> 2.39 us
    pallas_call x5 -> x6, Pallas kernels: 18.8 us -> 24.5 us  [call(): pl.pallas_call(body, out_shape=shapes, in_specs=[SMEM] * scalars + [VMEM]...]
    ppermute x2 -> x7, waiting for transfers between devices: 2.75 us -> 7.78 us  [swapped(): lax.ppermute(value, axis, [(i, i ^ bit) for i in range(lax.axis_size(axis...]
  transfers between devices with their start and end apart: 5 -> 11, of which waited for: 3 -> 8; matrix products, arithmetic and copies ran while one was open for 0% -> 1% of each run, Pallas kernels for 1% -> 7%
where the time goes in v4:
time: 202 us; the launch traced here: 201 us
  starting transfers between devices  89.5 us (44%)
  waiting for transfers between devices  43.8 us (22%)
  Pallas kernels  24.5 us (12%)
  blocking collectives  23.4 us (12%)
  between operations  13.6 us (7%)
  other arithmetic  3.58 us (2%)
  local copies, waits for them, and re-layouts  2.39 us (1%)
    all_to_all x3, starting transfers between devices, exchange(): lax.all_to_all(blocks, axis, 0, 0, tiled=True, axis_index_groups=groups)  53.9 us
    ppermute x7, starting transfers between devices, swapped(): lax.ppermute(value, axis, [(i, i ^ bit) for i in range(lax.axis_size(axis...  35.6 us
    pallas_call x6, Pallas kernels, call(): pl.pallas_call(body, out_shape=shapes, in_specs=[SMEM] * scalars + [VMEM]...  24.5 us
    all_to_all x1, blocking collectives, exchange(): lax.all_to_all(blocks, axis, 0, 0, tiled=True, axis_index_groups=groups)  23.4 us
    all_to_all x3, waiting for transfers between devices, exchange(): lax.all_to_all(blocks, axis, 0, 0, tiled=True, axis_index_groups=groups)  21.6 us
    all_gather x1, waiting for transfers between devices, shards(): emit = lax.all_gather(emit_matrix, 'sp', axis=0)  14.4 us
    ppermute x7, waiting for transfers between devices, swapped(): lax.ppermute(value, axis, [(i, i ^ bit) for i in range(lax.axis_size(axis...  7.78 us
  transfers between devices with their start and end apart: 11, of which 8 were waited for; matrix products, arithmetic and copies ran while one was open for 1% of the time, Pallas kernels for 7%

profile of v4, /device:TPU:65, one launch (start us, length us, event | category | flops | bytes accessed | tf_op | source)
XLA Modules:
  0.0 200.8 jit_solution(12693743796530629733)
XLA Ops:
  6.5 8.5 %collective-permute-start.1 = (bf16[1,8,4096]{2,1,0:T(8,128)(2,1)}, bf16[1,8,4096]{2,1,0:T(8,128)(2,1)S(1)}, u32[]{:S(2)}, u32[]{:S(2)}) collective-permute-start(bf16[1,8,4096]{2,1,0:T(8,128)(2,1)} %bitcast.14), channel_id=1, source_target_pairs={{0,8},{1,9},{2,10},{3,11},{4,12},{5,13},{6,14},{7,15},{8,0},{9,1},... | collective-permute-start | bytes 196616 | tf_op jit(solution)/shard_map/ppermute | solution.py:488
  15.0 2.0 collective-permute-done.1
  17.0 0.9 pad_maximum_fusion.2
  17.9 5.2 %collective-permute-start.2 = (bf16[2,8,4096]{2,1,0:T(8,128)(2,1)S(1)}, bf16[2,8,4096]{2,1,0:T(8,128)(2,1)S(1)}, u32[]{:S(2)}, u32[]{:S(2)}) collective-permute-start(bf16[2,8,4096]{2,1,0:T(8,128)(2,1)S(1)} %pad_maximum_fusion.2), channel_id=1, source_target_pairs={{0,4},{1,5},{2,6},{3,7},{4,0},{5,1},{6,2},{7,3},{8,12},{9,13},{10,... | collective-permute-start | bytes 393224 | tf_op jit(solution)/shard_map/ppermute | solution.py:488
  23.1 0.7 pad_add_fusion.place
  23.7 2.6 %shard_map.163 = bf16[16,4,8,128]{3,2,1,0:T(8,128)(2,1)} custom-call(s32[3]{0:T(128)} %pad_add_fusion.place, bf16[32,128]{1,0:T(8,128)(2,1)} %bitcast.21, bf16[32,128]{1,0:T(8,128)(2,1)} %bitcast.22, bf16[64,256]{1,0:T(8,128)(2,1)} %bitcast.20, bf16[256,256]{1,0:T(8,128)(2,1)} %shifting.1, bf16[256,256]{1,0:T(8,128)(2,1)} %stretch.1, bf16[256,256]{1,0:T(8,128)(2,1)} %valve.1), custom_call_target="tpu_custom_call" | custom-call | flops 3145728 | bytes 442380 | tf_op jit(solution)/shard_map/pallas_call | solution.py:26
  26.4 0.0 copy-start
  26.4 44.5 %all-to-all-start = ((bf16[16,4,8,128]{3,2,1,0:T(8,128)(2,1)}), bf16[16,4,8,128]{3,2,1,0:T(8,128)(2,1)S(1)}, u32[]{:S(2)}, u32[]{:S(2)}) async-start(bf16[16,4,8,128]{3,2,1,0:T(8,128)(2,1)} %shard_map.163), calls=%async_computation | async-start | bytes 262144 | tf_op jit(solution)/shard_map/all_to_all | solution.py:484
  70.9 0.1 all-gather.3.cloned.1.call-start
  70.9 0.0 collective-permute-done.2
  70.9 0.0 copy-done
  71.0 2.0 collective-permute-start.3
  72.9 0.1 all-gather.3.cloned.1.call-update
  73.0 9.6 %all-to-all-done.parts = bf16[16,4,8,128]{3,2,1,0:T(8,128)(2,1)S(1)} async-done(((bf16[16,4,8,128]{3,2,1,0:T(8,128)(2,1)}), bf16[16,4,8,128]{3,2,1,0:T(8,128)(2,1)S(1)}, u32[]{:S(2)}, u32[]{:S(2)}) %all-to-all-start) | async-done | bytes 131104 | tf_op jit(solution)/shard_map/all_to_all | solution.py:484
  82.6 0.8 shard_map.164
  83.4 4.2 %all-to-all-start.1 = ((bf16[8,19,8,128]{3,2,1,0:T(8,128)(2,1)}), bf16[8,19,8,128]{3,2,1,0:T(8,128)(2,1)S(1)}, u32[]{:S(2)}, u32[]{:S(2)}) async-start(bf16[8,19,8,128]{3,2,1,0:T(8,128)(2,1)} %shard_map.164), calls=%async_computation.1 | async-start | bytes 622592 | tf_op jit(solution)/shard_map/all_to_all | solution.py:484
  87.6 0.0 collective-permute-done.3
  87.6 0.9 pad_maximum_fusion
  88.5 5.9 %collective-permute-start.4 = (bf16[8,8,4096]{2,1,0:T(8,128)(2,1)S(1)}, bf16[8,8,4096]{2,1,0:T(8,128)(2,1)S(1)}, u32[]{:S(2)}, u32[]{:S(2)}) collective-permute-start(bf16[8,8,4096]{2,1,0:T(8,128)(2,1)S(1)} %get-tuple-element.17), channel_id=1, source_target_pairs={{0,1},{1,0},{2,3},{3,2},{4,5},{5,4},{6,7},{7,6},{8,9},{9,8},{10,11... | collective-permute-start | bytes 1572872 | tf_op jit(solution)/shard_map/ppermute | solution.py:488
  94.4 3.2 %all-to-all-done.1.mine = bf16[8,19,8,128]{3,2,1,0:T(8,128)(2,1)S(1)} async-done(((bf16[8,19,8,128]{3,2,1,0:T(8,128)(2,1)}), bf16[8,19,8,128]{3,2,1,0:T(8,128)(2,1)S(1)}, u32[]{:S(2)}, u32[]{:S(2)}) %all-to-all-start.1) | async-done | bytes 311328 | tf_op jit(solution)/shard_map/all_to_all | solution.py:484
  97.6 0.0 copy-start.6
  97.6 6.9 %collective-permute-start = (bf16[8,19,8,128]{3,2,1,0:T(8,128)(2,1)S(1)}, bf16[8,19,8,128]{3,2,1,0:T(8,128)(2,1)S(1)}, u32[]{:S(2)}, u32[]{:S(2)}) collective-permute-start(bf16[8,19,8,128]{3,2,1,0:T(8,128)(2,1)S(1)} %all-to-all-done.1.mine), channel_id=1, source_target_pairs={{0,1},{1,0},{2,3},{3,2},{4,5},{5,4},{6,7},{7,6},{8,9},{9,8},{10,11... | collective-permute-start | bytes 933896 | tf_op jit(solution)/shard_map/ppermute | solution.py:488
  104.5 0.0 collective-permute-done.4
  104.5 0.0 copy-start.7
  104.5 1.2 collective-permute-done.theirs
  105.7 0.7 copy-done.8
  106.5 0.0 copy-done.6
  106.5 0.0 copy-done.7
  106.5 10.0 %shard_map.165 = (bf16[288,128]{1,0:T(8,128)(2,1)}, bf16[2,128,128]{2,1,0:T(8,128)(2,1)}, f32[128,128]{1,0:T(8,128)}, f32[16,8,256]{2,1,0:T(8,128)}) custom-call(s32[3]{0:T(128)} %pad_add_fusion.place, bf16[8,19,8,128]{3,2,1,0:T(8,128)(2,1)} %copy-done.6, bf16[8,19,8,128]{3,2,1,0:T(8,128)(2,1)} %copy-done.8, bf16[64,4096]{1,0:T(8,128)(2,1)} %get-tuple-element.18.near, ...), custom_call_target="tpu_custom_call" | custom-call | flops 603979776 | bytes 4916748 | tf_op jit(solution)/shard_map/pallas_call | solution.py:26
  116.5 0.0 copy-start.4
  116.5 3.0 %collective-permute-start.5 = (bf16[288,128]{1,0:T(8,128)(2,1)}, bf16[288,128]{1,0:T(8,128)(2,1)S(1)}, u32[]{:S(2)}, u32[]{:S(2)}) collective-permute-start(bf16[288,128]{1,0:T(8,128)(2,1)} %get-tuple-element.11.mine), channel_id=1, source_target_pairs={{0,16},{16,0},{32,48},{48,32},{64,80},{80,64},{96,112},{112,96},{1... | collective-permute-start | bytes 221192 | tf_op jit(solution)/shard_map/ppermute | solution.py:488
  119.4 2.9 %collective-permute-done.5.other = bf16[288,128]{1,0:T(8,128)(2,1)S(1)} collective-permute-done((bf16[288,128]{1,0:T(8,128)(2,1)}, bf16[288,128]{1,0:T(8,128)(2,1)S(1)}, u32[]{:S(2)}, u32[]{:S(2)}) %collective-permute-start.5) | collective-permute-done | bytes 73760 | tf_op jit(solution)/shard_map/ppermute | solution.py:488
  122.4 0.0 copy-done.4
  122.4 0.9 copy-done.3
  123.2 1.5 shard_map.166
  124.7 0.0 copy-done.1
  124.7 5.2 %all-to-all-start.2 = ((bf16[8,176,128]{2,1,0:T(8,128)(2,1)}), bf16[8,176,128]{2,1,0:T(8,128)(2,1)S(1)}, u32[]{:S(2)}, u32[]{:S(2)}) async-start(bf16[8,176,128]{2,1,0:T(8,128)(2,1)} %shard_map.166), calls=%async_computation.2 | async-start | bytes 720896 | tf_op jit(solution)/shard_map/all_to_all | solution.py:484
  130.0 14.4 %all-gather.3.cloned.1.call-done = bf16[2048,256]{1,0:T(8,128)(2,1)} async-done(((bf16[128,256]{1,0:T(8,128)(2,1)}), bf16[2048,256]{1,0:T(8,128)(2,1)}) %all-gather.3.cloned.1.call-update) | async-done | bytes 1048592 | tf_op jit(solution)/shard_map/all_gather | solution.py:542
  144.3 8.8 %all-to-all-done.2.maps = bf16[8,176,128]{2,1,0:T(8,128)(2,1)S(1)} async-done(((bf16[8,176,128]{2,1,0:T(8,128)(2,1)}), bf16[8,176,128]{2,1,0:T(8,128)(2,1)S(1)}, u32[]{:S(2)}, u32[]{:S(2)}) %all-to-all-start.2) | async-done | bytes 360480 | tf_op jit(solution)/shard_map/all_to_all | solution.py:484
  153.1 0.7 copy-done.5
  153.9 8.9 %shard_map.167 = (bf16[8,8,4096]{2,1,0:T(8,128)(2,1)}, bf16[8,8,4096]{2,1,0:T(8,128)(2,1)}) custom-call(s32[3]{0:T(128)} %pad_add_fusion.place, bf16[8,176,128]{2,1,0:T(8,128)(2,1)} %copy-done.5, bf16[288,128]{1,0:T(8,128)(2,1)} %copy-done.1, bf16[2,128,128]{2,1,0:T(8,128)(2,1)} %get-tuple-element.12.asked, f32[128,128]{1,0:T(8,128)} %get-tuple-element.13.base, ...), custom_call_target="tpu_custom_call" | custom-call | flops 134217728 | bytes 1647628 | tf_op jit(solution)/shard_map/pallas_call | solution.py:26
  162.7 4.2 %collective-permute-start.6 = (bf16[8,8,4096]{2,1,0:T(8,128)(2,1)}, bf16[8,8,4096]{2,1,0:T(8,128)(2,1)S(1)}, u32[]{:S(2)}, u32[]{:S(2)}) collective-permute-start(bf16[8,8,4096]{2,1,0:T(8,128)(2,1)} %get-tuple-element.15), channel_id=1, source_target_pairs={{0,1},{1,0},{2,3},{3,2},{4,5},{5,4},{6,7},{7,6},{8,9},{9,8},{10,11... | collective-permute-start | bytes 1572872 | tf_op jit(solution)/shard_map/ppermute | solution.py:488
  166.9 1.7 collective-permute-done.6
  168.6 1.2 add_convert_fusion
  169.8 0.0 copy-start.2
  169.8 23.4 %all_to_all.20.parts = bf16[8,8,4096]{2,1,0:T(8,128)(2,1)S(1)} all-to-all(bf16[8,8,4096]{2,1,0:T(8,128)(2,1)S(1)} %add_convert_fusion), channel_id=1, replica_groups={{0,2,4,6,8,10,12,14},{1,3,5,7,9,11,13,15},{16,18,20,22,24,26,28,30},{17..., dimensions={0} | all-to-all | bytes 1048576 | tf_op jit(solution)/shard_map/all_to_all | solution.py:484
  193.2 0.0 copy-done.2
  193.2 0.7 shard_map.168
  (5 shorter events, 0.0 us)
Async XLA Ops:
  6.5 10.5 %collective-permute-start.1 = (bf16[1,8,4096]{2,1,0:T(8,128)(2,1)}, bf16[1,8,4096]{2,1,0:T(8,128)(2,1)S(1)}, u32[]{:S(2)}, u32[]{:S(2)}) collective-permute-start(bf16[1,8,4096]{2,1,0:T(8,128)(2,1)} %bitcast.14), channel_id=1, source_target_pairs={{0,8},{1,9},{2,10},{3,11},{4,12},{5,13},{6,14},{7,15},{8,0},{9,1},... | collective-permute-start | bytes 196616 | tf_op jit(solution)/shard_map/ppermute | solution.py:488
  17.9 53.1 %collective-permute-start.2 = (bf16[2,8,4096]{2,1,0:T(8,128)(2,1)S(1)}, bf16[2,8,4096]{2,1,0:T(8,128)(2,1)S(1)}, u32[]{:S(2)}, u32[]{:S(2)}) collective-permute-start(bf16[2,8,4096]{2,1,0:T(8,128)(2,1)S(1)} %pad_maximum_fusion.2), channel_id=1, source_target_pairs={{0,4},{1,5},{2,6},{3,7},{4,0},{5,1},{6,2},{7,3},{8,12},{9,13},{10,... | collective-permute-start | bytes 393224 | tf_op jit(solution)/shard_map/ppermute | solution.py:488
  26.4 44.6 %copy-start = (bf16[8,4096]{1,0:T(8,128)(2,1)S(1)}, bf16[8,4096]{1,0:T(8,128)(2,1)}, u32[]{:S(2)}) copy-start(bf16[8,4096]{1,0:T(8,128)(2,1)} %hidden.1) | copy-start | bytes 196612
  26.4 56.2 %all-to-all-start = ((bf16[16,4,8,128]{3,2,1,0:T(8,128)(2,1)}), bf16[16,4,8,128]{3,2,1,0:T(8,128)(2,1)S(1)}, u32[]{:S(2)}, u32[]{:S(2)}) async-start(bf16[16,4,8,128]{3,2,1,0:T(8,128)(2,1)} %shard_map.163), calls=%async_computation | async-start | bytes 262144 | tf_op jit(solution)/shard_map/all_to_all | solution.py:484
  70.9 73.5 %all-gather.3.cloned.1.call-start = ((), (), s32[]{:S(2)}) async-start(), calls=%async_computation.4 | async-start | bytes 1114112 | tf_op jit(solution)/shard_map/all_gather | solution.py:542
  71.0 16.6 %collective-permute-start.3 = (bf16[4,8,4096]{2,1,0:T(8,128)(2,1)S(1)}, bf16[4,8,4096]{2,1,0:T(8,128)(2,1)S(1)}, u32[]{:S(2)}, u32[]{:S(2)}) collective-permute-start(bf16[4,8,4096]{2,1,0:T(8,128)(2,1)S(1)} %pad_maximum_fusion.1), channel_id=1, source_target_pairs={{0,2},{1,3},{2,0},{3,1},{4,6},{5,7},{6,4},{7,5},{8,10},{9,11},{10,... | collective-permute-start | bytes 786440 | tf_op jit(solution)/shard_map/ppermute | solution.py:488
  83.4 14.2 %all-to-all-start.1 = ((bf16[8,19,8,128]{3,2,1,0:T(8,128)(2,1)}), bf16[8,19,8,128]{3,2,1,0:T(8,128)(2,1)S(1)}, u32[]{:S(2)}, u32[]{:S(2)}) async-start(bf16[8,19,8,128]{3,2,1,0:T(8,128)(2,1)} %shard_map.164), calls=%async_computation.1 | async-start | bytes 622592 | tf_op jit(solution)/shard_map/all_to_all | solution.py:484
  88.5 16.0 %collective-permute-start.4 = (bf16[8,8,4096]{2,1,0:T(8,128)(2,1)S(1)}, bf16[8,8,4096]{2,1,0:T(8,128)(2,1)S(1)}, u32[]{:S(2)}, u32[]{:S(2)}) collective-permute-start(bf16[8,8,4096]{2,1,0:T(8,128)(2,1)S(1)} %get-tuple-element.17), channel_id=1, source_target_pairs={{0,1},{1,0},{2,3},{3,2},{4,5},{5,4},{6,7},{7,6},{8,9},{9,8},{10,11... | collective-permute-start | bytes 1572872 | tf_op jit(solution)/shard_map/ppermute | solution.py:488
  97.6 8.9 %copy-start.6 = (bf16[8,19,8,128]{3,2,1,0:T(8,128)(2,1)}, bf16[8,19,8,128]{3,2,1,0:T(8,128)(2,1)S(1)}, u32[]{:S(2)}) copy-start(bf16[8,19,8,128]{3,2,1,0:T(8,128)(2,1)S(1)} %all-to-all-done.1.mine) | copy-start | bytes 933892
  97.6 8.1 %collective-permute-start = (bf16[8,19,8,128]{3,2,1,0:T(8,128)(2,1)S(1)}, bf16[8,19,8,128]{3,2,1,0:T(8,128)(2,1)S(1)}, u32[]{:S(2)}, u32[]{:S(2)}) collective-permute-start(bf16[8,19,8,128]{3,2,1,0:T(8,128)(2,1)S(1)} %all-to-all-done.1.mine), channel_id=1, source_target_pairs={{0,1},{1,0},{2,3},{3,2},{4,5},{5,4},{6,7},{7,6},{8,9},{9,8},{10,11... | collective-permute-start | bytes 933896 | tf_op jit(solution)/shard_map/ppermute | solution.py:488
  104.5 1.9 copy-start.7
  105.7 0.7 copy-start.8
  116.5 5.9 %copy-start.4 = (s32[3]{0:T(128)S(1)}, s32[3]{0:T(128)}, u32[]{:S(2)}) copy-start(s32[3]{0:T(128)} %pad_add_fusion.place) | copy-start | bytes 40
  116.5 5.9 %collective-permute-start.5 = (bf16[288,128]{1,0:T(8,128)(2,1)}, bf16[288,128]{1,0:T(8,128)(2,1)S(1)}, u32[]{:S(2)}, u32[]{:S(2)}) collective-permute-start(bf16[288,128]{1,0:T(8,128)(2,1)} %get-tuple-element.11.mine), channel_id=1, source_target_pairs={{0,16},{16,0},{32,48},{48,32},{64,80},{80,64},{96,112},{112,96},{1... | collective-permute-start | bytes 221192 | tf_op jit(solution)/shard_map/ppermute | solution.py:488
  122.4 0.9 copy-start.3
  123.2 1.5 copy-start.1
  124.7 28.4 %all-to-all-start.2 = ((bf16[8,176,128]{2,1,0:T(8,128)(2,1)}), bf16[8,176,128]{2,1,0:T(8,128)(2,1)S(1)}, u32[]{:S(2)}, u32[]{:S(2)}) async-start(bf16[8,176,128]{2,1,0:T(8,128)(2,1)} %shard_map.166), calls=%async_computation.2 | async-start | bytes 720896 | tf_op jit(solution)/shard_map/all_to_all | solution.py:484
  153.1 0.7 copy-start.5
  162.7 5.9 %collective-permute-start.6 = (bf16[8,8,4096]{2,1,0:T(8,128)(2,1)}, bf16[8,8,4096]{2,1,0:T(8,128)(2,1)S(1)}, u32[]{:S(2)}, u32[]{:S(2)}) collective-permute-start(bf16[8,8,4096]{2,1,0:T(8,128)(2,1)} %get-tuple-element.15), channel_id=1, source_target_pairs={{0,1},{1,0},{2,3},{3,2},{4,5},{5,4},{6,7},{7,6},{8,9},{9,8},{10,11... | collective-permute-start | bytes 1572872 | tf_op jit(solution)/shard_map/ppermute | solution.py:488
  169.8 23.4 %copy-start.2 = (f32[16,8,256]{2,1,0:T(8,128)S(1)}, f32[16,8,256]{2,1,0:T(8,128)}, u32[]{:S(2)}) copy-start(f32[16,8,256]{2,1,0:T(8,128)} %get-tuple-element.16.vectors) | copy-start | bytes 393220
Sparse Core Ops, SparseCore 0:
  73.8 70.5 all-gather.2

commit v5 on v4

--- a/solution.py
+++ b/solution.py
@@ -12,7 +12,7 @@
 EPS_KEY = 1e-06
 RATE_SHIFT = 5.0
 NEVER = -1e30
-SOME, ALL = 32 * 1024 * 1024, 63 * 1024 * 1024
+SOME, MOST, ALL, READ = 24 * 1024 * 1024, 52 * 1024 * 1024, 63 * 1024 * 1024, 52 * 1024 * 1024
 BF16, F32 = jnp.bfloat16, jnp.float32
 
 VMEM = pl.BlockSpec(memory_space=pltpu.VMEM)
@@ -130,18 +130,15 @@
     return jnp.where(core == 0, own, other), jnp.where(core == 0, other, own)
 
 
-def mask_of(n, count):
-    half = count // 2
-    bits = half.bit_length() - 1
-    inner = n % half
-    mask = sum(((inner >> b) & 1) << (bits - b) for b in range(bits))
-    return mask | (n // half)
+STEPS = (0, -2, 2, 4, -1, -3, 1, 3)
 
 
 def placed_rows(value, tp, held):
     count, rows, lanes = held.shape
     for n in range(count):
-        held[tp ^ mask_of(n, count)] = value[n * rows : (n + 1) * rows]
+        core = tp % 2 if n < len(STEPS) else 1 - tp % 2
+        chip = (tp // 2 + STEPS[n % len(STEPS)] + count // 2) % (count // 2)
+        held[2 * chip + core] = value[n * rows : (n + 1) * rows]
     return held[...].reshape(count * rows, lanes)
 
 
@@ -186,16 +183,16 @@
         down[(2 * s + 1) * lanes : (2 * s + 2) * lanes] = pltpu.roll(piece, HEAD, 1).astype(BF16)
 
 
-def inverse(mixing, row, col, upper):
-    size = mixing[0].shape[0]
+def inverse(mixing, row, col):
+    size = row.shape[0]
     eye = (row == col).astype(F32)
     width = 1
     found = None
     while width < size:
-        here, there = (col, row) if upper else (row, col)
         shared = (row // (2 * width)) == (col // (2 * width))
-        corner = shared & ((here // width) % 2 == 1) & ((there // width) % 2 == 0)
-        parts = [jnp.where(corner, m, 0.0) for m in mixing]
+        low_row, low_col = (row // width) % 2 == 1, (col // width) % 2 == 1
+        corner = {False: shared & low_row & ~low_col, True: shared & low_col & ~low_row}
+        parts = [jnp.where(corner[upper], m, 0.0) for m, upper in mixing]
         if found is None:
             found = [eye - p for p in parts]
         else:
@@ -279,11 +276,7 @@
     masks = {(d, h): pair(h, d == 1, True) for d, h in chains}
     mixing = {c: scores[n][:count, :count] * masks[c] for n, c in enumerate(chains)}
     seen = {c: dot(scores[n][:count, count:] * masks[c], v) for n, c in enumerate(chains)}
-    solved = {}
-    for d in range(2):
-        found = inverse([mixing[d, h] for h in range(heads)], row, col, d == 1)
-        for h in range(heads):
-            solved[d, h] = found[h]
+    solved = dict(zip(chains, inverse([(mixing[c], c[0] == 1) for c in chains], row, col)))
 
     whole = jnp.exp(end)
     starts = (
@@ -355,23 +348,29 @@
     modulated(place, near, far, context, mine, theirs, u, vectors, down)
     for copy in copies[1:]:
         copy.wait()
+    wq, wk, wv = (held.at[n] for n in range(3))
     count, extra = asked.shape[1], context.shape[0]
     low = dot(u[...], down[...])
     low = jnp.where(iota(low.shape, 1) < HEAD, low, 0.0)
-    k, v = dot(u[...], held[1]), dot(u[...], held[2])
+    k, v = dot(u[...], wk[...]), dot(u[...], wv[...])
     own = [
         placed_rows(part[:count], place[2], to).astype(BF16)
-        for part, to in ((low, moved_low), (k, moved_k), (v, moved_v), (dot(u[:count], held[0]), moved_q))
+        for part, to in ((low, moved_low), (k, moved_k), (v, moved_v), (dot(u[:count], wq[...]), moved_q))
     ]
     ahead, behind = block_terms(
         own[1], own[2], own[0][:, :HEAD], fading[...], step[...], rates[...], spikes[...], own[3]
     )
     same = same_head(ahead[0].shape)
     size = same.shape[0]
-    for n, (factor, offset) in enumerate((ahead[:2], behind[:2])):
-        sent[n * size : (n + 1) * size] = jnp.where(same, factor, pltpu.roll(offset, HEAD, 0)).astype(BF16)
+    packed = [
+        jnp.where(same, factor, pltpu.roll(offset, HEAD, 0)).astype(BF16)
+        for factor, offset in (ahead[:2], behind[:2])
+    ]
     tail = [part[count : count + extra] for part in (k, v, low)]
-    sent[2 * size :] = jnp.concatenate(tail + [jnp.zeros_like(tail[0])], axis=0).astype(BF16)
+    tail = jnp.concatenate(tail + [jnp.zeros_like(tail[0])], axis=0).astype(BF16)
+    for j in range(sent.shape[0]):
+        sent[j, :size] = jnp.where(place[0] < j, packed[0], packed[1])
+        sent[j, size:] = tail
     asked[0], asked[1] = ahead[2].astype(BF16), behind[2].astype(BF16)
     base[...] = ahead[3] + behind[3]
 
@@ -381,28 +380,8 @@
     return jnp.where(same, packed, 0.0), jnp.where(same, pltpu.roll(packed, HEAD, 0), 0.0)
 
 
-def pair_kernel(place, mine, other, out):
-    pairs, _, size = out.shape
-    odd = place[0] % 2
-    same = same_head((size, size))
-    early = jnp.where(odd == 0, mine[...].astype(F32), other[...].astype(F32))
-    late = jnp.where(odd == 0, other[...].astype(F32), mine[...].astype(F32))
-    both = []
-    for first, second, at in ((early, late, 0), (late, early, size)):
-        left, right = (opened(part[at : at + size], same) for part in (first, second))
-        new = dot(jnp.concatenate(left, axis=0), right[0])
-        both.append(jnp.where(same, new[:size], pltpu.roll(new[size:] + right[1], HEAD, 0)).astype(BF16))
-    extra = (early.shape[0] - 2 * size) // 4
-    tails = [[part[2 * size + n * extra : 2 * size + (n + 1) * extra] for part in (early, late)] for n in range(3)]
-    low = tails[2][0] + pltpu.roll(tails[2][1], HEAD, 1)
-    tail = jnp.concatenate(tails[0] + tails[1] + [low, jnp.zeros_like(low)], axis=0).astype(BF16)
-    for j in range(pairs):
-        out[j, :size] = jnp.where(place[0] // 2 < j, both[0], both[1])
-        out[j, size:] = tail
-
-
 def read_kernel(
-    place, maps, other, asked, base, fading_, step_, rates_, gains_, emit_,
+    place, maps, asked, base, fading_, step_, rates_, gains_, emit_,
     keep, give,
     fading, step, rates, gains, emit, sems,
 ):
@@ -410,38 +389,26 @@
     copies = [pltpu.make_async_copy(ref, to, sems.at[n]) for n, (ref, to) in enumerate(pairs)]
     for copy in copies:
         copy.start()
+    for copy in copies[:4]:
+        copy.wait()
     peers, _, size = maps.shape
     extra = keep.shape[1]
     same = same_head((size, size))
     me, core = place[0], place[1]
-    mine = me // 2
-    for copy in copies[:4]:
-        copy.wait()
-    wide = 2 * extra
     parts = [
-        jnp.concatenate([maps[j, size + n * wide : size + (n + 1) * wide].astype(F32) for j in range(peers)], axis=0)
-        for n in range(2)
+        jnp.concatenate([maps[j, size + n * extra : size + (n + 1) * extra].astype(F32) for j in range(peers)], axis=0)
+        for n in range(3)
     ]
-    low = []
-    for j in range(peers):
-        packed = maps[j, size + 2 * wide : size + 2 * wide + extra].astype(F32)
-        low += [packed, pltpu.roll(packed, HEAD, 1)]
-    parts = [part.astype(BF16) for part in (*parts, jnp.concatenate(low, axis=0))]
+    parts = [part.astype(BF16) for part in parts]
     context = block_terms(parts[0], parts[1], parts[2][:, :HEAD], fading[...], step[...], rates[...])
     eye = (iota((size, size), 0) == iota((size, size), 1)).astype(F32)
     composed = [jnp.concatenate([eye, jnp.zeros_like(eye)], axis=0) for _ in range(2)]
-
-    def follow(d, packed, reached):
-        factor, offset = opened(packed, same)
-        new = dot(composed[d], factor)
-        new = jnp.concatenate([new[:size], new[size:] + offset], axis=0)
-        composed[d] = jnp.where(reached, new, composed[d])
-
     for n in range(peers - 1):
-        follow(0, maps[n, :size], n < mine)
-        follow(1, maps[peers - 1 - n, :size], peers - 1 - n > mine)
-    follow(0, other[:size], me % 2 == 1)
-    follow(1, other[size : 2 * size], me % 2 == 0)
+        for d, j, reached in ((0, n, n < me), (1, peers - 1 - n, peers - 1 - n > me)):
+            factor, offset = opened(maps[j, :size], same)
+            new = dot(composed[d], factor)
+            new = jnp.concatenate([new[:size], new[size:] + offset], axis=0)
+            composed[d] = jnp.where(reached, new, composed[d])
     out = base[...]
     for d in range(2):
         start = jnp.where(same, context[d][1], 0.0)
@@ -542,11 +509,15 @@
     emit = lax.all_gather(emit_matrix, "sp", axis=0)
     parts = exchange(parts, "sp")
 
-    near, bit = hidden_items[None], n_tp // 2
-    while bit > 1:
-        far = swapped(near, "tp", bit)
-        near = jnp.concatenate([near, far], axis=0)
-        bit //= 2
+    def shifted(value, chips_on):
+        return lax.ppermute(value, "tp", [(i, (i + 2 * chips_on) % n_tp) for i in range(n_tp)])
+
+    below = shifted(hidden_items, 2)
+    above = shifted(hidden_items, -2)
+    across = shifted(hidden_items, 4)
+    odd_below = shifted(jnp.stack([hidden_items, below]), 1)
+    odd_above = shifted(jnp.stack([hidden_items, above]), -1)
+    near = jnp.concatenate([jnp.stack([hidden_items, below, above, across]), odd_below, odd_above], axis=0)
     far = swapped(near, "tp", 1)
 
     mine = call(sum_kernel, ((chips, n_sp + 3, 8, lanes), BF16), parts)
@@ -555,15 +526,10 @@
 
     padded = count + -(-extra // 16) * 16
     rates = feature_fading.reshape(1, lanes)
-    small = [
-        pltpu.VMEM(fading_raise_matrix.shape, BF16),
-        pltpu.VMEM(step_raise_matrix.shape, BF16),
-        pltpu.VMEM(rates.shape, F32),
-    ]
     sent, asked, base, vectors = call(
         block_kernel,
         [
-            ((2 * lanes + 4 * extra, lanes), BF16),
+            ((n_sp, lanes + 4 * extra, lanes), BF16),
             ((2, count, lanes), BF16),
             ((count, lanes), F32),
             ((n_tp, 8, chunk), F32),
@@ -583,12 +549,14 @@
         spike_logfade.T,
         scalars=1,
         fetched=8,
-        room=ALL,
+        room=MOST,
         flops=2 * padded * width * lanes * 4,
         scratch=[
             pltpu.VMEM((extra, width), BF16),
             pltpu.VMEM((3, width, lanes), BF16),
-            *small,
+            pltpu.VMEM(fading_raise_matrix.shape, BF16),
+            pltpu.VMEM(step_raise_matrix.shape, BF16),
+            pltpu.VMEM(rates.shape, F32),
             pltpu.VMEM(spike_logfade.shape[::-1], F32),
             pltpu.VMEM((padded, width), BF16),
             pltpu.VMEM((width, lanes), BF16),
@@ -596,23 +564,12 @@
             pltpu.SemaphoreType.DMA((8,)),
         ],
     )
-    other = swapped(sent, "sp", 1)
-    sent = call(
-        pair_kernel,
-        ((n_sp // 2, lanes + 6 * extra, lanes), BF16),
-        place,
-        sent,
-        other,
-        scalars=1,
-        flops=2 * 128**3 * 8,
-    )
-    maps = exchange(sent, "sp", [[2 * i + c for i in range(n_sp // 2)] for c in range(2)])
+    maps = exchange(sent, "sp")
     keep, give = call(
         read_kernel,
         [((chips, rows, width), BF16)] * 2,
         place,
         maps,
-        other,
         asked,
         base,
         fading_raise_matrix,
@@ -622,10 +579,12 @@
         emit,
         scalars=1,
         fetched=5,
-        room=ALL,
+        room=READ,
         flops=2 * count * lanes * width,
         scratch=[
-            *small,
+            pltpu.VMEM(fading_raise_matrix.shape, BF16),
+            pltpu.VMEM(step_raise_matrix.shape, BF16),
+            pltpu.VMEM(rates.shape, F32),
             pltpu.VMEM((1, lanes), F32),
             pltpu.VMEM((n_sp, *emit_matrix.shape), BF16),
             pltpu.SemaphoreType.DMA((5,)),

time: 202 us -> 236 us (1.17)
  waiting for transfers between devices: 43.8 us -> 79.8 us
  starting transfers between devices: 89.5 us -> 99.3 us
  Pallas kernels: 24.5 us -> 18.7 us
  other arithmetic: 3.58 us -> 0.71 us
    all_gather x1, waiting for transfers between devices: 14.4 us -> 67.3 us  [shards(): emit = lax.all_gather(emit_matrix, 'sp', axis=0)]
    ppermute x0 -> x5, starting transfers between devices: none -> 22.5 us  [shifted(): lax.ppermute(value, 'tp', [(i, (i + 2 * chips_on) % n_tp) for i in range(...]
    all_to_all x3, waiting for transfers between devices: 21.6 us -> 8.45 us  [exchange(): lax.all_to_all(blocks, axis, 0, 0, tiled=True, axis_index_groups=groups)]
    ppermute x7 -> x3, starting transfers between devices: 35.6 us -> 23.3 us  [swapped(): lax.ppermute(value, axis, [(i, i ^ bit) for i in range(lax.axis_size(axis...]
    pallas_call x6 -> x5, Pallas kernels: 24.5 us -> 18.7 us  [call(): pl.pallas_call(body, out_shape=shapes, in_specs=[SMEM] * scalars + [VMEM]...]
    ppermute x7 -> x3, waiting for transfers between devices: 7.78 us -> 2.71 us  [swapped(): lax.ppermute(value, axis, [(i, i ^ bit) for i in range(lax.axis_size(axis...]
  transfers between devices with their start and end apart: 11 -> 12, of which waited for: 8 -> 6; matrix products, arithmetic and copies ran while one was open for 1% -> 0% of each run, Pallas kernels for 7% -> 1%
where the time goes in v5:
time: 236 us; the launch traced here: 235 us
  starting transfers between devices  99.3 us (42%)
  waiting for transfers between devices  79.8 us (34%)
  blocking collectives  21.7 us (9%)
  Pallas kernels  18.7 us (8%)
  between operations  13.7 us (6%)
    all_gather x1, waiting for transfers between devices, shards(): emit = lax.all_gather(emit_matrix, 'sp', axis=0)  67.3 us
    all_to_all x3, starting transfers between devices, exchange(): lax.all_to_all(blocks, axis, 0, 0, tiled=True, axis_index_groups=groups)  53.4 us
    ppermute x3, starting transfers between devices, swapped(): lax.ppermute(value, axis, [(i, i ^ bit) for i in range(lax.axis_size(axis...  23.3 us
    ppermute x5, starting transfers between devices, shifted(): lax.ppermute(value, 'tp', [(i, (i + 2 * chips_on) % n_tp) for i in range(...  22.5 us
    all_to_all x1, blocking collectives, exchange(): lax.all_to_all(blocks, axis, 0, 0, tiled=True, axis_index_groups=groups)  21.7 us
    pallas_call x5, Pallas kernels, call(): pl.pallas_call(body, out_shape=shapes, in_specs=[SMEM] * scalars + [VMEM]...  18.7 us
    all_to_all x3, waiting for transfers between devices, exchange(): lax.all_to_all(blocks, axis, 0, 0, tiled=True, axis_index_groups=groups)  8.45 us
  transfers between devices with their start and end apart: 12, of which 6 were waited for; matrix products, arithmetic and copies ran while one was open for 0% of the time, Pallas kernels for 1%

profile of v5, /device:TPU:65, one launch (start us, length us, event | category | flops | bytes accessed | tf_op | source)
XLA Modules:
  0.0 235.2 jit_solution(193984232355154671)
XLA Ops:
  6.5 5.2 %collective-permute-start.1 = (bf16[8,4096]{1,0:T(8,128)(2,1)}, bf16[8,4096]{1,0:T(8,128)(2,1)S(1)}, u32[]{:S(2)}, u32[]{:S(2)}) collective-permute-start(bf16[8,4096]{1,0:T(8,128)(2,1)} %hidden.1), channel_id=1, source_target_pairs={{0,4},{1,5},{2,6},{3,7},{4,8},{5,9},{6,10},{7,11},{8,12},{9,13},{1... | collective-permute-start | bytes 196616 | tf_op jit(solution)/shard_map/ppermute | solution.py:513
  11.7 3.8 %collective-permute-start.2 = (bf16[8,4096]{1,0:T(8,128)(2,1)}, bf16[8,4096]{1,0:T(8,128)(2,1)S(1)}, u32[]{:S(2)}, u32[]{:S(2)}) collective-permute-start(bf16[8,4096]{1,0:T(8,128)(2,1)} %hidden.1), channel_id=1, source_target_pairs={{0,12},{1,13},{2,14},{3,15},{4,0},{5,1},{6,2},{7,3},{8,4},{9,5},{1... | collective-permute-start | bytes 196616 | tf_op jit(solution)/shard_map/ppermute | solution.py:513
  15.5 7.0 %collective-permute-start.3 = (bf16[8,4096]{1,0:T(8,128)(2,1)}, bf16[8,4096]{1,0:T(8,128)(2,1)S(1)}, u32[]{:S(2)}, u32[]{:S(2)}) collective-permute-start(bf16[8,4096]{1,0:T(8,128)(2,1)} %hidden.1), channel_id=1, source_target_pairs={{0,8},{1,9},{2,10},{3,11},{4,12},{5,13},{6,14},{7,15},{8,0},{9,1},... | collective-permute-start | bytes 196616 | tf_op jit(solution)/shard_map/ppermute | solution.py:513
  22.5 0.6 pad_add_fusion.place
  23.1 2.7 %shard_map.163 = bf16[16,4,8,128]{3,2,1,0:T(8,128)(2,1)} custom-call(s32[3]{0:T(128)} %pad_add_fusion.place, bf16[32,128]{1,0:T(8,128)(2,1)} %bitcast.31, bf16[32,128]{1,0:T(8,128)(2,1)} %bitcast.32, bf16[64,256]{1,0:T(8,128)(2,1)} %bitcast.30, bf16[256,256]{1,0:T(8,128)(2,1)} %shifting.1, bf16[256,256]{1,0:T(8,128)(2,1)} %stretch.1, bf16[256,256]{1,0:T(8,128)(2,1)} %valve.1), custom_call_target="tpu_custom_call" | custom-call | flops 3145728 | bytes 442380 | tf_op jit(solution)/shard_map/pallas_call | solution.py:26
  25.8 0.0 copy-start
  25.8 43.5 %all-to-all-start = ((bf16[16,4,8,128]{3,2,1,0:T(8,128)(2,1)}), bf16[16,4,8,128]{3,2,1,0:T(8,128)(2,1)S(1)}, u32[]{:S(2)}, u32[]{:S(2)}) async-start(bf16[16,4,8,128]{3,2,1,0:T(8,128)(2,1)} %shard_map.163), calls=%async_computation | async-start | bytes 262144 | tf_op jit(solution)/shard_map/all_to_all | solution.py:451
  69.3 0.0 copy-done
  69.4 0.0 collective-permute-done.1
  69.4 0.0 collective-permute-done.2
  69.4 2.4 %collective-permute-start.4 = (bf16[2,8,4096]{2,1,0:T(8,128)(2,1)S(1)}, bf16[2,8,4096]{2,1,0:T(8,128)(2,1)S(1)}, u32[]{:S(2)}, u32[]{:S(2)}) collective-permute-start(bf16[2,8,4096]{2,1,0:T(8,128)(2,1)S(1)} %get-tuple-element.18), channel_id=1, source_target_pairs={{0,2},{1,3},{2,4},{3,5},{4,6},{5,7},{6,8},{7,9},{8,10},{9,11},{10,... | collective-permute-start | bytes 393224 | tf_op jit(solution)/shard_map/ppermute | solution.py:513
  71.8 4.2 %collective-permute-start.5 = (bf16[2,8,4096]{2,1,0:T(8,128)(2,1)S(1)}, bf16[2,8,4096]{2,1,0:T(8,128)(2,1)S(1)}, u32[]{:S(2)}, u32[]{:S(2)}) collective-permute-start(bf16[2,8,4096]{2,1,0:T(8,128)(2,1)S(1)} %get-tuple-element.17), channel_id=1, source_target_pairs={{0,14},{1,15},{2,0},{3,1},{4,2},{5,3},{6,4},{7,5},{8,6},{9,7},{10,... | collective-permute-start | bytes 393224 | tf_op jit(solution)/shard_map/ppermute | solution.py:513
  76.0 0.0 collective-permute-done.3
  76.0 0.6 collective-permute-done.4
  76.7 4.5 %all-to-all-done.parts = bf16[16,4,8,128]{3,2,1,0:T(8,128)(2,1)S(1)} async-done(((bf16[16,4,8,128]{3,2,1,0:T(8,128)(2,1)}), bf16[16,4,8,128]{3,2,1,0:T(8,128)(2,1)S(1)}, u32[]{:S(2)}, u32[]{:S(2)}) %all-to-all-start) | async-done | bytes 131104 | tf_op jit(solution)/shard_map/all_to_all | solution.py:451
  81.1 0.8 shard_map.164
  81.9 3.6 %all-to-all-start.1 = ((bf16[8,19,8,128]{3,2,1,0:T(8,128)(2,1)}), bf16[8,19,8,128]{3,2,1,0:T(8,128)(2,1)S(1)}, u32[]{:S(2)}, u32[]{:S(2)}) async-start(bf16[8,19,8,128]{3,2,1,0:T(8,128)(2,1)} %shard_map.164), calls=%async_computation.1 | async-start | bytes 622592 | tf_op jit(solution)/shard_map/all_to_all | solution.py:451
  85.6 0.0 copy-start.1
  85.6 0.0 collective-permute-done.5
  85.6 0.0 copy-start.2
  85.6 0.0 copy-start.3
  85.6 0.0 copy-start.6
  85.6 5.6 %collective-permute-start.6 = (bf16[8,8,4096]{2,1,0:T(8,128)(2,1)S(1)}, bf16[8,8,4096]{2,1,0:T(8,128)(2,1)S(1)}, u32[]{:S(2)}, u32[]{:S(2)}) collective-permute-start(bf16[8,8,4096]{2,1,0:T(8,128)(2,1)S(1)} %constant_dynamic-update-slice_fusion), channel_id=1, source_target_pairs={{0,1},{1,0},{2,3},{3,2},{4,5},{5,4},{6,7},{7,6},{8,9},{9,8},{10,11... | collective-permute-start | bytes 1572872 | tf_op jit(solution)/shard_map/ppermute | solution.py:455
  91.3 4.0 %all-to-all-done.1.mine = bf16[8,19,8,128]{3,2,1,0:T(8,128)(2,1)S(1)} async-done(((bf16[8,19,8,128]{3,2,1,0:T(8,128)(2,1)}), bf16[8,19,8,128]{3,2,1,0:T(8,128)(2,1)S(1)}, u32[]{:S(2)}, u32[]{:S(2)}) %all-to-all-start.1) | async-done | bytes 311328 | tf_op jit(solution)/shard_map/all_to_all | solution.py:451
  95.3 6.6 %collective-permute-start = (bf16[8,19,8,128]{3,2,1,0:T(8,128)(2,1)S(1)}, bf16[8,19,8,128]{3,2,1,0:T(8,128)(2,1)S(1)}, u32[]{:S(2)}, u32[]{:S(2)}) collective-permute-start(bf16[8,19,8,128]{3,2,1,0:T(8,128)(2,1)S(1)} %all-to-all-done.1.mine), channel_id=1, source_target_pairs={{0,1},{1,0},{2,3},{3,2},{4,5},{5,4},{6,7},{7,6},{8,9},{9,8},{10,11... | collective-permute-start | bytes 933896 | tf_op jit(solution)/shard_map/ppermute | solution.py:455
  101.9 0.0 collective-permute-done.6
  101.9 0.0 copy-start.8
  101.9 1.2 collective-permute-done.theirs
  103.1 0.0 copy-done.8
  103.1 0.0 copy-done.1
  103.1 0.0 copy-done.2
  103.2 0.0 copy-done.3
  103.2 0.0 copy-done.6
  103.2 0.5 copy-done.4
  103.7 0.1 copy-done.5
  103.8 8.4 %shard_map.165 = (bf16[16,160,128]{2,1,0:T(8,128)(2,1)}, bf16[2,128,128]{2,1,0:T(8,128)(2,1)S(1)}, f32[128,128]{1,0:T(8,128)S(1)}, f32[16,8,256]{2,1,0:T(8,128)S(1)}) custom-call(s32[3]{0:T(128)S(1)} %copy-done.4, bf16[8,19,8,128]{3,2,1,0:T(8,128)(2,1)S(1)} %all-to-all-done.1.mine, bf16[8,19,8,128]{3,2,1,0:T(8,128)(2,1)S(1)} %collective-permute-done.theirs, ...), custom_call_target="tpu_custom_call" | custom-call | flops 603979776 | bytes 4916748 | tf_op jit(solution)/shard_map/pallas_call | solution.py:26
  112.1 6.2 %all-to-all-start.2 = ((bf16[16,160,128]{2,1,0:T(8,128)(2,1)}), bf16[16,160,128]{2,1,0:T(8,128)(2,1)S(1)}, u32[]{:S(2)}, u32[]{:S(2)}) async-start(bf16[16,160,128]{2,1,0:T(8,128)(2,1)} %get-tuple-element.11), calls=%async_computation.2 | async-start | bytes 1310720 | tf_op jit(solution)/shard_map/all_to_all | solution.py:451
  118.4 0.1 all-gather.3.cloned.1.call-start
  118.5 0.7 all-gather.3.cloned.1.call-update
  119.2 67.3 %all-gather.3.cloned.1.call-done = bf16[2048,256]{1,0:T(8,128)(2,1)} async-done(((bf16[128,256]{1,0:T(8,128)(2,1)}), bf16[2048,256]{1,0:T(8,128)(2,1)}) %all-gather.3.cloned.1.call-update) | async-done | bytes 1048592 | tf_op jit(solution)/shard_map/all_gather | solution.py:509
  186.5 0.0 all-to-all-done.2.maps
  186.5 0.7 copy-done.7
  187.2 6.1 %shard_map.166 = (bf16[8,8,4096]{2,1,0:T(8,128)(2,1)S(1)}, bf16[8,8,4096]{2,1,0:T(8,128)(2,1)S(1)}) custom-call(s32[3]{0:T(128)S(1)} %copy-done.4, bf16[16,160,128]{2,1,0:T(8,128)(2,1)S(1)} %all-to-all-done.2.maps, bf16[2,128,128]{2,1,0:T(8,128)(2,1)S(1)} %get-tuple-element.12.asked, f32[128,128]{1,0:T(8,128)S(1)} %get-tuple-element.13.base, ...), custom_call_target="tpu_custom_call" | custom-call | flops 134217728 | bytes 1868812 | tf_op jit(solution)/shard_map/pallas_call | solution.py:26
  193.3 11.0 %collective-permute-start.7 = (bf16[8,8,4096]{2,1,0:T(8,128)(2,1)S(1)}, bf16[8,8,4096]{2,1,0:T(8,128)(2,1)S(1)}, u32[]{:S(2)}, u32[]{:S(2)}) collective-permute-start(bf16[8,8,4096]{2,1,0:T(8,128)(2,1)S(1)} %get-tuple-element.15), channel_id=1, source_target_pairs={{0,1},{1,0},{2,3},{3,2},{4,5},{5,4},{6,7},{7,6},{8,9},{9,8},{10,11... | collective-permute-start | bytes 1572872 | tf_op jit(solution)/shard_map/ppermute | solution.py:455
  204.3 1.5 collective-permute-done.7
  205.9 0.1 add_convert_fusion
  206.0 21.7 %all_to_all.20.parts = bf16[8,8,4096]{2,1,0:T(8,128)(2,1)S(1)} all-to-all(bf16[8,8,4096]{2,1,0:T(8,128)(2,1)S(1)} %add_convert_fusion), channel_id=1, replica_groups={{0,2,4,6,8,10,12,14},{1,3,5,7,9,11,13,15},{16,18,20,22,24,26,28,30},{17..., dimensions={0} | all-to-all | bytes 1048576 | tf_op jit(solution)/shard_map/all_to_all | solution.py:451
  227.6 0.7 shard_map.167
  (10 shorter events, 0.1 us)
Async XLA Ops:
  6.5 62.8 %collective-permute-start.1 = (bf16[8,4096]{1,0:T(8,128)(2,1)}, bf16[8,4096]{1,0:T(8,128)(2,1)S(1)}, u32[]{:S(2)}, u32[]{:S(2)}) collective-permute-start(bf16[8,4096]{1,0:T(8,128)(2,1)} %hidden.1), channel_id=1, source_target_pairs={{0,4},{1,5},{2,6},{3,7},{4,8},{5,9},{6,10},{7,11},{8,12},{9,13},{1... | collective-permute-start | bytes 196616 | tf_op jit(solution)/shard_map/ppermute | solution.py:513
  11.7 57.7 %collective-permute-start.2 = (bf16[8,4096]{1,0:T(8,128)(2,1)}, bf16[8,4096]{1,0:T(8,128)(2,1)S(1)}, u32[]{:S(2)}, u32[]{:S(2)}) collective-permute-start(bf16[8,4096]{1,0:T(8,128)(2,1)} %hidden.1), channel_id=1, source_target_pairs={{0,12},{1,13},{2,14},{3,15},{4,0},{5,1},{6,2},{7,3},{8,4},{9,5},{1... | collective-permute-start | bytes 196616 | tf_op jit(solution)/shard_map/ppermute | solution.py:513
  15.5 60.5 %collective-permute-start.3 = (bf16[8,4096]{1,0:T(8,128)(2,1)}, bf16[8,4096]{1,0:T(8,128)(2,1)S(1)}, u32[]{:S(2)}, u32[]{:S(2)}) collective-permute-start(bf16[8,4096]{1,0:T(8,128)(2,1)} %hidden.1), channel_id=1, source_target_pairs={{0,8},{1,9},{2,10},{3,11},{4,12},{5,13},{6,14},{7,15},{8,0},{9,1},... | collective-permute-start | bytes 196616 | tf_op jit(solution)/shard_map/ppermute | solution.py:513
  25.8 43.6 %copy-start = (bf16[8,4096]{1,0:T(8,128)(2,1)S(1)}, bf16[8,4096]{1,0:T(8,128)(2,1)}, u32[]{:S(2)}) copy-start(bf16[8,4096]{1,0:T(8,128)(2,1)} %hidden.1) | copy-start | bytes 196612
  25.8 55.3 %all-to-all-start = ((bf16[16,4,8,128]{3,2,1,0:T(8,128)(2,1)}), bf16[16,4,8,128]{3,2,1,0:T(8,128)(2,1)S(1)}, u32[]{:S(2)}, u32[]{:S(2)}) async-start(bf16[16,4,8,128]{3,2,1,0:T(8,128)(2,1)} %shard_map.163), calls=%async_computation | async-start | bytes 262144 | tf_op jit(solution)/shard_map/all_to_all | solution.py:451
  69.4 7.2 %collective-permute-start.4 = (bf16[2,8,4096]{2,1,0:T(8,128)(2,1)S(1)}, bf16[2,8,4096]{2,1,0:T(8,128)(2,1)S(1)}, u32[]{:S(2)}, u32[]{:S(2)}) collective-permute-start(bf16[2,8,4096]{2,1,0:T(8,128)(2,1)S(1)} %get-tuple-element.18), channel_id=1, source_target_pairs={{0,2},{1,3},{2,4},{3,5},{4,6},{5,7},{6,8},{7,9},{8,10},{9,11},{10,... | collective-permute-start | bytes 393224 | tf_op jit(solution)/shard_map/ppermute | solution.py:513
  71.8 13.8 %collective-permute-start.5 = (bf16[2,8,4096]{2,1,0:T(8,128)(2,1)S(1)}, bf16[2,8,4096]{2,1,0:T(8,128)(2,1)S(1)}, u32[]{:S(2)}, u32[]{:S(2)}) collective-permute-start(bf16[2,8,4096]{2,1,0:T(8,128)(2,1)S(1)} %get-tuple-element.17), channel_id=1, source_target_pairs={{0,14},{1,15},{2,0},{3,1},{4,2},{5,3},{6,4},{7,5},{8,6},{9,7},{10,... | collective-permute-start | bytes 393224 | tf_op jit(solution)/shard_map/ppermute | solution.py:513
  81.9 13.4 %all-to-all-start.1 = ((bf16[8,19,8,128]{3,2,1,0:T(8,128)(2,1)}), bf16[8,19,8,128]{3,2,1,0:T(8,128)(2,1)S(1)}, u32[]{:S(2)}, u32[]{:S(2)}) async-start(bf16[8,19,8,128]{3,2,1,0:T(8,128)(2,1)} %shard_map.164), calls=%async_computation.1 | async-start | bytes 622592 | tf_op jit(solution)/shard_map/all_to_all | solution.py:451
  85.6 17.6 %copy-start.1 = (bf16[8,4096]{1,0:T(8,128)(2,1)S(1)}, bf16[8,4096]{1,0:T(8,128)(2,1)}, u32[]{:S(2)}) copy-start(bf16[8,4096]{1,0:T(8,128)(2,1)} %context_.1) | copy-start | bytes 196612
  85.6 17.6 %copy-start.2 = (bf16[64,128]{1,0:T(8,128)(2,1)S(1)}, bf16[64,128]{1,0:T(8,128)(2,1)}, u32[]{:S(2)}) copy-start(bf16[64,128]{1,0:T(8,128)(2,1)} %fading_.3) | copy-start | bytes 49156
  85.6 17.6 %copy-start.3 = (bf16[64,128]{1,0:T(8,128)(2,1)S(1)}, bf16[64,128]{1,0:T(8,128)(2,1)}, u32[]{:S(2)}) copy-start(bf16[64,128]{1,0:T(8,128)(2,1)} %step_.3) | copy-start | bytes 49156
  85.6 17.6 %copy-start.6 = (f32[128,2]{0,1:T(2,128)S(1)}, f32[128,2]{0,1:T(2,128)}, u32[]{:S(2)}) copy-start(f32[128,2]{0,1:T(2,128)} %param.31) | copy-start | bytes 3076
  85.6 16.3 %collective-permute-start.6 = (bf16[8,8,4096]{2,1,0:T(8,128)(2,1)S(1)}, bf16[8,8,4096]{2,1,0:T(8,128)(2,1)S(1)}, u32[]{:S(2)}, u32[]{:S(2)}) collective-permute-start(bf16[8,8,4096]{2,1,0:T(8,128)(2,1)S(1)} %constant_dynamic-update-slice_fusion), channel_id=1, source_target_pairs={{0,1},{1,0},{2,3},{3,2},{4,5},{5,4},{6,7},{7,6},{8,9},{9,8},{10,11... | collective-permute-start | bytes 1572872 | tf_op jit(solution)/shard_map/ppermute | solution.py:455
  95.3 7.9 %collective-permute-start = (bf16[8,19,8,128]{3,2,1,0:T(8,128)(2,1)S(1)}, bf16[8,19,8,128]{3,2,1,0:T(8,128)(2,1)S(1)}, u32[]{:S(2)}, u32[]{:S(2)}) collective-permute-start(bf16[8,19,8,128]{3,2,1,0:T(8,128)(2,1)S(1)} %all-to-all-done.1.mine), channel_id=1, source_target_pairs={{0,1},{1,0},{2,3},{3,2},{4,5},{5,4},{6,7},{7,6},{8,9},{9,8},{10,11... | collective-permute-start | bytes 933896 | tf_op jit(solution)/shard_map/ppermute | solution.py:455
  101.9 1.2 copy-start.8
  103.1 0.6 copy-start.4
  103.1 0.7 copy-start.5
  112.1 74.4 %all-to-all-start.2 = ((bf16[16,160,128]{2,1,0:T(8,128)(2,1)}), bf16[16,160,128]{2,1,0:T(8,128)(2,1)S(1)}, u32[]{:S(2)}, u32[]{:S(2)}) async-start(bf16[16,160,128]{2,1,0:T(8,128)(2,1)} %get-tuple-element.11), calls=%async_computation.2 | async-start | bytes 1310720 | tf_op jit(solution)/shard_map/all_to_all | solution.py:451
  118.4 68.1 %all-gather.3.cloned.1.call-start = ((), (), s32[]{:S(2)}) async-start(), calls=%async_computation.4 | async-start | bytes 1114112 | tf_op jit(solution)/shard_map/all_gather | solution.py:509
  186.5 0.7 copy-start.7
  193.3 12.5 %collective-permute-start.7 = (bf16[8,8,4096]{2,1,0:T(8,128)(2,1)S(1)}, bf16[8,8,4096]{2,1,0:T(8,128)(2,1)S(1)}, u32[]{:S(2)}, u32[]{:S(2)}) collective-permute-start(bf16[8,8,4096]{2,1,0:T(8,128)(2,1)S(1)} %get-tuple-element.15), channel_id=1, source_target_pairs={{0,1},{1,0},{2,3},{3,2},{4,5},{5,4},{6,7},{7,6},{8,9},{9,8},{10,11... | collective-permute-start | bytes 1572872 | tf_op jit(solution)/shard_map/ppermute | solution.py:455
Sparse Core Ops, SparseCore 0:
  121.3 65.1 all-gather.2

commit v6 on v5

--- a/solution.py
+++ b/solution.py
@@ -336,26 +336,26 @@
 def block_kernel(
     place, mine, theirs, near, far, context_, wq, wk, wv, fading_, step_, rates_, spikes_,
     sent, asked, base, vectors,
-    context, held, fading, step, rates, spikes, u, down, moved_q, moved_k, moved_v, moved_low, sems,
+    context, held, fading, step, rates, spikes, u, moved_q, moved_k, moved_v, moved_low, sems,
 ):
+    lanes = wq.shape[1]
     pairs = [(context_, context)]
-    pairs += [(ref, held.at[n]) for n, ref in enumerate((wq, wk, wv))]
+    pairs += [(ref, held.at[n // 2, :, pl.ds(n % 2 * lanes, lanes)]) for n, ref in enumerate((wq, wk, wv))]
     pairs += [(fading_, fading), (step_, step), (rates_, rates), (spikes_, spikes)]
     copies = [pltpu.make_async_copy(ref, to, sems.at[n]) for n, (ref, to) in enumerate(pairs)]
     for copy in copies:
         copy.start()
     copies[0].wait()
-    modulated(place, near, far, context, mine, theirs, u, vectors, down)
+    modulated(place, near, far, context, mine, theirs, u, vectors, held.at[1, :, pl.ds(lanes, lanes)])
     for copy in copies[1:]:
         copy.wait()
-    wq, wk, wv = (held.at[n] for n in range(3))
     count, extra = asked.shape[1], context.shape[0]
-    low = dot(u[...], down[...])
+    first, second = dot(u[...], held[0]), dot(u[...], held[1])
+    q, k, v, low = first[:, :lanes], first[:, lanes:], second[:, :lanes], second[:, lanes:]
     low = jnp.where(iota(low.shape, 1) < HEAD, low, 0.0)
-    k, v = dot(u[...], wk[...]), dot(u[...], wv[...])
     own = [
         placed_rows(part[:count], place[2], to).astype(BF16)
-        for part, to in ((low, moved_low), (k, moved_k), (v, moved_v), (dot(u[:count], wq[...]), moved_q))
+        for part, to in ((low, moved_low), (k, moved_k), (v, moved_v), (q, moved_q))
     ]
     ahead, behind = block_terms(
         own[1], own[2], own[0][:, :HEAD], fading[...], step[...], rates[...], spikes[...], own[3]
@@ -366,11 +366,11 @@
         jnp.where(same, factor, pltpu.roll(offset, HEAD, 0)).astype(BF16)
         for factor, offset in (ahead[:2], behind[:2])
     ]
-    tail = [part[count : count + extra] for part in (k, v, low)]
-    tail = jnp.concatenate(tail + [jnp.zeros_like(tail[0])], axis=0).astype(BF16)
+    tail = [part[count : count + extra].astype(BF16) for part in (k, v, low)]
     for j in range(sent.shape[0]):
         sent[j, :size] = jnp.where(place[0] < j, packed[0], packed[1])
-        sent[j, size:] = tail
+        for n, part in enumerate(tail):
+            sent[j, size + n * extra : size + (n + 1) * extra] = part
     asked[0], asked[1] = ahead[2].astype(BF16), behind[2].astype(BF16)
     base[...] = ahead[3] + behind[3]
 
@@ -529,7 +529,7 @@
     sent, asked, base, vectors = call(
         block_kernel,
         [
-            ((n_sp, lanes + 4 * extra, lanes), BF16),
+            ((n_sp, lanes + 3 * extra, lanes), BF16),
             ((2, count, lanes), BF16),
             ((count, lanes), F32),
             ((n_tp, 8, chunk), F32),
@@ -553,13 +553,12 @@
         flops=2 * padded * width * lanes * 4,
         scratch=[
             pltpu.VMEM((extra, width), BF16),
-            pltpu.VMEM((3, width, lanes), BF16),
+            pltpu.VMEM((2, width, 2 * lanes), BF16),
             pltpu.VMEM(fading_raise_matrix.shape, BF16),
             pltpu.VMEM(step_raise_matrix.shape, BF16),
             pltpu.VMEM(rates.shape, F32),
             pltpu.VMEM(spike_logfade.shape[::-1], F32),
             pltpu.VMEM((padded, width), BF16),
-            pltpu.VMEM((width, lanes), BF16),
             *[pltpu.VMEM((n_tp, rows, lanes), F32)] * 4,
             pltpu.SemaphoreType.DMA((8,)),
         ],

time: 236 us -> 235 us (level)
  no operation moved by 1% of the time
where the time goes in v6:
time: 235 us; the launch traced here: 234 us
  starting transfers between devices  99.6 us (42%)
  waiting for transfers between devices  78.8 us (34%)
  blocking collectives  21 us (9%)
  Pallas kernels  18.3 us (8%)
  between operations  13.7 us (6%)
    all_gather x1, waiting for transfers between devices, shards(): emit = lax.all_gather(emit_matrix, 'sp', axis=0)  66.3 us
    all_to_all x3, starting transfers between devices, exchange(): lax.all_to_all(blocks, axis, 0, 0, tiled=True, axis_index_groups=groups)  53.4 us
    ppermute x3, starting transfers between devices, swapped(): lax.ppermute(value, axis, [(i, i ^ bit) for i in range(lax.axis_size(axis...  23.7 us
    ppermute x5, starting transfers between devices, shifted(): lax.ppermute(value, 'tp', [(i, (i + 2 * chips_on) % n_tp) for i in range(...  22.5 us
    all_to_all x1, blocking collectives, exchange(): lax.all_to_all(blocks, axis, 0, 0, tiled=True, axis_index_groups=groups)  21 us
    pallas_call x5, Pallas kernels, call(): pl.pallas_call(body, out_shape=shapes, in_specs=[SMEM] * scalars + [VMEM]...  18.3 us
    all_to_all x3, waiting for transfers between devices, exchange(): lax.all_to_all(blocks, axis, 0, 0, tiled=True, axis_index_groups=groups)  8.45 us
  transfers between devices with their start and end apart: 12, of which 6 were waited for; matrix products, arithmetic and copies ran while one was open for 0% of the time, Pallas kernels for 1%

profile of v6, /device:TPU:65, one launch (start us, length us, event | category | flops | bytes accessed | tf_op | source)
XLA Modules:
  0.0 233.5 jit_solution(12633377808154427196)
XLA Ops:
  6.5 5.2 %collective-permute-start.1 = (bf16[8,4096]{1,0:T(8,128)(2,1)}, bf16[8,4096]{1,0:T(8,128)(2,1)S(1)}, u32[]{:S(2)}, u32[]{:S(2)}) collective-permute-start(bf16[8,4096]{1,0:T(8,128)(2,1)} %hidden.1), channel_id=1, source_target_pairs={{0,4},{1,5},{2,6},{3,7},{4,8},{5,9},{6,10},{7,11},{8,12},{9,13},{1... | collective-permute-start | bytes 196616 | tf_op jit(solution)/shard_map/ppermute | solution.py:513
  11.7 3.8 %collective-permute-start.2 = (bf16[8,4096]{1,0:T(8,128)(2,1)}, bf16[8,4096]{1,0:T(8,128)(2,1)S(1)}, u32[]{:S(2)}, u32[]{:S(2)}) collective-permute-start(bf16[8,4096]{1,0:T(8,128)(2,1)} %hidden.1), channel_id=1, source_target_pairs={{0,12},{1,13},{2,14},{3,15},{4,0},{5,1},{6,2},{7,3},{8,4},{9,5},{1... | collective-permute-start | bytes 196616 | tf_op jit(solution)/shard_map/ppermute | solution.py:513
  15.5 7.0 %collective-permute-start.3 = (bf16[8,4096]{1,0:T(8,128)(2,1)}, bf16[8,4096]{1,0:T(8,128)(2,1)S(1)}, u32[]{:S(2)}, u32[]{:S(2)}) collective-permute-start(bf16[8,4096]{1,0:T(8,128)(2,1)} %hidden.1), channel_id=1, source_target_pairs={{0,8},{1,9},{2,10},{3,11},{4,12},{5,13},{6,14},{7,15},{8,0},{9,1},... | collective-permute-start | bytes 196616 | tf_op jit(solution)/shard_map/ppermute | solution.py:513
  22.5 0.6 pad_add_fusion.place
  23.1 2.7 %shard_map.163 = bf16[16,4,8,128]{3,2,1,0:T(8,128)(2,1)} custom-call(s32[3]{0:T(128)} %pad_add_fusion.place, bf16[32,128]{1,0:T(8,128)(2,1)} %bitcast.31, bf16[32,128]{1,0:T(8,128)(2,1)} %bitcast.32, bf16[64,256]{1,0:T(8,128)(2,1)} %bitcast.30, bf16[256,256]{1,0:T(8,128)(2,1)} %shifting.1, bf16[256,256]{1,0:T(8,128)(2,1)} %stretch.1, bf16[256,256]{1,0:T(8,128)(2,1)} %valve.1), custom_call_target="tpu_custom_call" | custom-call | flops 3145728 | bytes 442380 | tf_op jit(solution)/shard_map/pallas_call | solution.py:26
  25.8 0.0 copy-start
  25.8 43.5 %all-to-all-start = ((bf16[16,4,8,128]{3,2,1,0:T(8,128)(2,1)}), bf16[16,4,8,128]{3,2,1,0:T(8,128)(2,1)S(1)}, u32[]{:S(2)}, u32[]{:S(2)}) async-start(bf16[16,4,8,128]{3,2,1,0:T(8,128)(2,1)} %shard_map.163), calls=%async_computation | async-start | bytes 262144 | tf_op jit(solution)/shard_map/all_to_all | solution.py:451
  69.3 0.0 copy-done
  69.4 0.0 collective-permute-done.1
  69.4 0.0 collective-permute-done.2
  69.4 2.4 %collective-permute-start.4 = (bf16[2,8,4096]{2,1,0:T(8,128)(2,1)S(1)}, bf16[2,8,4096]{2,1,0:T(8,128)(2,1)S(1)}, u32[]{:S(2)}, u32[]{:S(2)}) collective-permute-start(bf16[2,8,4096]{2,1,0:T(8,128)(2,1)S(1)} %get-tuple-element.18), channel_id=1, source_target_pairs={{0,2},{1,3},{2,4},{3,5},{4,6},{5,7},{6,8},{7,9},{8,10},{9,11},{10,... | collective-permute-start | bytes 393224 | tf_op jit(solution)/shard_map/ppermute | solution.py:513
  71.8 4.2 %collective-permute-start.5 = (bf16[2,8,4096]{2,1,0:T(8,128)(2,1)S(1)}, bf16[2,8,4096]{2,1,0:T(8,128)(2,1)S(1)}, u32[]{:S(2)}, u32[]{:S(2)}) collective-permute-start(bf16[2,8,4096]{2,1,0:T(8,128)(2,1)S(1)} %get-tuple-element.17), channel_id=1, source_target_pairs={{0,14},{1,15},{2,0},{3,1},{4,2},{5,3},{6,4},{7,5},{8,6},{9,7},{10,... | collective-permute-start | bytes 393224 | tf_op jit(solution)/shard_map/ppermute | solution.py:513
  76.0 0.0 collective-permute-done.3
  76.0 0.6 collective-permute-done.4
  76.7 4.5 %all-to-all-done.parts = bf16[16,4,8,128]{3,2,1,0:T(8,128)(2,1)S(1)} async-done(((bf16[16,4,8,128]{3,2,1,0:T(8,128)(2,1)}), bf16[16,4,8,128]{3,2,1,0:T(8,128)(2,1)S(1)}, u32[]{:S(2)}, u32[]{:S(2)}) %all-to-all-start) | async-done | bytes 131104 | tf_op jit(solution)/shard_map/all_to_all | solution.py:451
  81.1 0.8 shard_map.164
  81.9 3.6 %all-to-all-start.1 = ((bf16[8,19,8,128]{3,2,1,0:T(8,128)(2,1)}), bf16[8,19,8,128]{3,2,1,0:T(8,128)(2,1)S(1)}, u32[]{:S(2)}, u32[]{:S(2)}) async-start(bf16[8,19,8,128]{3,2,1,0:T(8,128)(2,1)} %shard_map.164), calls=%async_computation.1 | async-start | bytes 622592 | tf_op jit(solution)/shard_map/all_to_all | solution.py:451
  85.6 0.0 copy-start.1
  85.6 0.0 collective-permute-done.5
  85.6 0.0 copy-start.2
  85.6 0.0 copy-start.3
  85.6 0.0 copy-start.6
  85.6 5.6 %collective-permute-start.6 = (bf16[8,8,4096]{2,1,0:T(8,128)(2,1)S(1)}, bf16[8,8,4096]{2,1,0:T(8,128)(2,1)S(1)}, u32[]{:S(2)}, u32[]{:S(2)}) collective-permute-start(bf16[8,8,4096]{2,1,0:T(8,128)(2,1)S(1)} %constant_dynamic-update-slice_fusion), channel_id=1, source_target_pairs={{0,1},{1,0},{2,3},{3,2},{4,5},{5,4},{6,7},{7,6},{8,9},{9,8},{10,11... | collective-permute-start | bytes 1572872 | tf_op jit(solution)/shard_map/ppermute | solution.py:455
  91.3 4.0 %all-to-all-done.1.mine = bf16[8,19,8,128]{3,2,1,0:T(8,128)(2,1)S(1)} async-done(((bf16[8,19,8,128]{3,2,1,0:T(8,128)(2,1)}), bf16[8,19,8,128]{3,2,1,0:T(8,128)(2,1)S(1)}, u32[]{:S(2)}, u32[]{:S(2)}) %all-to-all-start.1) | async-done | bytes 311328 | tf_op jit(solution)/shard_map/all_to_all | solution.py:451
  95.3 6.6 %collective-permute-start = (bf16[8,19,8,128]{3,2,1,0:T(8,128)(2,1)S(1)}, bf16[8,19,8,128]{3,2,1,0:T(8,128)(2,1)S(1)}, u32[]{:S(2)}, u32[]{:S(2)}) collective-permute-start(bf16[8,19,8,128]{3,2,1,0:T(8,128)(2,1)S(1)} %all-to-all-done.1.mine), channel_id=1, source_target_pairs={{0,1},{1,0},{2,3},{3,2},{4,5},{5,4},{6,7},{7,6},{8,9},{9,8},{10,11... | collective-permute-start | bytes 933896 | tf_op jit(solution)/shard_map/ppermute | solution.py:455
  101.9 0.0 collective-permute-done.6
  101.9 0.0 copy-start.8
  101.9 1.2 collective-permute-done.theirs
  103.1 0.0 copy-done.8
  103.1 0.0 copy-done.1
  103.1 0.0 copy-done.2
  103.2 0.0 copy-done.3
  103.2 0.0 copy-done.6
  103.2 0.5 copy-done.4
  103.7 0.1 copy-done.5
  103.8 7.9 %shard_map.165 = (bf16[16,152,128]{2,1,0:T(8,128)(2,1)}, bf16[2,128,128]{2,1,0:T(8,128)(2,1)S(1)}, f32[128,128]{1,0:T(8,128)S(1)}, f32[16,8,256]{2,1,0:T(8,128)S(1)}) custom-call(s32[3]{0:T(128)S(1)} %copy-done.4, bf16[8,19,8,128]{3,2,1,0:T(8,128)(2,1)S(1)} %all-to-all-done.1.mine, bf16[8,19,8,128]{3,2,1,0:T(8,128)(2,1)S(1)} %collective-permute-done.theirs, ...), custom_call_target="tpu_custom_call" | custom-call | flops 603979776 | bytes 4916748 | tf_op jit(solution)/shard_map/pallas_call | solution.py:26
  111.7 6.2 %all-to-all-start.2 = ((bf16[16,152,128]{2,1,0:T(8,128)(2,1)}), bf16[16,152,128]{2,1,0:T(8,128)(2,1)S(1)}, u32[]{:S(2)}, u32[]{:S(2)}) async-start(bf16[16,152,128]{2,1,0:T(8,128)(2,1)} %get-tuple-element.11), calls=%async_computation.2 | async-start | bytes 1245184 | tf_op jit(solution)/shard_map/all_to_all | solution.py:451
  118.0 0.1 all-gather.3.cloned.1.call-start
  118.0 0.7 all-gather.3.cloned.1.call-update
  118.8 66.3 %all-gather.3.cloned.1.call-done = bf16[2048,256]{1,0:T(8,128)(2,1)} async-done(((bf16[128,256]{1,0:T(8,128)(2,1)}), bf16[2048,256]{1,0:T(8,128)(2,1)}) %all-gather.3.cloned.1.call-update) | async-done | bytes 1048592 | tf_op jit(solution)/shard_map/all_gather | solution.py:509
  185.1 0.0 all-to-all-done.2.maps
  185.1 0.7 copy-done.7
  185.7 6.2 %shard_map.166 = (bf16[8,8,4096]{2,1,0:T(8,128)(2,1)S(1)}, bf16[8,8,4096]{2,1,0:T(8,128)(2,1)S(1)}) custom-call(s32[3]{0:T(128)S(1)} %copy-done.4, bf16[16,152,128]{2,1,0:T(8,128)(2,1)S(1)} %all-to-all-done.2.maps, bf16[2,128,128]{2,1,0:T(8,128)(2,1)S(1)} %get-tuple-element.12.asked, f32[128,128]{1,0:T(8,128)S(1)} %get-tuple-element.13.base, ...), custom_call_target="tpu_custom_call" | custom-call | flops 134217728 | bytes 1836044 | tf_op jit(solution)/shard_map/pallas_call | solution.py:26
  191.9 11.4 %collective-permute-start.7 = (bf16[8,8,4096]{2,1,0:T(8,128)(2,1)S(1)}, bf16[8,8,4096]{2,1,0:T(8,128)(2,1)S(1)}, u32[]{:S(2)}, u32[]{:S(2)}) collective-permute-start(bf16[8,8,4096]{2,1,0:T(8,128)(2,1)S(1)} %get-tuple-element.15), channel_id=1, source_target_pairs={{0,1},{1,0},{2,3},{3,2},{4,5},{5,4},{6,7},{7,6},{8,9},{9,8},{10,11... | collective-permute-start | bytes 1572872 | tf_op jit(solution)/shard_map/ppermute | solution.py:455
  203.3 1.5 collective-permute-done.7
  204.8 0.1 add_convert_fusion
  204.9 21.0 %all_to_all.20.parts = bf16[8,8,4096]{2,1,0:T(8,128)(2,1)S(1)} all-to-all(bf16[8,8,4096]{2,1,0:T(8,128)(2,1)S(1)} %add_convert_fusion), channel_id=1, replica_groups={{0,2,4,6,8,10,12,14},{1,3,5,7,9,11,13,15},{16,18,20,22,24,26,28,30},{17..., dimensions={0} | all-to-all | bytes 1048576 | tf_op jit(solution)/shard_map/all_to_all | solution.py:451
  225.9 0.7 shard_map.167
  (10 shorter events, 0.1 us)
Async XLA Ops:
  6.5 62.8 %collective-permute-start.1 = (bf16[8,4096]{1,0:T(8,128)(2,1)}, bf16[8,4096]{1,0:T(8,128)(2,1)S(1)}, u32[]{:S(2)}, u32[]{:S(2)}) collective-permute-start(bf16[8,4096]{1,0:T(8,128)(2,1)} %hidden.1), channel_id=1, source_target_pairs={{0,4},{1,5},{2,6},{3,7},{4,8},{5,9},{6,10},{7,11},{8,12},{9,13},{1... | collective-permute-start | bytes 196616 | tf_op jit(solution)/shard_map/ppermute | solution.py:513
  11.7 57.7 %collective-permute-start.2 = (bf16[8,4096]{1,0:T(8,128)(2,1)}, bf16[8,4096]{1,0:T(8,128)(2,1)S(1)}, u32[]{:S(2)}, u32[]{:S(2)}) collective-permute-start(bf16[8,4096]{1,0:T(8,128)(2,1)} %hidden.1), channel_id=1, source_target_pairs={{0,12},{1,13},{2,14},{3,15},{4,0},{5,1},{6,2},{7,3},{8,4},{9,5},{1... | collective-permute-start | bytes 196616 | tf_op jit(solution)/shard_map/ppermute | solution.py:513
  15.5 60.5 %collective-permute-start.3 = (bf16[8,4096]{1,0:T(8,128)(2,1)}, bf16[8,4096]{1,0:T(8,128)(2,1)S(1)}, u32[]{:S(2)}, u32[]{:S(2)}) collective-permute-start(bf16[8,4096]{1,0:T(8,128)(2,1)} %hidden.1), channel_id=1, source_target_pairs={{0,8},{1,9},{2,10},{3,11},{4,12},{5,13},{6,14},{7,15},{8,0},{9,1},... | collective-permute-start | bytes 196616 | tf_op jit(solution)/shard_map/ppermute | solution.py:513
  25.8 43.6 %copy-start = (bf16[8,4096]{1,0:T(8,128)(2,1)S(1)}, bf16[8,4096]{1,0:T(8,128)(2,1)}, u32[]{:S(2)}) copy-start(bf16[8,4096]{1,0:T(8,128)(2,1)} %hidden.1) | copy-start | bytes 196612
  25.8 55.3 %all-to-all-start = ((bf16[16,4,8,128]{3,2,1,0:T(8,128)(2,1)}), bf16[16,4,8,128]{3,2,1,0:T(8,128)(2,1)S(1)}, u32[]{:S(2)}, u32[]{:S(2)}) async-start(bf16[16,4,8,128]{3,2,1,0:T(8,128)(2,1)} %shard_map.163), calls=%async_computation | async-start | bytes 262144 | tf_op jit(solution)/shard_map/all_to_all | solution.py:451
  69.4 7.2 %collective-permute-start.4 = (bf16[2,8,4096]{2,1,0:T(8,128)(2,1)S(1)}, bf16[2,8,4096]{2,1,0:T(8,128)(2,1)S(1)}, u32[]{:S(2)}, u32[]{:S(2)}) collective-permute-start(bf16[2,8,4096]{2,1,0:T(8,128)(2,1)S(1)} %get-tuple-element.18), channel_id=1, source_target_pairs={{0,2},{1,3},{2,4},{3,5},{4,6},{5,7},{6,8},{7,9},{8,10},{9,11},{10,... | collective-permute-start | bytes 393224 | tf_op jit(solution)/shard_map/ppermute | solution.py:513
  71.8 13.8 %collective-permute-start.5 = (bf16[2,8,4096]{2,1,0:T(8,128)(2,1)S(1)}, bf16[2,8,4096]{2,1,0:T(8,128)(2,1)S(1)}, u32[]{:S(2)}, u32[]{:S(2)}) collective-permute-start(bf16[2,8,4096]{2,1,0:T(8,128)(2,1)S(1)} %get-tuple-element.17), channel_id=1, source_target_pairs={{0,14},{1,15},{2,0},{3,1},{4,2},{5,3},{6,4},{7,5},{8,6},{9,7},{10,... | collective-permute-start | bytes 393224 | tf_op jit(solution)/shard_map/ppermute | solution.py:513
  81.9 13.4 %all-to-all-start.1 = ((bf16[8,19,8,128]{3,2,1,0:T(8,128)(2,1)}), bf16[8,19,8,128]{3,2,1,0:T(8,128)(2,1)S(1)}, u32[]{:S(2)}, u32[]{:S(2)}) async-start(bf16[8,19,8,128]{3,2,1,0:T(8,128)(2,1)} %shard_map.164), calls=%async_computation.1 | async-start | bytes 622592 | tf_op jit(solution)/shard_map/all_to_all | solution.py:451
  85.6 17.6 %copy-start.1 = (bf16[8,4096]{1,0:T(8,128)(2,1)S(1)}, bf16[8,4096]{1,0:T(8,128)(2,1)}, u32[]{:S(2)}) copy-start(bf16[8,4096]{1,0:T(8,128)(2,1)} %context_.1) | copy-start | bytes 196612
  85.6 17.6 %copy-start.2 = (bf16[64,128]{1,0:T(8,128)(2,1)S(1)}, bf16[64,128]{1,0:T(8,128)(2,1)}, u32[]{:S(2)}) copy-start(bf16[64,128]{1,0:T(8,128)(2,1)} %fading_.3) | copy-start | bytes 49156
  85.6 17.6 %copy-start.3 = (bf16[64,128]{1,0:T(8,128)(2,1)S(1)}, bf16[64,128]{1,0:T(8,128)(2,1)}, u32[]{:S(2)}) copy-start(bf16[64,128]{1,0:T(8,128)(2,1)} %step_.3) | copy-start | bytes 49156
  85.6 17.6 %copy-start.6 = (f32[128,2]{0,1:T(2,128)S(1)}, f32[128,2]{0,1:T(2,128)}, u32[]{:S(2)}) copy-start(f32[128,2]{0,1:T(2,128)} %param.31) | copy-start | bytes 3076
  85.6 16.3 %collective-permute-start.6 = (bf16[8,8,4096]{2,1,0:T(8,128)(2,1)S(1)}, bf16[8,8,4096]{2,1,0:T(8,128)(2,1)S(1)}, u32[]{:S(2)}, u32[]{:S(2)}) collective-permute-start(bf16[8,8,4096]{2,1,0:T(8,128)(2,1)S(1)} %constant_dynamic-update-slice_fusion), channel_id=1, source_target_pairs={{0,1},{1,0},{2,3},{3,2},{4,5},{5,4},{6,7},{7,6},{8,9},{9,8},{10,11... | collective-permute-start | bytes 1572872 | tf_op jit(solution)/shard_map/ppermute | solution.py:455
  95.3 7.9 %collective-permute-start = (bf16[8,19,8,128]{3,2,1,0:T(8,128)(2,1)S(1)}, bf16[8,19,8,128]{3,2,1,0:T(8,128)(2,1)S(1)}, u32[]{:S(2)}, u32[]{:S(2)}) collective-permute-start(bf16[8,19,8,128]{3,2,1,0:T(8,128)(2,1)S(1)} %all-to-all-done.1.mine), channel_id=1, source_target_pairs={{0,1},{1,0},{2,3},{3,2},{4,5},{5,4},{6,7},{7,6},{8,9},{9,8},{10,11... | collective-permute-start | bytes 933896 | tf_op jit(solution)/shard_map/ppermute | solution.py:455
  101.9 1.2 copy-start.8
  103.1 0.6 copy-start.4
  103.1 0.7 copy-start.5
  111.7 73.3 %all-to-all-start.2 = ((bf16[16,152,128]{2,1,0:T(8,128)(2,1)}), bf16[16,152,128]{2,1,0:T(8,128)(2,1)S(1)}, u32[]{:S(2)}, u32[]{:S(2)}) async-start(bf16[16,152,128]{2,1,0:T(8,128)(2,1)} %get-tuple-element.11), calls=%async_computation.2 | async-start | bytes 1245184 | tf_op jit(solution)/shard_map/all_to_all | solution.py:451
  118.0 67.1 %all-gather.3.cloned.1.call-start = ((), (), s32[]{:S(2)}) async-start(), calls=%async_computation.4 | async-start | bytes 1114112 | tf_op jit(solution)/shard_map/all_gather | solution.py:509
  185.1 0.7 copy-start.7
  191.9 12.9 %collective-permute-start.7 = (bf16[8,8,4096]{2,1,0:T(8,128)(2,1)S(1)}, bf16[8,8,4096]{2,1,0:T(8,128)(2,1)S(1)}, u32[]{:S(2)}, u32[]{:S(2)}) collective-permute-start(bf16[8,8,4096]{2,1,0:T(8,128)(2,1)S(1)} %get-tuple-element.15), channel_id=1, source_target_pairs={{0,1},{1,0},{2,3},{3,2},{4,5},{5,4},{6,7},{7,6},{8,9},{9,8},{10,11... | collective-permute-start | bytes 1572872 | tf_op jit(solution)/shard_map/ppermute | solution.py:455
Sparse Core Ops, SparseCore 0:
  120.9 64.1 all-gather.2

commit v7 on v6

--- a/solution.py
+++ b/solution.py
@@ -16,17 +16,16 @@
 BF16, F32 = jnp.bfloat16, jnp.float32
 
 VMEM = pl.BlockSpec(memory_space=pltpu.VMEM)
-SMEM = pl.BlockSpec(memory_space=pltpu.SMEM)
 HBM = pl.BlockSpec(memory_space=pltpu.HBM)
 
 
-def call(body, outs, *args, flops=0, scalars=0, scratch=(), fetched=0, room=SOME):
+def call(body, outs, *args, flops=0, scratch=(), fetched=0, room=SOME):
     many = isinstance(outs, list)
     shapes = [jax.ShapeDtypeStruct(s, d) for s, d in (outs if many else [outs])]
     got = pl.pallas_call(
         body,
         out_shape=shapes,
-        in_specs=[SMEM] * scalars + [VMEM] * (len(args) - scalars - fetched) + [HBM] * fetched,
+        in_specs=[VMEM] * (len(args) - fetched) + [HBM] * fetched,
         out_specs=[VMEM] * len(shapes),
         scratch_shapes=list(scratch),
         compiler_params=pltpu.CompilerParams(vmem_limit_bytes=room),
@@ -72,7 +71,8 @@
     return jnp.concatenate([first + third, second + last], axis=1)
 
 
-def partials_kernel(place, sample, prompt, lower, shifting, stretch, valve, out, conds, low_rows, held, sems):
+def partials_kernel(sample, prompt, lower, shifting, stretch, valve, out, conds, low_rows, held, sems):
+    place = here()
     pairs = [(sample, conds.at[0]), (prompt, conds.at[1]), (lower, low_rows)]
     pairs += [(ref, held.at[n]) for n, ref in enumerate((shifting, stretch, valve))]
     copies = [pltpu.make_async_copy(ref, to, sems.at[n]) for n, (ref, to) in enumerate(pairs)]
@@ -124,6 +124,11 @@
     for p in range(out.shape[0]):
         for n, block in enumerate(blocks):
             out[p, n] = block
+
+
+def here():
+    tp = lax.axis_index("tp")
+    return lax.axis_index("sp"), tp % 2, tp
 
 
 def by_core(core, own, other):
@@ -334,14 +339,15 @@
 
 
 def block_kernel(
-    place, mine, theirs, near, far, context_, wq, wk, wv, fading_, step_, rates_, spikes_,
-    sent, asked, base, vectors,
-    context, held, fading, step, rates, spikes, u, moved_q, moved_k, moved_v, moved_low, sems,
+    mine, theirs, near, far, context_, wq, wk, wv, fading_, step_, rates_, gains_, spikes_,
+    sent, asked, base, vectors, fading, step, lines,
+    context, held, spikes, u, moved_q, moved_k, moved_v, moved_low, sems,
 ):
+    place = here()
     lanes = wq.shape[1]
     pairs = [(context_, context)]
     pairs += [(ref, held.at[n // 2, :, pl.ds(n % 2 * lanes, lanes)]) for n, ref in enumerate((wq, wk, wv))]
-    pairs += [(fading_, fading), (step_, step), (rates_, rates), (spikes_, spikes)]
+    pairs += [(fading_, fading), (step_, step), (rates_, lines.at[0:1]), (gains_, lines.at[1:2]), (spikes_, spikes)]
     copies = [pltpu.make_async_copy(ref, to, sems.at[n]) for n, (ref, to) in enumerate(pairs)]
     for copy in copies:
         copy.start()
@@ -358,7 +364,7 @@
         for part, to in ((low, moved_low), (k, moved_k), (v, moved_v), (q, moved_q))
     ]
     ahead, behind = block_terms(
-        own[1], own[2], own[0][:, :HEAD], fading[...], step[...], rates[...], spikes[...], own[3]
+        own[1], own[2], own[0][:, :HEAD], fading[...], step[...], lines[0:1], spikes[...], own[3]
     )
     same = same_head(ahead[0].shape)
     size = same.shape[0]
@@ -380,27 +386,20 @@
     return jnp.where(same, packed, 0.0), jnp.where(same, pltpu.roll(packed, HEAD, 0), 0.0)
 
 
-def read_kernel(
-    place, maps, asked, base, fading_, step_, rates_, gains_, emit_,
-    keep, give,
-    fading, step, rates, gains, emit, sems,
-):
-    pairs = [(fading_, fading), (step_, step), (rates_, rates), (gains_, gains), (emit_, emit)]
-    copies = [pltpu.make_async_copy(ref, to, sems.at[n]) for n, (ref, to) in enumerate(pairs)]
-    for copy in copies:
-        copy.start()
-    for copy in copies[:4]:
-        copy.wait()
+def read_kernel(maps, asked, base, fading, step, lines, emit_, keep, give, emit, sem):
+    copy = pltpu.make_async_copy(emit_, emit, sem)
+    copy.start()
+    rates, gains = lines[0:1], lines[1:2]
     peers, _, size = maps.shape
     extra = keep.shape[1]
     same = same_head((size, size))
-    me, core = place[0], place[1]
+    me, core, _ = here()
     parts = [
         jnp.concatenate([maps[j, size + n * extra : size + (n + 1) * extra].astype(F32) for j in range(peers)], axis=0)
         for n in range(3)
     ]
     parts = [part.astype(BF16) for part in parts]
-    context = block_terms(parts[0], parts[1], parts[2][:, :HEAD], fading[...], step[...], rates[...])
+    context = block_terms(parts[0], parts[1], parts[2][:, :HEAD], fading[...], step[...], rates)
     eye = (iota((size, size), 0) == iota((size, size), 1)).astype(F32)
     composed = [jnp.concatenate([eye, jnp.zeros_like(eye)], axis=0) for _ in range(2)]
     for n in range(peers - 1):
@@ -422,14 +421,14 @@
         return jnp.where(first, left, right) * (1.0 / HEAD)
 
     out = out - mean(out)
-    normed = out * lax.rsqrt(mean(out * out) + EPS_HEAD) * gains[...]
+    normed = out * lax.rsqrt(mean(out * out) + EPS_HEAD) * gains
     chips, rows, _ = keep.shape
     split = normed.reshape(chips, 2, rows, size)
     even, odd = split[:, 0].reshape(chips * rows, size), split[:, 1].reshape(chips * rows, size)
     mine = jnp.where(core == 0, even, odd)
     other = jnp.where(core == 0, odd, even)
     left = jnp.concatenate([mine, other], axis=0).astype(BF16)
-    copies[4].wait()
+    copy.wait()
     lane = emit.shape[2]
     for s in range(emit.shape[0]):
         part = dot(left, emit[s]).reshape(2, chips, rows, lane).astype(BF16)
@@ -475,7 +474,6 @@
     emit_matrix,
 ):
     n_sp, n_tp = lax.axis_size("sp"), lax.axis_size("tp")
-    me, tp = lax.axis_index("sp"), lax.axis_index("tp")
     rows, width = hidden_items.shape
     extra = prompt_items.shape[0]
     count = rows * n_tp
@@ -483,19 +481,16 @@
     span, chunk = adjust_shifting.shape
     chips = n_tp // 2
     same_core = [[2 * i + c for i in range(chips)] for c in range(2)]
-    place = jnp.stack([me, tp % 2, tp]).astype(jnp.int32)
 
     parts = call(
         partials_kernel,
         ((n_sp, 4, 8, lanes), BF16),
-        place,
         sample_cond.reshape(-1, lanes),
         prompt_cond.reshape(-1, lanes),
         joint_lower_projector.T,
         adjust_shifting,
         adjust_stretch,
         skip_valve,
-        scalars=1,
         fetched=6,
         room=ALL,
         flops=8 * span * chunk * 6,
@@ -514,7 +509,7 @@
 
     below = shifted(hidden_items, 2)
     above = shifted(hidden_items, -2)
-    across = shifted(hidden_items, 4)
+    across = shifted(above, -2)
     odd_below = shifted(jnp.stack([hidden_items, below]), 1)
     odd_above = shifted(jnp.stack([hidden_items, above]), -1)
     near = jnp.concatenate([jnp.stack([hidden_items, below, above, across]), odd_below, odd_above], axis=0)
@@ -525,16 +520,17 @@
     theirs = swapped(mine, "tp", 1)
 
     padded = count + -(-extra // 16) * 16
-    rates = feature_fading.reshape(1, lanes)
-    sent, asked, base, vectors = call(
+    sent, asked, base, vectors, *small = call(
         block_kernel,
         [
             ((n_sp, lanes + 3 * extra, lanes), BF16),
             ((2, count, lanes), BF16),
             ((count, lanes), F32),
             ((n_tp, 8, chunk), F32),
+            (fading_raise_matrix.shape, BF16),
+            (step_raise_matrix.shape, BF16),
+            ((2, lanes), F32),
         ],
-        place,
         mine,
         theirs,
         near.reshape(count // 2, width),
@@ -545,48 +541,36 @@
         payload_matrix,
         fading_raise_matrix,
         step_raise_matrix,
-        rates,
+        feature_fading.reshape(1, lanes),
+        group_standard_factor.reshape(1, lanes),
         spike_logfade.T,
-        scalars=1,
-        fetched=8,
+        fetched=9,
         room=MOST,
         flops=2 * padded * width * lanes * 4,
         scratch=[
             pltpu.VMEM((extra, width), BF16),
             pltpu.VMEM((2, width, 2 * lanes), BF16),
-            pltpu.VMEM(fading_raise_matrix.shape, BF16),
-            pltpu.VMEM(step_raise_matrix.shape, BF16),
-            pltpu.VMEM(rates.shape, F32),
             pltpu.VMEM(spike_logfade.shape[::-1], F32),
             pltpu.VMEM((padded, width), BF16),
             *[pltpu.VMEM((n_tp, rows, lanes), F32)] * 4,
-            pltpu.SemaphoreType.DMA((8,)),
+            pltpu.SemaphoreType.DMA((9,)),
         ],
     )
     maps = exchange(sent, "sp")
     keep, give = call(
         read_kernel,
         [((chips, rows, width), BF16)] * 2,
-        place,
         maps,
         asked,
         base,
-        fading_raise_matrix,
-        step_raise_matrix,
-        rates,
-        group_standard_factor.reshape(1, lanes),
+        *small,
         emit,
-        scalars=1,
-        fetched=5,
+        fetched=1,
         room=READ,
         flops=2 * count * lanes * width,
         scratch=[
-            pltpu.VMEM(fading_raise_matrix.shape, BF16),
-            pltpu.VMEM(step_raise_matrix.shape, BF16),
-            pltpu.VMEM(rates.shape, F32),
-            pltpu.VMEM((1, lanes), F32),
             pltpu.VMEM((n_sp, *emit_matrix.shape), BF16),
-            pltpu.SemaphoreType.DMA((5,)),
+            pltpu.SemaphoreType.DMA,
         ],
     )
     given = swapped(give, "tp", 1)

time: 235 us -> 234 us (level)
  starting transfers between devices: 99.6 us -> 103 us
    all_to_all x3, starting transfers between devices: 53.4 us -> 60.6 us  [exchange(): lax.all_to_all(blocks, axis, 0, 0, tiled=True, axis_index_groups=groups)]
    all_to_all x3, waiting for transfers between devices: 8.45 us -> 5.05 us  [exchange(): lax.all_to_all(blocks, axis, 0, 0, tiled=True, axis_index_groups=groups)]
    ppermute x5, starting transfers between devices: 22.5 us -> 19.8 us  [shifted(): lax.ppermute(value, 'tp', [(i, (i + 2 * chips_on) % n_tp) for i in range(...]
  transfers between devices with their start and end apart: 12 -> 12, of which waited for: 6 -> 5; matrix products, arithmetic and copies ran while one was open for 0% -> 0% of each run, Pallas kernels for 1% -> 1%
where the time goes in v7:
time: 234 us; the launch traced here: 233 us
  starting transfers between devices  103 us (44%)
  waiting for transfers between devices  77.2 us (33%)
  blocking collectives  21 us (9%)
  Pallas kernels  17.9 us (8%)
  between operations  13.7 us (6%)
    all_gather x1, waiting for transfers between devices, shards(): emit = lax.all_gather(emit_matrix, 'sp', axis=0)  66.3 us
    all_to_all x3, starting transfers between devices, exchange(): lax.all_to_all(blocks, axis, 0, 0, tiled=True, axis_index_groups=groups)  60.6 us
    ppermute x3, starting transfers between devices, swapped(): lax.ppermute(value, axis, [(i, i ^ bit) for i in range(lax.axis_size(axis...  22.1 us
    all_to_all x1, blocking collectives, exchange(): lax.all_to_all(blocks, axis, 0, 0, tiled=True, axis_index_groups=groups)  21 us
    ppermute x5, starting transfers between devices, shifted(): lax.ppermute(value, 'tp', [(i, (i + 2 * chips_on) % n_tp) for i in range(...  19.8 us
    pallas_call x5, Pallas kernels, call(): pl.pallas_call(body, out_shape=shapes, in_specs=[VMEM] * (len(args) - fet...  17.9 us
    all_to_all x3, waiting for transfers between devices, exchange(): lax.all_to_all(blocks, axis, 0, 0, tiled=True, axis_index_groups=groups)  5.05 us
  transfers between devices with their start and end apart: 12, of which 5 were waited for; matrix products, arithmetic and copies ran while one was open for 0% of the time, Pallas kernels for 1%

profile of v7, /device:TPU:65, one launch (start us, length us, event | category | flops | bytes accessed | tf_op | source)
XLA Modules:
  0.0 233.3 jit_solution(12369821846454208166)
XLA Ops:
  6.5 7.0 %collective-permute-start.2 = (bf16[8,4096]{1,0:T(8,128)(2,1)}, bf16[8,4096]{1,0:T(8,128)(2,1)S(1)}, u32[]{:S(2)}, u32[]{:S(2)}) collective-permute-start(bf16[8,4096]{1,0:T(8,128)(2,1)} %hidden.1), channel_id=1, source_target_pairs={{0,12},{1,13},{2,14},{3,15},{4,0},{5,1},{6,2},{7,3},{8,4},{9,5},{1... | collective-permute-start | bytes 196616 | tf_op jit(solution)/shard_map/ppermute | solution.py:508
  13.6 2.0 collective-permute-start.1
  15.5 2.0 shard_map.163
  17.5 0.0 copy-start
  17.5 43.5 %all-to-all-start = ((bf16[16,4,8,128]{3,2,1,0:T(8,128)(2,1)}), bf16[16,4,8,128]{3,2,1,0:T(8,128)(2,1)S(1)}, u32[]{:S(2)}, u32[]{:S(2)}) async-start(bf16[16,4,8,128]{3,2,1,0:T(8,128)(2,1)} %shard_map.163), calls=%async_computation | async-start | bytes 262144 | tf_op jit(solution)/shard_map/all_to_all | solution.py:450
  61.1 0.0 copy-done
  61.1 0.0 collective-permute-done.2
  61.1 0.0 collective-permute-done.1
  61.2 2.4 %collective-permute-start.4 = (bf16[2,8,4096]{2,1,0:T(8,128)(2,1)S(1)}, bf16[2,8,4096]{2,1,0:T(8,128)(2,1)S(1)}, u32[]{:S(2)}, u32[]{:S(2)}) collective-permute-start(bf16[2,8,4096]{2,1,0:T(8,128)(2,1)S(1)} %get-tuple-element.24), channel_id=1, source_target_pairs={{0,2},{1,3},{2,4},{3,5},{4,6},{5,7},{6,8},{7,9},{8,10},{9,11},{10,... | collective-permute-start | bytes 393224 | tf_op jit(solution)/shard_map/ppermute | solution.py:508
  63.6 4.3 %collective-permute-start.5 = (bf16[2,8,4096]{2,1,0:T(8,128)(2,1)S(1)}, bf16[2,8,4096]{2,1,0:T(8,128)(2,1)S(1)}, u32[]{:S(2)}, u32[]{:S(2)}) collective-permute-start(bf16[2,8,4096]{2,1,0:T(8,128)(2,1)S(1)} %get-tuple-element.23), channel_id=1, source_target_pairs={{0,14},{1,15},{2,0},{3,1},{4,2},{5,3},{6,4},{7,5},{8,6},{9,7},{10,... | collective-permute-start | bytes 393224 | tf_op jit(solution)/shard_map/ppermute | solution.py:508
  67.9 4.1 %collective-permute-start.3 = (bf16[8,4096]{1,0:T(8,128)(2,1)S(1)}, bf16[8,4096]{1,0:T(8,128)(2,1)S(1)}, u32[]{:S(2)}, u32[]{:S(2)}) collective-permute-start(bf16[8,4096]{1,0:T(8,128)(2,1)S(1)} %collective-permute-done.2), channel_id=1, source_target_pairs={{0,12},{1,13},{2,14},{3,15},{4,0},{5,1},{6,2},{7,3},{8,4},{9,5},{1... | collective-permute-start | bytes 196616 | tf_op jit(solution)/shard_map/ppermute | solution.py:508
  72.1 2.4 %collective-permute-done.3 = bf16[8,4096]{1,0:T(8,128)(2,1)S(1)} collective-permute-done((bf16[8,4096]{1,0:T(8,128)(2,1)S(1)}, bf16[8,4096]{1,0:T(8,128)(2,1)S(1)}, u32[]{:S(2)}, u32[]{:S(2)}) %collective-permute-start.3) | collective-permute-done | bytes 65568 | tf_op jit(solution)/shard_map/ppermute | solution.py:508
  74.5 0.0 collective-permute-done.4
  74.5 0.0 all-to-all-done.parts
  74.5 0.8 shard_map.164
  75.3 5.2 %all-to-all-start.1 = ((bf16[8,19,8,128]{3,2,1,0:T(8,128)(2,1)}), bf16[8,19,8,128]{3,2,1,0:T(8,128)(2,1)S(1)}, u32[]{:S(2)}, u32[]{:S(2)}) async-start(bf16[8,19,8,128]{3,2,1,0:T(8,128)(2,1)} %shard_map.164), calls=%async_computation.1 | async-start | bytes 622592 | tf_op jit(solution)/shard_map/all_to_all | solution.py:450
  80.5 0.0 copy-start.1
  80.5 0.0 collective-permute-done.5
  80.5 0.0 copy-start.2
  80.5 0.0 copy-start.3
  80.6 0.0 copy-start.6
  80.6 4.8 %collective-permute-start.6 = (bf16[8,8,4096]{2,1,0:T(8,128)(2,1)S(1)}, bf16[8,8,4096]{2,1,0:T(8,128)(2,1)S(1)}, u32[]{:S(2)}, u32[]{:S(2)}) collective-permute-start(bf16[8,8,4096]{2,1,0:T(8,128)(2,1)S(1)} %constant_dynamic-update-slice_fusion), channel_id=1, source_target_pairs={{0,1},{1,0},{2,3},{3,2},{4,5},{5,4},{6,7},{7,6},{8,9},{9,8},{10,11... | collective-permute-start | bytes 1572872 | tf_op jit(solution)/shard_map/ppermute | solution.py:454
  85.4 5.0 %all-to-all-done.1.mine = bf16[8,19,8,128]{3,2,1,0:T(8,128)(2,1)S(1)} async-done(((bf16[8,19,8,128]{3,2,1,0:T(8,128)(2,1)}), bf16[8,19,8,128]{3,2,1,0:T(8,128)(2,1)S(1)}, u32[]{:S(2)}, u32[]{:S(2)}) %all-to-all-start.1) | async-done | bytes 311328 | tf_op jit(solution)/shard_map/all_to_all | solution.py:450
  90.5 5.9 %collective-permute-start = (bf16[8,19,8,128]{3,2,1,0:T(8,128)(2,1)S(1)}, bf16[8,19,8,128]{3,2,1,0:T(8,128)(2,1)S(1)}, u32[]{:S(2)}, u32[]{:S(2)}) collective-permute-start(bf16[8,19,8,128]{3,2,1,0:T(8,128)(2,1)S(1)} %all-to-all-done.1.mine), channel_id=1, source_target_pairs={{0,1},{1,0},{2,3},{3,2},{4,5},{5,4},{6,7},{7,6},{8,9},{9,8},{10,11... | collective-permute-start | bytes 933896 | tf_op jit(solution)/shard_map/ppermute | solution.py:454
  96.4 0.0 collective-permute-done.6
  96.4 0.0 copy-start.7
  96.4 1.2 collective-permute-done.theirs
  97.6 0.0 copy-start.4
  97.6 0.0 copy-start.5
  97.6 0.0 copy-done.7
  97.6 0.0 copy-done.1
  97.6 0.0 copy-done.2
  97.6 0.0 copy-done.3
  97.6 0.0 copy-done.6
  97.6 0.6 copy-done.4
  98.3 0.0 copy-done.5
  98.3 7.9 %shard_map.165 = (bf16[16,152,128]{2,1,0:T(8,128)(2,1)}, bf16[2,128,128]{2,1,0:T(8,128)(2,1)S(1)}, f32[128,128]{1,0:T(8,128)S(1)}, f32[16,8,256]{2,1,0:T(8,128)S...) custom-call(bf16[8,19,8,128]{3,2,1,0:T(8,128)(2,1)S(1)} %all-to-all-done.1.mine, ...), custom_call_target="tpu_custom_call" | custom-call | flops 603979776 | bytes 4917248 | tf_op jit(solution)/shard_map/pallas_call | solution.py:25
  106.2 11.8 %all-to-all-start.2 = ((bf16[16,152,128]{2,1,0:T(8,128)(2,1)}), bf16[16,152,128]{2,1,0:T(8,128)(2,1)S(1)}, u32[]{:S(2)}, u32[]{:S(2)}) async-start(bf16[16,152,128]{2,1,0:T(8,128)(2,1)} %get-tuple-element.14), calls=%async_computation.2 | async-start | bytes 1245184 | tf_op jit(solution)/shard_map/all_to_all | solution.py:450
  118.0 0.1 all-gather.3.cloned.1.call-start
  118.1 0.7 all-gather.3.cloned.1.call-update
  118.8 66.3 %all-gather.3.cloned.1.call-done = bf16[2048,256]{1,0:T(8,128)(2,1)} async-done(((bf16[128,256]{1,0:T(8,128)(2,1)}), bf16[2048,256]{1,0:T(8,128)(2,1)}) %all-gather.3.cloned.1.call-update) | async-done | bytes 1048592 | tf_op jit(solution)/shard_map/all_gather | solution.py:504
  185.1 0.0 all-to-all-done.2.maps
  185.1 6.5 %shard_map.166 = (bf16[8,8,4096]{2,1,0:T(8,128)(2,1)S(1)}, bf16[8,8,4096]{2,1,0:T(8,128)(2,1)S(1)}) custom-call(bf16[16,152,128]{2,1,0:T(8,128)(2,1)S(1)} %all-to-all-done.2.maps, bf16[2,128,128]{2,1,0:T(8,128)(2,1)S(1)} %get-tuple-element.15.asked, f32[128,128]{1,0:T(8,128)S(1)} %get-tuple-element.16.base, bf16[64,128]{1,0:T(8,128)(2,1)S(1)} %get-tuple-element.17.fading, ...), custom_call_target="tpu_custom_call" | custom-call | flops 134217728 | bytes 1836032 | tf_op jit(solution)/shard_map/pallas_call | solution.py:25
  191.7 11.4 %collective-permute-start.7 = (bf16[8,8,4096]{2,1,0:T(8,128)(2,1)S(1)}, bf16[8,8,4096]{2,1,0:T(8,128)(2,1)S(1)}, u32[]{:S(2)}, u32[]{:S(2)}) collective-permute-start(bf16[8,8,4096]{2,1,0:T(8,128)(2,1)S(1)} %get-tuple-element.21), channel_id=1, source_target_pairs={{0,1},{1,0},{2,3},{3,2},{4,5},{5,4},{6,7},{7,6},{8,9},{9,8},{10,11... | collective-permute-start | bytes 1572872 | tf_op jit(solution)/shard_map/ppermute | solution.py:454
  203.1 1.5 collective-permute-done.7
  204.6 0.1 add_convert_fusion
  204.7 21.0 %all_to_all.20.parts = bf16[8,8,4096]{2,1,0:T(8,128)(2,1)S(1)} all-to-all(bf16[8,8,4096]{2,1,0:T(8,128)(2,1)S(1)} %add_convert_fusion), channel_id=1, replica_groups={{0,2,4,6,8,10,12,14},{1,3,5,7,9,11,13,15},{16,18,20,22,24,26,28,30},{17..., dimensions={0} | all-to-all | bytes 1048576 | tf_op jit(solution)/shard_map/all_to_all | solution.py:450
  225.7 0.7 shard_map.167
  (7 shorter events, 0.1 us)
Async XLA Ops:
  6.5 54.6 %collective-permute-start.2 = (bf16[8,4096]{1,0:T(8,128)(2,1)}, bf16[8,4096]{1,0:T(8,128)(2,1)S(1)}, u32[]{:S(2)}, u32[]{:S(2)}) collective-permute-start(bf16[8,4096]{1,0:T(8,128)(2,1)} %hidden.1), channel_id=1, source_target_pairs={{0,12},{1,13},{2,14},{3,15},{4,0},{5,1},{6,2},{7,3},{8,4},{9,5},{1... | collective-permute-start | bytes 196616 | tf_op jit(solution)/shard_map/ppermute | solution.py:508
  13.6 47.6 %collective-permute-start.1 = (bf16[8,4096]{1,0:T(8,128)(2,1)}, bf16[8,4096]{1,0:T(8,128)(2,1)S(1)}, u32[]{:S(2)}, u32[]{:S(2)}) collective-permute-start(bf16[8,4096]{1,0:T(8,128)(2,1)} %hidden.1), channel_id=1, source_target_pairs={{0,4},{1,5},{2,6},{3,7},{4,8},{5,9},{6,10},{7,11},{8,12},{9,13},{1... | collective-permute-start | bytes 196616 | tf_op jit(solution)/shard_map/ppermute | solution.py:508
  17.5 43.6 %copy-start = (bf16[8,4096]{1,0:T(8,128)(2,1)S(1)}, bf16[8,4096]{1,0:T(8,128)(2,1)}, u32[]{:S(2)}) copy-start(bf16[8,4096]{1,0:T(8,128)(2,1)} %hidden.1) | copy-start | bytes 196612
  17.5 56.9 %all-to-all-start = ((bf16[16,4,8,128]{3,2,1,0:T(8,128)(2,1)}), bf16[16,4,8,128]{3,2,1,0:T(8,128)(2,1)S(1)}, u32[]{:S(2)}, u32[]{:S(2)}) async-start(bf16[16,4,8,128]{3,2,1,0:T(8,128)(2,1)} %shard_map.163), calls=%async_computation | async-start | bytes 262144 | tf_op jit(solution)/shard_map/all_to_all | solution.py:450
  61.2 13.3 %collective-permute-start.4 = (bf16[2,8,4096]{2,1,0:T(8,128)(2,1)S(1)}, bf16[2,8,4096]{2,1,0:T(8,128)(2,1)S(1)}, u32[]{:S(2)}, u32[]{:S(2)}) collective-permute-start(bf16[2,8,4096]{2,1,0:T(8,128)(2,1)S(1)} %get-tuple-element.24), channel_id=1, source_target_pairs={{0,2},{1,3},{2,4},{3,5},{4,6},{5,7},{6,8},{7,9},{8,10},{9,11},{10,... | collective-permute-start | bytes 393224 | tf_op jit(solution)/shard_map/ppermute | solution.py:508
  63.6 17.0 %collective-permute-start.5 = (bf16[2,8,4096]{2,1,0:T(8,128)(2,1)S(1)}, bf16[2,8,4096]{2,1,0:T(8,128)(2,1)S(1)}, u32[]{:S(2)}, u32[]{:S(2)}) collective-permute-start(bf16[2,8,4096]{2,1,0:T(8,128)(2,1)S(1)} %get-tuple-element.23), channel_id=1, source_target_pairs={{0,14},{1,15},{2,0},{3,1},{4,2},{5,3},{6,4},{7,5},{8,6},{9,7},{10,... | collective-permute-start | bytes 393224 | tf_op jit(solution)/shard_map/ppermute | solution.py:508
  67.9 6.5 %collective-permute-start.3 = (bf16[8,4096]{1,0:T(8,128)(2,1)S(1)}, bf16[8,4096]{1,0:T(8,128)(2,1)S(1)}, u32[]{:S(2)}, u32[]{:S(2)}) collective-permute-start(bf16[8,4096]{1,0:T(8,128)(2,1)S(1)} %collective-permute-done.2), channel_id=1, source_target_pairs={{0,12},{1,13},{2,14},{3,15},{4,0},{5,1},{6,2},{7,3},{8,4},{9,5},{1... | collective-permute-start | bytes 196616 | tf_op jit(solution)/shard_map/ppermute | solution.py:508
  75.3 15.2 %all-to-all-start.1 = ((bf16[8,19,8,128]{3,2,1,0:T(8,128)(2,1)}), bf16[8,19,8,128]{3,2,1,0:T(8,128)(2,1)S(1)}, u32[]{:S(2)}, u32[]{:S(2)}) async-start(bf16[8,19,8,128]{3,2,1,0:T(8,128)(2,1)} %shard_map.164), calls=%async_computation.1 | async-start | bytes 622592 | tf_op jit(solution)/shard_map/all_to_all | solution.py:450
  80.5 17.1 %copy-start.1 = (bf16[8,4096]{1,0:T(8,128)(2,1)S(1)}, bf16[8,4096]{1,0:T(8,128)(2,1)}, u32[]{:S(2)}) copy-start(bf16[8,4096]{1,0:T(8,128)(2,1)} %context_.1) | copy-start | bytes 196612
  80.5 17.1 %copy-start.2 = (bf16[64,128]{1,0:T(8,128)(2,1)S(1)}, bf16[64,128]{1,0:T(8,128)(2,1)}, u32[]{:S(2)}) copy-start(bf16[64,128]{1,0:T(8,128)(2,1)} %fading_.1) | copy-start | bytes 49156
  80.5 17.1 %copy-start.3 = (bf16[64,128]{1,0:T(8,128)(2,1)S(1)}, bf16[64,128]{1,0:T(8,128)(2,1)}, u32[]{:S(2)}) copy-start(bf16[64,128]{1,0:T(8,128)(2,1)} %step_.1) | copy-start | bytes 49156
  80.6 17.1 %copy-start.6 = (f32[128]{0:T(128)S(1)}, f32[128]{0:T(128)}, u32[]{:S(2)}) copy-start(f32[128]{0:T(128)} %param.32) | copy-start | bytes 1540
  80.6 15.8 %collective-permute-start.6 = (bf16[8,8,4096]{2,1,0:T(8,128)(2,1)S(1)}, bf16[8,8,4096]{2,1,0:T(8,128)(2,1)S(1)}, u32[]{:S(2)}, u32[]{:S(2)}) collective-permute-start(bf16[8,8,4096]{2,1,0:T(8,128)(2,1)S(1)} %constant_dynamic-update-slice_fusion), channel_id=1, source_target_pairs={{0,1},{1,0},{2,3},{3,2},{4,5},{5,4},{6,7},{7,6},{8,9},{9,8},{10,11... | collective-permute-start | bytes 1572872 | tf_op jit(solution)/shard_map/ppermute | solution.py:454
  90.5 7.1 %collective-permute-start = (bf16[8,19,8,128]{3,2,1,0:T(8,128)(2,1)S(1)}, bf16[8,19,8,128]{3,2,1,0:T(8,128)(2,1)S(1)}, u32[]{:S(2)}, u32[]{:S(2)}) collective-permute-start(bf16[8,19,8,128]{3,2,1,0:T(8,128)(2,1)S(1)} %all-to-all-done.1.mine), channel_id=1, source_target_pairs={{0,1},{1,0},{2,3},{3,2},{4,5},{5,4},{6,7},{7,6},{8,9},{9,8},{10,11... | collective-permute-start | bytes 933896 | tf_op jit(solution)/shard_map/ppermute | solution.py:454
  96.4 1.2 copy-start.7
  97.6 0.7 copy-start.4
  97.6 0.7 copy-start.5
  106.2 79.0 %all-to-all-start.2 = ((bf16[16,152,128]{2,1,0:T(8,128)(2,1)}), bf16[16,152,128]{2,1,0:T(8,128)(2,1)S(1)}, u32[]{:S(2)}, u32[]{:S(2)}) async-start(bf16[16,152,128]{2,1,0:T(8,128)(2,1)} %get-tuple-element.14), calls=%async_computation.2 | async-start | bytes 1245184 | tf_op jit(solution)/shard_map/all_to_all | solution.py:450
  118.0 67.1 %all-gather.3.cloned.1.call-start = ((), (), s32[]{:S(2)}) async-start(), calls=%async_computation.4 | async-start | bytes 1114112 | tf_op jit(solution)/shard_map/all_gather | solution.py:504
  191.7 12.9 %collective-permute-start.7 = (bf16[8,8,4096]{2,1,0:T(8,128)(2,1)S(1)}, bf16[8,8,4096]{2,1,0:T(8,128)(2,1)S(1)}, u32[]{:S(2)}, u32[]{:S(2)}) collective-permute-start(bf16[8,8,4096]{2,1,0:T(8,128)(2,1)S(1)} %get-tuple-element.21), channel_id=1, source_target_pairs={{0,1},{1,0},{2,3},{3,2},{4,5},{5,4},{6,7},{7,6},{8,9},{9,8},{10,11... | collective-permute-start | bytes 1572872 | tf_op jit(solution)/shard_map/ppermute | solution.py:454
Sparse Core Ops, SparseCore 0:
  121.0 64.1 all-gather.2

commit v8 on v7

--- a/solution.py
+++ b/solution.py
@@ -188,7 +188,7 @@
         down[(2 * s + 1) * lanes : (2 * s + 2) * lanes] = pltpu.roll(piece, HEAD, 1).astype(BF16)
 
 
-def inverse(mixing, row, col):
+def inverse(mixing, row, col, between):
     size = row.shape[0]
     eye = (row == col).astype(F32)
     width = 1
@@ -202,12 +202,14 @@
             found = [eye - p for p in parts]
         else:
             lefts = [dot(p, f) for p, f in zip(parts, found)]
+            next(between, None)
             found = [f - dot(f, g) for f, g in zip(found, lefts)]
+            next(between, None)
         width *= 2
     return found
 
 
-def block_terms(k, v, low, fading, step, rates, spikes=None, q=None):
+def block_terms(k, v, low, fading, step, rates, spikes=None, q=None, between=iter(())):
     count, lanes = k.shape
     row, col = iota((count, lanes), 0), iota((count, lanes), 1)
     heads = lanes // HEAD
@@ -281,7 +283,7 @@
     masks = {(d, h): pair(h, d == 1, True) for d, h in chains}
     mixing = {c: scores[n][:count, :count] * masks[c] for n, c in enumerate(chains)}
     seen = {c: dot(scores[n][:count, count:] * masks[c], v) for n, c in enumerate(chains)}
-    solved = dict(zip(chains, inverse([(mixing[c], c[0] == 1) for c in chains], row, col)))
+    solved = dict(zip(chains, inverse([(mixing[c], c[0] == 1) for c in chains], row, col, between)))
 
     whole = jnp.exp(end)
     starts = (
@@ -339,24 +341,25 @@
 
 
 def block_kernel(
-    mine, theirs, near, far, context_, wq, wk, wv, fading_, step_, rates_, gains_, spikes_,
+    mine, theirs, near_, far_, context_, wq, wk, wv, fading_, step_, rates_, gains_, spikes_,
     sent, asked, base, vectors, fading, step, lines,
-    context, held, spikes, u, moved_q, moved_k, moved_v, moved_low, sems,
+    near, far, context, held, spikes, u, moved_q, moved_k, moved_v, moved_low, sems,
 ):
     place = here()
     lanes = wq.shape[1]
-    pairs = [(context_, context)]
-    pairs += [(ref, held.at[n // 2, :, pl.ds(n % 2 * lanes, lanes)]) for n, ref in enumerate((wq, wk, wv))]
+    pairs = [(near_, near), (far_, far), (context_, context)]
+    pairs += [(ref, held.at[n]) for n, ref in enumerate((wq, wk, wv))]
     pairs += [(fading_, fading), (step_, step), (rates_, lines.at[0:1]), (gains_, lines.at[1:2]), (spikes_, spikes)]
     copies = [pltpu.make_async_copy(ref, to, sems.at[n]) for n, (ref, to) in enumerate(pairs)]
     for copy in copies:
         copy.start()
-    copies[0].wait()
-    modulated(place, near, far, context, mine, theirs, u, vectors, held.at[1, :, pl.ds(lanes, lanes)])
-    for copy in copies[1:]:
+    for copy in copies[:3]:
+        copy.wait()
+    modulated(place, near, far, context, mine, theirs, u, vectors, held.at[3])
+    for copy in copies[3:]:
         copy.wait()
     count, extra = asked.shape[1], context.shape[0]
-    first, second = dot(u[...], held[0]), dot(u[...], held[1])
+    first, second = (dot(u[...], jnp.concatenate([held[n], held[n + 1]], axis=1)) for n in (0, 2))
     q, k, v, low = first[:, :lanes], first[:, lanes:], second[:, :lanes], second[:, lanes:]
     low = jnp.where(iota(low.shape, 1) < HEAD, low, 0.0)
     own = [
@@ -399,15 +402,24 @@
         for n in range(3)
     ]
     parts = [part.astype(BF16) for part in parts]
-    context = block_terms(parts[0], parts[1], parts[2][:, :HEAD], fading[...], step[...], rates)
     eye = (iota((size, size), 0) == iota((size, size), 1)).astype(F32)
     composed = [jnp.concatenate([eye, jnp.zeros_like(eye)], axis=0) for _ in range(2)]
-    for n in range(peers - 1):
-        for d, j, reached in ((0, n, n < me), (1, peers - 1 - n, peers - 1 - n > me)):
-            factor, offset = opened(maps[j, :size], same)
-            new = dot(composed[d], factor)
-            new = jnp.concatenate([new[:size], new[size:] + offset], axis=0)
-            composed[d] = jnp.where(reached, new, composed[d])
+
+    def composing():
+        for n in range(peers - 1):
+            for d, j, reached in ((0, n, n < me), (1, peers - 1 - n, peers - 1 - n > me)):
+                factor, offset = opened(maps[j, :size], same)
+                new = dot(composed[d], factor)
+                new = jnp.concatenate([new[:size], new[size:] + offset], axis=0)
+                composed[d] = jnp.where(reached, new, composed[d])
+            yield
+
+    steps = composing()
+    context = block_terms(
+        parts[0], parts[1], parts[2][:, :HEAD], fading[...], step[...], rates, between=steps
+    )
+    for _ in steps:
+        pass
     out = base[...]
     for d in range(2):
         start = jnp.where(same, context[d][1], 0.0)
@@ -544,16 +556,17 @@
         feature_fading.reshape(1, lanes),
         group_standard_factor.reshape(1, lanes),
         spike_logfade.T,
-        fetched=9,
+        fetched=11,
         room=MOST,
         flops=2 * padded * width * lanes * 4,
         scratch=[
+            *[pltpu.VMEM((count // 2, width), BF16)] * 2,
             pltpu.VMEM((extra, width), BF16),
-            pltpu.VMEM((2, width, 2 * lanes), BF16),
+            pltpu.VMEM((4, width, lanes), BF16),
             pltpu.VMEM(spike_logfade.shape[::-1], F32),
             pltpu.VMEM((padded, width), BF16),
             *[pltpu.VMEM((n_tp, rows, lanes), F32)] * 4,
-            pltpu.SemaphoreType.DMA((9,)),
+            pltpu.SemaphoreType.DMA((11,)),
         ],
     )
     maps = exchange(sent, "sp")

time: 234 us -> 232 us (level)
  no operation moved by 1% of the time
where the time goes in v8:
time: 232 us; the launch traced here: 231 us
  starting transfers between devices  102 us (44%)
  waiting for transfers between devices  77.4 us (33%)
  blocking collectives  21.2 us (9%)
  Pallas kernels  15.9 us (7%)
  between operations  13.7 us (6%)
    all_gather x1, waiting for transfers between devices, shards(): emit = lax.all_gather(emit_matrix, 'sp', axis=0)  66.6 us
    all_to_all x3, starting transfers between devices, exchange(): lax.all_to_all(blocks, axis, 0, 0, tiled=True, axis_index_groups=groups)  60.6 us
    ppermute x3, starting transfers between devices, swapped(): lax.ppermute(value, axis, [(i, i ^ bit) for i in range(lax.axis_size(axis...  21.8 us
    all_to_all x1, blocking collectives, exchange(): lax.all_to_all(blocks, axis, 0, 0, tiled=True, axis_index_groups=groups)  21.2 us
    ppermute x5, starting transfers between devices, shifted(): lax.ppermute(value, 'tp', [(i, (i + 2 * chips_on) % n_tp) for i in range(...  19.8 us
    pallas_call x5, Pallas kernels, call(): pl.pallas_call(body, out_shape=shapes, in_specs=[VMEM] * (len(args) - fet...  15.9 us
    all_to_all x3, waiting for transfers between devices, exchange(): lax.all_to_all(blocks, axis, 0, 0, tiled=True, axis_index_groups=groups)  5.05 us
  transfers between devices with their start and end apart: 12, of which 5 were waited for; matrix products, arithmetic and copies ran while one was open for 0% of the time, Pallas kernels for 1%

profile of v8, /device:TPU:65, one launch (start us, length us, event | category | flops | bytes accessed | tf_op | source)
XLA Modules:
  0.0 231.4 jit_solution(10558355994519540954)
XLA Ops:
  6.5 7.0 %collective-permute-start.2 = (bf16[8,4096]{1,0:T(8,128)(2,1)}, bf16[8,4096]{1,0:T(8,128)(2,1)S(1)}, u32[]{:S(2)}, u32[]{:S(2)}) collective-permute-start(bf16[8,4096]{1,0:T(8,128)(2,1)} %hidden.1), channel_id=1, source_target_pairs={{0,12},{1,13},{2,14},{3,15},{4,0},{5,1},{6,2},{7,3},{8,4},{9,5},{1... | collective-permute-start | bytes 196616 | tf_op jit(solution)/shard_map/ppermute | solution.py:520
  13.6 2.0 collective-permute-start.1
  15.5 2.0 shard_map.163
  17.5 0.0 copy-start
  17.5 43.5 %all-to-all-start = ((bf16[16,4,8,128]{3,2,1,0:T(8,128)(2,1)}), bf16[16,4,8,128]{3,2,1,0:T(8,128)(2,1)S(1)}, u32[]{:S(2)}, u32[]{:S(2)}) async-start(bf16[16,4,8,128]{3,2,1,0:T(8,128)(2,1)} %shard_map.163), calls=%async_computation | async-start | bytes 262144 | tf_op jit(solution)/shard_map/all_to_all | solution.py:462
  61.1 0.0 copy-done
  61.1 0.0 collective-permute-done.2
  61.1 0.0 collective-permute-done.1
  61.2 2.4 %collective-permute-start.4 = (bf16[2,8,4096]{2,1,0:T(8,128)(2,1)S(1)}, bf16[2,8,4096]{2,1,0:T(8,128)(2,1)S(1)}, u32[]{:S(2)}, u32[]{:S(2)}) collective-permute-start(bf16[2,8,4096]{2,1,0:T(8,128)(2,1)S(1)} %get-tuple-element.24), channel_id=1, source_target_pairs={{0,2},{1,3},{2,4},{3,5},{4,6},{5,7},{6,8},{7,9},{8,10},{9,11},{10,... | collective-permute-start | bytes 393224 | tf_op jit(solution)/shard_map/ppermute | solution.py:520
  63.6 4.3 %collective-permute-start.5 = (bf16[2,8,4096]{2,1,0:T(8,128)(2,1)S(1)}, bf16[2,8,4096]{2,1,0:T(8,128)(2,1)S(1)}, u32[]{:S(2)}, u32[]{:S(2)}) collective-permute-start(bf16[2,8,4096]{2,1,0:T(8,128)(2,1)S(1)} %get-tuple-element.23), channel_id=1, source_target_pairs={{0,14},{1,15},{2,0},{3,1},{4,2},{5,3},{6,4},{7,5},{8,6},{9,7},{10,... | collective-permute-start | bytes 393224 | tf_op jit(solution)/shard_map/ppermute | solution.py:520
  67.9 4.1 %collective-permute-start.3 = (bf16[8,4096]{1,0:T(8,128)(2,1)S(1)}, bf16[8,4096]{1,0:T(8,128)(2,1)S(1)}, u32[]{:S(2)}, u32[]{:S(2)}) collective-permute-start(bf16[8,4096]{1,0:T(8,128)(2,1)S(1)} %collective-permute-done.2), channel_id=1, source_target_pairs={{0,12},{1,13},{2,14},{3,15},{4,0},{5,1},{6,2},{7,3},{8,4},{9,5},{1... | collective-permute-start | bytes 196616 | tf_op jit(solution)/shard_map/ppermute | solution.py:520
  72.1 2.4 %collective-permute-done.3 = bf16[8,4096]{1,0:T(8,128)(2,1)S(1)} collective-permute-done((bf16[8,4096]{1,0:T(8,128)(2,1)S(1)}, bf16[8,4096]{1,0:T(8,128)(2,1)S(1)}, u32[]{:S(2)}, u32[]{:S(2)}) %collective-permute-start.3) | collective-permute-done | bytes 65568 | tf_op jit(solution)/shard_map/ppermute | solution.py:520
  74.5 0.0 collective-permute-done.4
  74.5 0.0 all-to-all-done.parts
  74.5 0.8 shard_map.164
  75.3 5.2 %all-to-all-start.1 = ((bf16[8,19,8,128]{3,2,1,0:T(8,128)(2,1)}), bf16[8,19,8,128]{3,2,1,0:T(8,128)(2,1)S(1)}, u32[]{:S(2)}, u32[]{:S(2)}) async-start(bf16[8,19,8,128]{3,2,1,0:T(8,128)(2,1)} %shard_map.164), calls=%async_computation.1 | async-start | bytes 622592 | tf_op jit(solution)/shard_map/all_to_all | solution.py:462
  80.5 0.0 copy-start.1
  80.5 0.0 collective-permute-done.5
  80.5 0.0 copy-start.2
  80.5 0.0 copy-start.3
  80.6 0.0 copy-start.6
  80.6 4.8 %collective-permute-start.6 = (bf16[8,8,4096]{2,1,0:T(8,128)(2,1)S(1)}, bf16[8,8,4096]{2,1,0:T(8,128)(2,1)S(1)}, u32[]{:S(2)}, u32[]{:S(2)}) collective-permute-start(bf16[8,8,4096]{2,1,0:T(8,128)(2,1)S(1)} %constant_dynamic-update-slice_fusion), channel_id=1, source_target_pairs={{0,1},{1,0},{2,3},{3,2},{4,5},{5,4},{6,7},{7,6},{8,9},{9,8},{10,11... | collective-permute-start | bytes 1572872 | tf_op jit(solution)/shard_map/ppermute | solution.py:466
  85.4 5.0 %all-to-all-done.1.mine = bf16[8,19,8,128]{3,2,1,0:T(8,128)(2,1)S(1)} async-done(((bf16[8,19,8,128]{3,2,1,0:T(8,128)(2,1)}), bf16[8,19,8,128]{3,2,1,0:T(8,128)(2,1)S(1)}, u32[]{:S(2)}, u32[]{:S(2)}) %all-to-all-start.1) | async-done | bytes 311328 | tf_op jit(solution)/shard_map/all_to_all | solution.py:462
  90.5 5.9 %collective-permute-start = (bf16[8,19,8,128]{3,2,1,0:T(8,128)(2,1)S(1)}, bf16[8,19,8,128]{3,2,1,0:T(8,128)(2,1)S(1)}, u32[]{:S(2)}, u32[]{:S(2)}) collective-permute-start(bf16[8,19,8,128]{3,2,1,0:T(8,128)(2,1)S(1)} %all-to-all-done.1.mine), channel_id=1, source_target_pairs={{0,1},{1,0},{2,3},{3,2},{4,5},{5,4},{6,7},{7,6},{8,9},{9,8},{10,11... | collective-permute-start | bytes 933896 | tf_op jit(solution)/shard_map/ppermute | solution.py:466
  96.4 0.0 collective-permute-done.6
  96.4 0.0 copy-start.7
  96.4 1.2 collective-permute-done.theirs
  97.6 0.0 copy-start.4
  97.6 0.0 copy-start.5
  97.6 0.0 copy-done.7
  97.6 0.0 copy-done.1
  97.6 0.0 copy-done.2
  97.6 0.0 copy-done.3
  97.6 0.0 copy-done.6
  97.6 0.6 copy-done.4
  98.3 0.0 copy-done.5
  98.3 7.2 %shard_map.165 = (bf16[16,152,128]{2,1,0:T(8,128)(2,1)}, bf16[2,128,128]{2,1,0:T(8,128)(2,1)S(1)}, f32[128,128]{1,0:T(8,128)S(1)}, f32[16,8,256]{2,1,0:T(8,128)S...) custom-call(bf16[8,19,8,128]{3,2,1,0:T(8,128)(2,1)S(1)} %all-to-all-done.1.mine, ...), custom_call_target="tpu_custom_call" | custom-call | flops 603979776 | bytes 4917248 | tf_op jit(solution)/shard_map/pallas_call | solution.py:25
  105.5 11.8 %all-to-all-start.2 = ((bf16[16,152,128]{2,1,0:T(8,128)(2,1)}), bf16[16,152,128]{2,1,0:T(8,128)(2,1)S(1)}, u32[]{:S(2)}, u32[]{:S(2)}) async-start(bf16[16,152,128]{2,1,0:T(8,128)(2,1)} %get-tuple-element.14), calls=%async_computation.2 | async-start | bytes 1245184 | tf_op jit(solution)/shard_map/all_to_all | solution.py:462
  117.3 0.1 all-gather.3.cloned.1.call-start
  117.4 0.7 all-gather.3.cloned.1.call-update
  118.1 66.6 %all-gather.3.cloned.1.call-done = bf16[2048,256]{1,0:T(8,128)(2,1)} async-done(((bf16[128,256]{1,0:T(8,128)(2,1)}), bf16[2048,256]{1,0:T(8,128)(2,1)}) %all-gather.3.cloned.1.call-update) | async-done | bytes 1048592 | tf_op jit(solution)/shard_map/all_gather | solution.py:516
  184.7 0.0 all-to-all-done.2.maps
  184.7 5.2 %shard_map.166 = (bf16[8,8,4096]{2,1,0:T(8,128)(2,1)S(1)}, bf16[8,8,4096]{2,1,0:T(8,128)(2,1)S(1)}) custom-call(bf16[16,152,128]{2,1,0:T(8,128)(2,1)S(1)} %all-to-all-done.2.maps, bf16[2,128,128]{2,1,0:T(8,128)(2,1)S(1)} %get-tuple-element.15.asked, f32[128,128]{1,0:T(8,128)S(1)} %get-tuple-element.16.base, bf16[64,128]{1,0:T(8,128)(2,1)S(1)} %get-tuple-element.17.fading, ...), custom_call_target="tpu_custom_call" | custom-call | flops 134217728 | bytes 1836032 | tf_op jit(solution)/shard_map/pallas_call | solution.py:25
  189.9 11.1 %collective-permute-start.7 = (bf16[8,8,4096]{2,1,0:T(8,128)(2,1)S(1)}, bf16[8,8,4096]{2,1,0:T(8,128)(2,1)S(1)}, u32[]{:S(2)}, u32[]{:S(2)}) collective-permute-start(bf16[8,8,4096]{2,1,0:T(8,128)(2,1)S(1)} %get-tuple-element.21), channel_id=1, source_target_pairs={{0,1},{1,0},{2,3},{3,2},{4,5},{5,4},{6,7},{7,6},{8,9},{9,8},{10,11... | collective-permute-start | bytes 1572872 | tf_op jit(solution)/shard_map/ppermute | solution.py:466
  200.9 1.5 collective-permute-done.7
  202.4 0.1 add_convert_fusion
  202.6 21.2 %all_to_all.20.parts = bf16[8,8,4096]{2,1,0:T(8,128)(2,1)S(1)} all-to-all(bf16[8,8,4096]{2,1,0:T(8,128)(2,1)S(1)} %add_convert_fusion), channel_id=1, replica_groups={{0,2,4,6,8,10,12,14},{1,3,5,7,9,11,13,15},{16,18,20,22,24,26,28,30},{17..., dimensions={0} | all-to-all | bytes 1048576 | tf_op jit(solution)/shard_map/all_to_all | solution.py:462
  223.8 0.7 shard_map.167
  (7 shorter events, 0.1 us)
Async XLA Ops:
  6.5 54.6 %collective-permute-start.2 = (bf16[8,4096]{1,0:T(8,128)(2,1)}, bf16[8,4096]{1,0:T(8,128)(2,1)S(1)}, u32[]{:S(2)}, u32[]{:S(2)}) collective-permute-start(bf16[8,4096]{1,0:T(8,128)(2,1)} %hidden.1), channel_id=1, source_target_pairs={{0,12},{1,13},{2,14},{3,15},{4,0},{5,1},{6,2},{7,3},{8,4},{9,5},{1... | collective-permute-start | bytes 196616 | tf_op jit(solution)/shard_map/ppermute | solution.py:520
  13.6 47.6 %collective-permute-start.1 = (bf16[8,4096]{1,0:T(8,128)(2,1)}, bf16[8,4096]{1,0:T(8,128)(2,1)S(1)}, u32[]{:S(2)}, u32[]{:S(2)}) collective-permute-start(bf16[8,4096]{1,0:T(8,128)(2,1)} %hidden.1), channel_id=1, source_target_pairs={{0,4},{1,5},{2,6},{3,7},{4,8},{5,9},{6,10},{7,11},{8,12},{9,13},{1... | collective-permute-start | bytes 196616 | tf_op jit(solution)/shard_map/ppermute | solution.py:520
  17.5 43.6 %copy-start = (bf16[8,4096]{1,0:T(8,128)(2,1)S(1)}, bf16[8,4096]{1,0:T(8,128)(2,1)}, u32[]{:S(2)}) copy-start(bf16[8,4096]{1,0:T(8,128)(2,1)} %hidden.1) | copy-start | bytes 196612
  17.5 56.9 %all-to-all-start = ((bf16[16,4,8,128]{3,2,1,0:T(8,128)(2,1)}), bf16[16,4,8,128]{3,2,1,0:T(8,128)(2,1)S(1)}, u32[]{:S(2)}, u32[]{:S(2)}) async-start(bf16[16,4,8,128]{3,2,1,0:T(8,128)(2,1)} %shard_map.163), calls=%async_computation | async-start | bytes 262144 | tf_op jit(solution)/shard_map/all_to_all | solution.py:462
  61.2 13.3 %collective-permute-start.4 = (bf16[2,8,4096]{2,1,0:T(8,128)(2,1)S(1)}, bf16[2,8,4096]{2,1,0:T(8,128)(2,1)S(1)}, u32[]{:S(2)}, u32[]{:S(2)}) collective-permute-start(bf16[2,8,4096]{2,1,0:T(8,128)(2,1)S(1)} %get-tuple-element.24), channel_id=1, source_target_pairs={{0,2},{1,3},{2,4},{3,5},{4,6},{5,7},{6,8},{7,9},{8,10},{9,11},{10,... | collective-permute-start | bytes 393224 | tf_op jit(solution)/shard_map/ppermute | solution.py:520
  63.6 17.0 %collective-permute-start.5 = (bf16[2,8,4096]{2,1,0:T(8,128)(2,1)S(1)}, bf16[2,8,4096]{2,1,0:T(8,128)(2,1)S(1)}, u32[]{:S(2)}, u32[]{:S(2)}) collective-permute-start(bf16[2,8,4096]{2,1,0:T(8,128)(2,1)S(1)} %get-tuple-element.23), channel_id=1, source_target_pairs={{0,14},{1,15},{2,0},{3,1},{4,2},{5,3},{6,4},{7,5},{8,6},{9,7},{10,... | collective-permute-start | bytes 393224 | tf_op jit(solution)/shard_map/ppermute | solution.py:520
  67.9 6.5 %collective-permute-start.3 = (bf16[8,4096]{1,0:T(8,128)(2,1)S(1)}, bf16[8,4096]{1,0:T(8,128)(2,1)S(1)}, u32[]{:S(2)}, u32[]{:S(2)}) collective-permute-start(bf16[8,4096]{1,0:T(8,128)(2,1)S(1)} %collective-permute-done.2), channel_id=1, source_target_pairs={{0,12},{1,13},{2,14},{3,15},{4,0},{5,1},{6,2},{7,3},{8,4},{9,5},{1... | collective-permute-start | bytes 196616 | tf_op jit(solution)/shard_map/ppermute | solution.py:520
  75.3 15.2 %all-to-all-start.1 = ((bf16[8,19,8,128]{3,2,1,0:T(8,128)(2,1)}), bf16[8,19,8,128]{3,2,1,0:T(8,128)(2,1)S(1)}, u32[]{:S(2)}, u32[]{:S(2)}) async-start(bf16[8,19,8,128]{3,2,1,0:T(8,128)(2,1)} %shard_map.164), calls=%async_computation.1 | async-start | bytes 622592 | tf_op jit(solution)/shard_map/all_to_all | solution.py:462
  80.5 17.1 %copy-start.1 = (bf16[8,4096]{1,0:T(8,128)(2,1)S(1)}, bf16[8,4096]{1,0:T(8,128)(2,1)}, u32[]{:S(2)}) copy-start(bf16[8,4096]{1,0:T(8,128)(2,1)} %context_.1) | copy-start | bytes 196612
  80.5 17.1 %copy-start.2 = (bf16[64,128]{1,0:T(8,128)(2,1)S(1)}, bf16[64,128]{1,0:T(8,128)(2,1)}, u32[]{:S(2)}) copy-start(bf16[64,128]{1,0:T(8,128)(2,1)} %fading_.1) | copy-start | bytes 49156
  80.5 17.1 %copy-start.3 = (bf16[64,128]{1,0:T(8,128)(2,1)S(1)}, bf16[64,128]{1,0:T(8,128)(2,1)}, u32[]{:S(2)}) copy-start(bf16[64,128]{1,0:T(8,128)(2,1)} %step_.1) | copy-start | bytes 49156
  80.6 17.1 %copy-start.6 = (f32[128]{0:T(128)S(1)}, f32[128]{0:T(128)}, u32[]{:S(2)}) copy-start(f32[128]{0:T(128)} %param.32) | copy-start | bytes 1540
  80.6 15.8 %collective-permute-start.6 = (bf16[8,8,4096]{2,1,0:T(8,128)(2,1)S(1)}, bf16[8,8,4096]{2,1,0:T(8,128)(2,1)S(1)}, u32[]{:S(2)}, u32[]{:S(2)}) collective-permute-start(bf16[8,8,4096]{2,1,0:T(8,128)(2,1)S(1)} %constant_dynamic-update-slice_fusion), channel_id=1, source_target_pairs={{0,1},{1,0},{2,3},{3,2},{4,5},{5,4},{6,7},{7,6},{8,9},{9,8},{10,11... | collective-permute-start | bytes 1572872 | tf_op jit(solution)/shard_map/ppermute | solution.py:466
  90.5 7.1 %collective-permute-start = (bf16[8,19,8,128]{3,2,1,0:T(8,128)(2,1)S(1)}, bf16[8,19,8,128]{3,2,1,0:T(8,128)(2,1)S(1)}, u32[]{:S(2)}, u32[]{:S(2)}) collective-permute-start(bf16[8,19,8,128]{3,2,1,0:T(8,128)(2,1)S(1)} %all-to-all-done.1.mine), channel_id=1, source_target_pairs={{0,1},{1,0},{2,3},{3,2},{4,5},{5,4},{6,7},{7,6},{8,9},{9,8},{10,11... | collective-permute-start | bytes 933896 | tf_op jit(solution)/shard_map/ppermute | solution.py:466
  96.4 1.2 copy-start.7
  97.6 0.7 copy-start.4
  97.6 0.7 copy-start.5
  105.5 79.2 %all-to-all-start.2 = ((bf16[16,152,128]{2,1,0:T(8,128)(2,1)}), bf16[16,152,128]{2,1,0:T(8,128)(2,1)S(1)}, u32[]{:S(2)}, u32[]{:S(2)}) async-start(bf16[16,152,128]{2,1,0:T(8,128)(2,1)} %get-tuple-element.14), calls=%async_computation.2 | async-start | bytes 1245184 | tf_op jit(solution)/shard_map/all_to_all | solution.py:462
  117.3 67.4 %all-gather.3.cloned.1.call-start = ((), (), s32[]{:S(2)}) async-start(), calls=%async_computation.4 | async-start | bytes 1114112 | tf_op jit(solution)/shard_map/all_gather | solution.py:516
  189.9 12.6 %collective-permute-start.7 = (bf16[8,8,4096]{2,1,0:T(8,128)(2,1)S(1)}, bf16[8,8,4096]{2,1,0:T(8,128)(2,1)S(1)}, u32[]{:S(2)}, u32[]{:S(2)}) collective-permute-start(bf16[8,8,4096]{2,1,0:T(8,128)(2,1)S(1)} %get-tuple-element.21), channel_id=1, source_target_pairs={{0,1},{1,0},{2,3},{3,2},{4,5},{5,4},{6,7},{7,6},{8,9},{9,8},{10,11... | collective-permute-start | bytes 1572872 | tf_op jit(solution)/shard_map/ppermute | solution.py:466
Sparse Core Ops, SparseCore 0:
  120.2 64.3 all-gather.2
